TPU v7x, 32 devices: a whole 2x2x4 slice. The times are simulated.
32 devices in a mesh: sp: 8 (over z, x), tp: 4 (over y, core).
Axes of the slice: x: 2, y: 2, z: 4, core: 2. Of those that a mesh axis runs over, the one named last changes fastest.
Arguments:
- stream_in: bfloat16 [2048, 2048], P(('sp', 'tp')), may hold values from -6 to 6
- queries: bfloat16 [2048, 4096], P('sp', 'tp'), may hold values from -6 to 6
- key_rows: bfloat16 [2048, 4096], P('sp', 'tp'), may hold values from -6 to 6
- values: bfloat16 [2048, 8192], P('sp', 'tp'), may hold values from -6 to 6
- decay_low: bfloat16 [2048, 16], P('sp'), may hold values from -4 to 4
- decay_matrix: bfloat16 [16, 4096], P(None, 'tp'), may hold values from -1.5 to 1.5
- decay_bias: float32 [4096], P('tp')
- decay_shift: float32 [2048, 16], P('sp', 'tp'), may hold values from -1 to 0
- head_gain: float32 [512], replicated, may hold values from 0.1 to 1.9
- output_matrix: bfloat16 [8192, 2048], P('tp'), may hold values from -0.0625 to 0.0625
- feed_gain: float32 [2048], replicated, may hold values from 0.1 to 1.9
- routes: int32 [2048, 2], P('sp'), may hold values from 0 to 7, all different within a row; in each aligned block of 256 rows (0 to 255, 256 to 511, ...) at most 64 rows name the same one
- route_weights: float32 [2048, 2], P('sp'), may hold values from 0.2 to 1
- expert_gate: bfloat16 [8, 2048, 2816], P('sp', None, 'tp'), may hold values from -0.125 to 0.125
- specialist_widen: bfloat16 [8, 2048, 2816], P('sp', None, 'tp'), may hold values from -0.125 to 0.125
- expert_down: bfloat16 [8, 2816, 2048], P('sp', 'tp'), may hold values from -0.109375 to 0.109375
Outputs:
- layer_out: bfloat16 [2048, 2048], P(('sp', 'tp'))
Inputs may be any that keep to these rules, and one draw needn't show every extreme that they name: `routes`: each row names 2 different experts; within each aligned block of 256 rows no expert is named by more than 64 rows, and in every draw some expert is named by exactly 64 rows of some block.
All inputs are finite; a program needn't handle non-finite values.
Results may differ from a plain program's by a relative error of at most 0.02.
Values may be sent and summed in bfloat16 or wider, within the bound.
No kernel may reach another device: no remote copies, remote signals or barrier semaphores. Data moves between devices by JAX's collectives and lax.ppermute only.
A program may use at most 128 MiB of HBM per device.

v0:
```python
import functools
import jax
import jax.numpy as jnp
from jax import lax
from jax.experimental import pallas as pl
from jax.experimental.pallas import tpu as pltpu
from jax.sharding import PartitionSpec as P


HK = 256
HV = 512
TOP = 2
BLK = 128
TEMPER = 16.0
EPSILON = 1e-06
F32 = jnp.float32
BF16 = jnp.bfloat16
VMEM = pl.BlockSpec(memory_space=pltpu.VMEM)
SMEM = pl.BlockSpec(memory_space=pltpu.SMEM)
HBM = pl.BlockSpec(memory_space=pltpu.HBM)
QUAD = 4


def cost(flops, moved):
    return pl.CostEstimate(flops=int(flops), bytes_accessed=int(moved), transcendentals=0)


def params(mib):
    return pltpu.CompilerParams(vmem_limit_bytes=mib * 1024 * 1024)


def xor_perm(axis, k):
    return [(i, i ^ k) for i in range(lax.axis_size(axis))]


def tri(n, fn):
    row = lax.broadcasted_iota(jnp.int32, (n, n), 0)
    col = lax.broadcasted_iota(jnp.int32, (n, n), 1)
    return fn(row, col)


def contract0(a, b):
    return lax.dot_general(a, b, (((0,), (0,)), ((), ())), preferred_element_type=F32)


def contract1(a, b):
    return lax.dot_general(a, b, (((1,), (1,)), ((), ())), preferred_element_type=F32)


def split_dot(ones, value):
    total = None
    for _ in range(3):
        part = value.astype(BF16)
        value = value - part.astype(F32)
        term = jnp.dot(ones, part, preferred_element_type=F32)
        total = term if total is None else total + term
    return total


def head_log_decay(low, matrix, bias, shift, head):
    pre = contract0(low, matrix) + bias
    logged = (jnp.minimum(pre, 0.0) - jnp.log1p(jnp.exp(-jnp.abs(pre)))) / TEMPER
    return logged + jnp.transpose(shift)[:, head : head + 1]


def state_kernel(first, count, idx, low, matrix, bias, shift, key_rows, values, *rest):
    outs, (keys, vals, state, decays, sems) = rest[:QUAD], rest[QUAD:]
    length = low.shape[1]
    piece = HK // QUAD
    copies = []
    for h in range(count):
        at = first + h
        pair = (
            pltpu.make_async_copy(
                key_rows.at[:, at * HK : (at + 1) * HK], keys.at[h], sems.at[0, h]
            ),
            pltpu.make_async_copy(
                values.at[:, at * HV : (at + 1) * HV], vals.at[h], sems.at[1, h]
            ),
        )
        for copy in pair:
            copy.start()
        copies.append(pair)
    after = tri(length, lambda r, c: c > r).astype(F32).astype(BF16)
    me = idx[0] % QUAD
    decays[...] = jnp.zeros_like(decays)
    for h in range(count):
        span = slice((first + h) * HK, (first + h + 1) * HK)
        logs = head_log_decay(low[...], matrix[:, span], bias[:, span], shift[...], first + h)
        suffix = split_dot(after, logs)
        total = jnp.exp(suffix[0:1, :] + logs[0:1, :])
        high = total.astype(BF16).astype(F32)
        decays[h : h + 1, 0:HK] = high
        decays[h : h + 1, HK : 2 * HK] = total - high
        for copy in copies[h]:
            copy.wait()
        end_keys = (keys[h].astype(F32) * jnp.exp(suffix)).astype(BF16)
        state[...] = contract0(end_keys, vals[h])
        for k in range(QUAD):
            start = pl.multiple_of((me ^ k) * piece, piece)
            outs[k][h * piece : (h + 1) * piece, :] = state[pl.ds(start, piece), :].astype(BF16)
    for k in range(QUAD):
        outs[k][count * piece :, :] = decays[...].astype(BF16)


def device_states(first, count, idx, low, matrix, bias, shift, key_rows, values):
    length = key_rows.shape[0]
    rows = count * (HK // QUAD) + 8
    return pl.pallas_call(
        functools.partial(state_kernel, first, count),
        in_specs=[SMEM, VMEM, VMEM, VMEM, VMEM, HBM, HBM],
        out_specs=[VMEM] * QUAD,
        out_shape=[jax.ShapeDtypeStruct((rows, HV), BF16)] * QUAD,
        scratch_shapes=[
            pltpu.VMEM((count, length, HK), BF16),
            pltpu.VMEM((count, length, HV), BF16),
            pltpu.VMEM((HK, HV), F32),
            pltpu.VMEM((8, HV), F32),
            pltpu.SemaphoreType.DMA((2, count)),
        ],
        compiler_params=params(60),
        cost_estimate=cost(count * 4e8, count * 5e5),
    )(idx, low, matrix, bias, shift, key_rows, values)


def local_kernel(low, matrix, bias, shift, queries, key_rows, values, out, query_out):
    length = low.shape[1]
    logs = head_log_decay(low[...], matrix[...], bias[...], shift[0], 0)
    below = tri(BLK, lambda r, c: c <= r)
    lower = below.astype(F32).astype(BF16)
    scale = HK ** (-0.5)
    before = jnp.zeros((1, HK), F32)
    earlier = []
    for b in range(length // BLK):
        rows = slice(b * BLK, (b + 1) * BLK)
        inside = split_dot(lower, logs[rows])
        final = inside[BLK - 1 : BLK, :]
        middle = inside[BLK // 2 - 1 : BLK // 2, :]
        query = queries[rows, :].astype(F32) * scale
        keys = key_rows[rows, :].astype(F32)
        grown = query * jnp.exp(inside)
        near_query = (query * jnp.exp(inside - middle)).astype(BF16)
        near_key = (keys * jnp.exp(middle - inside)).astype(BF16)
        scores = jnp.where(below, contract1(near_query, near_key), 0.0).astype(BF16)
        total = jnp.dot(scores, values[rows, :], preferred_element_type=F32)
        here = grown.astype(BF16)
        for past_keys, past_rows in earlier:
            cross = contract1(here, past_keys.astype(BF16)).astype(BF16)
            total = total + jnp.dot(cross, values[past_rows, :], preferred_element_type=F32)
        out[rows, :] = total
        query_out[rows, :] = (grown * jnp.exp(before)).astype(BF16)
        earlier = [(old * jnp.exp(final), old_rows) for old, old_rows in earlier]
        earlier.append((keys * jnp.exp(final - inside), rows))
        before = before + final


def local_attention(heads, low, matrix, bias, shift, queries, key_rows, values):
    length = low.shape[1]
    return pl.pallas_call(
        local_kernel,
        grid=(heads,),
        in_specs=[
            pl.BlockSpec(low.shape, lambda h: (0, 0)),
            pl.BlockSpec((low.shape[0], HK), lambda h: (0, h)),
            pl.BlockSpec((1, HK), lambda h: (0, h)),
            pl.BlockSpec((1, 1, length), lambda h: (h, 0, 0)),
            pl.BlockSpec((length, HK), lambda h: (0, h)),
            pl.BlockSpec((length, HK), lambda h: (0, h)),
            pl.BlockSpec((length, HV), lambda h: (0, h)),
        ],
        out_specs=[
            pl.BlockSpec((length, HV), lambda h: (0, h)),
            pl.BlockSpec((length, HK), lambda h: (0, h)),
        ],
        out_shape=[
            jax.ShapeDtypeStruct((length, heads * HV), F32),
            jax.ShapeDtypeStruct((length, heads * HK), BF16),
        ],
        compiler_params=params(24),
        cost_estimate=cost(heads * 4e8, heads * 1.2e6),
        name="local_attention",
    )(low, matrix, bias, shift.reshape(heads, 1, length), queries, key_rows, values)


def prefix_kernel(count, emit, idx, start, *refs):
    ins, outs, (stage, decays, result) = refs[:QUAD], refs[QUAD:-3], refs[-3:]
    me = idx[0] % QUAD
    piece = HK // QUAD
    rows = count * piece
    for k in range(QUAD):
        stage[me ^ k] = ins[k][:rows, :].astype(F32)
        tail = ins[k][rows:, :].astype(F32)
        decays[me ^ k] = jnp.transpose(tail[:, :HK] + tail[:, HK:])
    mine = pl.multiple_of(me * piece, piece)
    for h in range(count):
        span = slice(h * piece, (h + 1) * piece)
        carry = start[span, :].astype(F32)
        for i in range(QUAD):
            if emit:
                result[i, span, :] = carry
                if i == QUAD - 1:
                    break
            factor = decays[i, pl.ds(mine, piece), h : h + 1]
            carry = carry * factor + stage[i, span, :]
        if not emit:
            outs[0][span, :] = carry.astype(BF16)
    if emit:
        for k in range(QUAD):
            outs[k][...] = result[me ^ k].astype(BF16)


def quad_prefix(count, emit, idx, start, pieces):
    rows = count * (HK // QUAD)
    outs = QUAD if emit else 1
    return pl.pallas_call(
        functools.partial(prefix_kernel, count, emit),
        in_specs=[SMEM] + [VMEM] * (QUAD + 1),
        out_specs=[VMEM] * outs,
        out_shape=[jax.ShapeDtypeStruct((rows, HV), BF16)] * outs,
        scratch_shapes=[
            pltpu.VMEM((QUAD, rows, HV), F32),
            pltpu.VMEM((QUAD, HK, 8), F32),
            pltpu.VMEM((QUAD, rows, HV), F32),
        ],
        compiler_params=params(24),
        cost_estimate=cost(1e8, 1e6),
        name="quad_prefix" if emit else "quad_total",
    )(idx, start, *pieces)


def quad_entry(count, idx, pieces):
    rows = count * (HK // QUAD)
    start = jnp.zeros((rows, HV), BF16)
    quads = lax.axis_size("sp") // QUAD
    entry = None
    for g in range(quads - 1):
        (total,) = quad_prefix(count, False, idx, start, pieces)
        perm = [(g * QUAD + i, (g + 1) * QUAD + i) for i in range(QUAD)]
        start = lax.ppermute(total, "sp", perm)
        entry = start if entry is None else entry + start
    return start if entry is None else entry


def block_spans(idx, groups, rows):
    core, line = idx[1], idx[2]
    for k in range(groups):
        base = (line ^ k) * 2
        own = pl.ds(pl.multiple_of((base + core) * rows, rows), rows)
        other = pl.ds(pl.multiple_of((base + 1 - core) * rows, rows), rows)
        yield slice(k * rows, (k + 1) * rows), own, other


def project_kernel(count, heads, groups, idx, queries, local, gain, matrix, *refs):
    pieces, (keep, send, carried, total) = refs[:-4], refs[-4:]
    head = pl.program_id(0)
    me = idx[0] % QUAD
    piece = HK // QUAD

    @pl.when(head == 0)
    def _():
        total[...] = jnp.zeros_like(total)
        for at, ref in enumerate(pieces):
            start = pl.multiple_of((me ^ (at % QUAD)) * piece, piece)
            for h in range(count):
                span = slice(h * piece, (h + 1) * piece)
                spot = at // QUAD * count + h
                carried[spot, pl.ds(start, piece), :] = ref[span, :].astype(F32)

    out = local[...] + jnp.dot(
        queries[...], carried[head].astype(BF16), preferred_element_type=F32
    )
    spread = lax.rsqrt(jnp.mean(out * out, axis=-1, keepdims=True) + EPSILON)
    mixed = (out * spread * gain[...]).astype(BF16)
    total[...] += jnp.dot(mixed, matrix[...], preferred_element_type=F32)

    @pl.when(head == heads - 1)
    def _():
        for span, own, other in block_spans(idx, groups, keep.shape[0] // groups):
            keep[span, :] = total[own, :]
            send[span, :] = total[other, :].astype(BF16)


def project(count, heads, groups, idx, queries, local, gain, matrix, pieces):
    length = queries.shape[0]
    width = matrix.shape[1]
    rows = count * (HK // QUAD)
    return pl.pallas_call(
        functools.partial(project_kernel, count, heads, groups),
        grid=(heads,),
        in_specs=[
            SMEM,
            pl.BlockSpec((length, HK), lambda h: (0, h)),
            pl.BlockSpec((length, HV), lambda h: (0, h)),
            pl.BlockSpec((1, HV), lambda h: (0, 0)),
            pl.BlockSpec((HV, width), lambda h: (h, 0)),
        ]
        + [pl.BlockSpec((rows, HV), lambda h: (0, 0))] * len(pieces),
        out_specs=[pl.BlockSpec((length // 2, width), lambda h: (0, 0))] * 2,
        out_shape=[
            jax.ShapeDtypeStruct((length // 2, width), F32),
            jax.ShapeDtypeStruct((length // 2, width), BF16),
        ],
        scratch_shapes=[
            pltpu.VMEM((heads, HK, HV), F32),
            pltpu.VMEM((length, width), F32),
        ],
        compiler_params=params(32),
        cost_estimate=cost(heads * 7e8, heads * 2.5e6),
        name="project",
    )(idx, queries, local, gain, matrix, *pieces)


def norm_kernel(groups, gain, keep, received, *refs):
    streams, arrived = refs[:groups], refs[groups : 2 * groups - 1]
    normed, mid = refs[2 * groups - 1 :]
    rows = mid.shape[0]
    for k in range(groups):
        span = slice(k * rows, (k + 1) * rows)
        value = keep[span, :] + received[span, :].astype(F32)
        for j in range(1, groups):
            there = k ^ j
            value = value + arrived[j - 1][there * rows : (there + 1) * rows, :].astype(F32)
        value = value + streams[k][...].astype(F32)
        if k == 0:
            mid[...] = value
        spread = lax.rsqrt(jnp.mean(value * value, axis=-1, keepdims=True) + EPSILON)
        normed[span, :] = (value * spread * gain[...]).astype(BF16)


def midstream_norm(groups, gain, keep, received, streams, arrived):
    rows, width = streams[0].shape
    return pl.pallas_call(
        functools.partial(norm_kernel, groups),
        in_specs=[VMEM] * (3 + 2 * groups - 1),
        out_specs=[VMEM] * 2,
        out_shape=[
            jax.ShapeDtypeStruct((groups * rows, width), BF16),
            jax.ShapeDtypeStruct((rows, width), F32),
        ],
        compiler_params=params(24),
        cost_estimate=cost(1e7, 3e6),
        name="midstream_norm",
    )(gain, keep, received, *streams, *arrived)


def route_kernel(n, half, idx, routes, weights, select, high, low):
    me, core = idx[0], idx[1]
    length = routes.shape[1]
    earlier = tri(length, lambda r, c: r < c).astype(F32).astype(BF16)
    first, second = routes[0:1, :], routes[1:2, :]
    expert = me ^ lax.broadcasted_iota(jnp.int32, (n, length), 0)
    is_first, is_second = first == expert, second == expert
    member = jnp.where(is_first | is_second, 1.0, 0.0)
    rank = jnp.dot(member.astype(BF16), earlier, preferred_element_type=F32)
    slot = jnp.where(member > 0.0, rank.astype(jnp.int32), -1)
    weight = jnp.where(is_first, weights[0:1, :], weights[1:2, :])
    for k in range(n):
        wanted = core * half + lax.broadcasted_iota(jnp.int32, (half, length), 0)
        hit = slot[k : k + 1, :] == wanted
        span = slice(k * half, (k + 1) * half)
        select[span, :] = jnp.where(hit, 1.0, 0.0).astype(BF16)
        value = jnp.where(hit, weight[k : k + 1, :], 0.0)
        top = value.astype(BF16)
        high[span, :] = top
        low[span, :] = (value - top.astype(F32)).astype(BF16)


def slot_tables(n, half, idx, routes, weights):
    length = routes.shape[1]
    return pl.pallas_call(
        functools.partial(route_kernel, n, half),
        in_specs=[SMEM, VMEM, VMEM],
        out_specs=[VMEM] * 3,
        out_shape=[jax.ShapeDtypeStruct((n * half, length), BF16)] * 3,
        compiler_params=params(16),
        cost_estimate=cost(1e8, 5e5),
        name="slot_tables",
    )(idx, routes, weights)


def dispatch_kernel(n, half, groups, idx, select, mine, theirs, *refs):
    outs, group = refs[:n], refs[n]
    rows = mine.shape[0] // groups
    for span, own, other in block_spans(idx, groups, rows):
        group[own, :] = mine[span, :]
        group[other, :] = theirs[span, :]
    for k in range(n):
        chosen = select[k * half : (k + 1) * half, :]
        outs[k][...] = jnp.dot(chosen, group[...], preferred_element_type=F32).astype(BF16)


def dispatch(n, half, groups, idx, select, mine, theirs):
    width = mine.shape[1]
    return pl.pallas_call(
        functools.partial(dispatch_kernel, n, half, groups),
        in_specs=[SMEM] + [VMEM] * 3,
        out_specs=[VMEM] * n,
        out_shape=[jax.ShapeDtypeStruct((half, width), BF16)] * n,
        scratch_shapes=[pltpu.VMEM((select.shape[1], width), BF16)],
        compiler_params=params(16),
        cost_estimate=cost(5e8, 2e6),
        name="dispatch",
    )(idx, select, mine, theirs)


def fetch_kernel(*refs):
    half = (len(refs) - 1) // 2
    ins, outs, sems = refs[:half], refs[half:-1], refs[-1]
    copies = [
        pltpu.make_async_copy(src, dst, sems.at[i])
        for i, (src, dst) in enumerate(zip(ins, outs))
    ]
    for copy in copies:
        copy.start()
    for copy in copies:
        copy.wait()


def fetch(*arrays):
    return pl.pallas_call(
        fetch_kernel,
        in_specs=[HBM] * len(arrays),
        out_specs=[VMEM] * len(arrays),
        out_shape=[jax.ShapeDtypeStruct(a.shape, a.dtype) for a in arrays],
        scratch_shapes=[pltpu.SemaphoreType.DMA((len(arrays),))],
        compiler_params=params(16),
        cost_estimate=cost(2e9, 1e7),
        name="fetch",
    )(*arrays)


def expert_kernel(count, gate, widen, down, *refs):
    ins, (keep, send) = refs[: 2 * count], refs[2 * count :]
    rows = jnp.concatenate([piece[...] for piece in ins], axis=0)
    gated = contract1(rows, gate[...])
    lifted = contract1(rows, widen[...])
    hidden = (gated * jax.nn.sigmoid(gated) * lifted).astype(BF16)
    out = jnp.dot(hidden, down[...], preferred_element_type=F32)
    split = keep.shape[0]
    keep[...] = out[:split, :]
    send[...] = out[split:, :].astype(BF16)


def expert(weights, mine, theirs):
    count = len(mine)
    half, width = mine[0].shape
    return pl.pallas_call(
        functools.partial(expert_kernel, count),
        in_specs=[VMEM] * (3 + 2 * count),
        out_specs=[VMEM] * 2,
        out_shape=[
            jax.ShapeDtypeStruct((count * half, width), F32),
            jax.ShapeDtypeStruct((count * half, width), BF16),
        ],
        compiler_params=params(24),
        cost_estimate=cost(6e8 * count, 4e6),
    )(*weights, *mine, *theirs)


def merge_kernel(count, keep, received, *outs):
    half = outs[0].shape[0]
    for k in range(count):
        span = slice(k * half, (k + 1) * half)
        outs[k][...] = (keep[span, :] + received[span, :].astype(F32)).astype(BF16)


def merge(count, half, keep, received):
    width = keep.shape[1]
    return pl.pallas_call(
        functools.partial(merge_kernel, count),
        in_specs=[VMEM] * 2,
        out_specs=[VMEM] * count,
        out_shape=[jax.ShapeDtypeStruct((half, width), BF16)] * count,
        compiler_params=params(16),
        cost_estimate=cost(1e7, 4e6),
    )(keep, received)


def combine_kernel(n, groups, idx, high, low, *refs):
    ins, (keep, send, total) = refs[:n], refs[n:]
    rows = jnp.concatenate([piece[...] for piece in ins], axis=0)
    total[...] = contract0(high[...], rows) + contract0(low[...], rows)
    for span, own, other in block_spans(idx, groups, keep.shape[0] // groups):
        keep[span, :] = total[own, :]
        send[span, :] = total[other, :].astype(BF16)


def combine(n, groups, idx, high, low, pieces):
    width = pieces[0].shape[1]
    length = high.shape[1]
    return pl.pallas_call(
        functools.partial(combine_kernel, n, groups),
        in_specs=[SMEM] + [VMEM] * (2 + n),
        out_specs=[VMEM] * 2,
        out_shape=[
            jax.ShapeDtypeStruct((length // 2, width), F32),
            jax.ShapeDtypeStruct((length // 2, width), BF16),
        ],
        scratch_shapes=[pltpu.VMEM((length, width), F32)],
        compiler_params=params(16),
        cost_estimate=cost(1e9, 3e6),
        name="combine",
    )(idx, high, low, *pieces)


def swap(value, axis, k):
    return lax.ppermute(value, axis, xor_perm(axis, k))


def exchange(pieces):
    return [pieces[0]] + [swap(pieces[k], "sp", k) for k in range(1, len(pieces))]


def body(
    stream_in,
    queries,
    key_rows,
    values,
    decay_low,
    decay_matrix,
    decay_bias,
    decay_shift,
    head_gain,
    output_matrix,
    feed_gain,
    routes,
    route_weights,
    expert_gate,
    specialist_widen,
    expert_down,
):
    length = queries.shape[0]
    heads = queries.shape[1] // HK
    n = lax.axis_size("sp")
    head_devices = lax.axis_size("tp")
    groups = head_devices // 2
    me, tp = lax.axis_index("sp"), lax.axis_index("tp")
    core, line = tp % 2, tp // 2
    idx = jnp.stack([me, core, line]).astype(jnp.int32)
    rows = length // head_devices
    half = TOP * length // n // 2
    bias = decay_bias.reshape(1, -1)

    low, shift = decay_low.T, decay_shift.T
    count = heads // 2 if heads % 2 == 0 else heads

    gathered, states = [], None
    for part, first in enumerate(range(0, heads, count)):
        head_idx = idx
        if states is not None:
            head_idx, states = lax.optimization_barrier((idx, states))
        states = device_states(
            first, count, head_idx, low, decay_matrix, bias, shift, key_rows, values
        )
        gathered.append(exchange(states))
    stream_in, _ = lax.optimization_barrier((stream_in, states))
    streams = [stream_in] + [swap(stream_in, "tp", 2 * k) for k in range(1, groups)]
    local, late_queries = local_attention(
        heads, low, decay_matrix, bias, shift, queries, key_rows, values
    )
    select, high, low_part = slot_tables(n, half, idx, routes.T, route_weights.T)
    gathered[0], streams, local, late_queries = lax.optimization_barrier(
        (gathered[0], streams, local, late_queries)
    )
    carried = []
    for part, pieces in enumerate(gathered):
        entry = quad_entry(count, idx, pieces)
        carried += exchange(quad_prefix(count, True, idx, entry, pieces))
    carried, select, high, low_part = lax.optimization_barrier(
        (carried, select, high, low_part)
    )
    keep, send = project(
        count,
        heads,
        groups,
        idx,
        late_queries,
        local,
        head_gain.reshape(1, -1),
        output_matrix,
        carried,
    )
    received = swap(send, "tp", 1)
    shared = (keep + received.astype(F32)).astype(BF16)
    arrived = [swap(shared, "tp", 2 * k) for k in range(1, groups)]
    weights, _ = lax.optimization_barrier(
        ((expert_gate[0].T, specialist_widen[0].T, expert_down[0]), shared)
    )
    weights = fetch(*weights)
    arrived, weights = lax.optimization_barrier((arrived, weights))
    normed, mid = midstream_norm(
        groups, feed_gain.reshape(1, -1), keep, received, streams, arrived
    )
    theirs = swap(normed, "tp", 1)
    slots = dispatch(n, half, groups, idx, select, normed, theirs)
    slots = exchange(slots)
    back, previous = {}, None
    for part, ks in enumerate(expert_chunks(n)):
        mine = [slots[k] for k in ks]
        if previous is not None:
            mine, previous = lax.optimization_barrier((mine, previous))
        theirs = [swap(slot, "tp", 1) for slot in mine]
        kept, sent = expert(weights, mine, theirs)
        received = swap(sent, "tp", 1)
        merged = merge(len(ks), half, kept, received)
        previous = merged
        for k, piece in zip(ks, merged):
            back[k] = piece if k == 0 else swap(piece, "sp", k)
    back = [back[k] for k in range(n)]
    keep, send = combine(n, groups, idx, high, low_part, back)
    summed = keep + swap(send, "tp", 1).astype(F32)
    total = mid + summed[:rows]
    for k in range(1, groups):
        part = summed[k * rows : (k + 1) * rows].astype(BF16)
        total = total + swap(part, "tp", 2 * k).astype(F32)
    return total.astype(BF16)


def expert_chunks(n):
    middle = (QUAD + n) // 2
    return [range(QUAD), range(QUAD, middle), range(middle, n)]


def solution(mesh):
    return jax.shard_map(
        body,
        mesh=mesh,
        in_specs=(
            P(("sp", "tp"), None),
            P("sp", "tp"),
            P("sp", "tp"),
            P("sp", "tp"),
            P("sp", None),
            P(None, "tp"),
            P("tp"),
            P("sp", "tp"),
            P(),
            P("tp", None),
            P(),
            P("sp", None),
            P("sp", None),
            P("sp", None, "tp"),
            P("sp", None, "tp"),
            P("sp", "tp", None),
        ),
        out_specs=P(("sp", "tp"), None),
        check_vma=False,
    )
```

profile of v0, /device:TPU:0, one launch (start us, length us, event | category | flops | bytes accessed | tf_op | source)
XLA Modules:
  0.0 164.1 jit_solution(5309360915073541017)
XLA Ops:
  0.7 4.0 %shard_map.154 = (bf16[136,512]{1,0:T(8,128)(2,1)}, bf16[136,512]{1,0:T(8,128)(2,1)}, bf16[136,512]{1,0:T(8,128)(2,1)}, bf16[136,512]{1,0:T(8,128)(2,1)}) custom-call(s32[3]{0:T(128)} %pad_add_fusion.idx, bf16[16,256]{1,0:T(8,128)(2,1)} %bitcast.22, bf16[16,1024]{1,0:T(8,128)(2,1)} %matrix.6, f32[1,1024]{1,0:T(1,128)} %bitcast.25, f32[4,256]{1,0:T(4,128)} %bitcast.30, ...), custom_call_target="tpu_custom_call" | custom-call | flops 800000000 | bytes 1000000 | tf_op jit(solution)/shard_map/pallas_call | solution.py:109
  4.7 3.9 %shard_map.155 = (bf16[136,512]{1,0:T(8,128)(2,1)}, bf16[136,512]{1,0:T(8,128)(2,1)}, bf16[136,512]{1,0:T(8,128)(2,1)}, bf16[136,512]{1,0:T(8,128)(2,1)}) custom-call(s32[3]{0:T(128)} %pad_add_fusion.idx, bf16[16,256]{1,0:T(8,128)(2,1)} %bitcast.23, bf16[16,1024]{1,0:T(8,128)(2,1)} %matrix.6, f32[1,1024]{1,0:T(1,128)} %bitcast.26, f32[4,256]{1,0:T(4,128)} %bitcast.31, ...), custom_call_target="tpu_custom_call" | custom-call | flops 800000000 | bytes 1000000 | tf_op jit(solution)/shard_map/pallas_call | solution.py:109
  8.7 3.0 %collective-permute-start.8 = (bf16[136,512]{1,0:T(8,128)(2,1)}, bf16[136,512]{1,0:T(8,128)(2,1)S(1)}, u32[]{:S(2)}, u32[]{:S(2)}) collective-permute-start(bf16[136,512]{1,0:T(8,128)(2,1)} %get-tuple-element.95), channel_id=1, source_target_pairs={{0,4},{4,0},{8,12},{12,8},{16,20},{20,16},{24,28},{28,24},{1,5},{5... | collective-permute-start | bytes 417800 | tf_op jit(solution)/shard_map/ppermute | solution.py:507
  22.9 4.8 %collective-permute-start.11 = (bf16[128,512]{1,0:T(8,128)(2,1)S(1)}, bf16[128,512]{1,0:T(8,128)(2,1)S(1)}, u32[]{:S(2)}, u32[]{:S(2)}) collective-permute-start(bf16[128,512]{1,0:T(8,128)(2,1)S(1)} %quad_total.3), channel_id=1, source_target_pairs={{0,16},{4,20},{8,24},{12,28},{1,17},{5,21},{9,25},{13,29},{2,18},{... | collective-permute-start | bytes 393224 | tf_op jit(solution)/shard_map/ppermute | solution.py:239
  27.7 5.9 %local_attention.1 = (f32[256,2048]{1,0:T(8,128)S(1)}, bf16[256,1024]{1,0:T(8,128)(2,1)S(1)}) custom-call(bf16[16,256]{1,0:T(8,128)(2,1)S(1)} %bitcast.24, bf16[16,1024]{1,0:T(8,128)(2,1)S(1)} %copy-done.14, f32[1,1024]{1,0:T(1,128)S(1)} %bitcast.27, f32[4,1,256]{2,1,0:T(1,128)S(1)} %reshape.14.shift, bf16[256,1024]{1,0:T(8,128)(2,1)S(1)} %copy-done.12, ...), custom_call_target="tpu_custom_call" | custom-call | flops 1600000000 | bytes 4800000 | tf_op jit(solution)/shard_map/local_attention/pallas_call | solution.py:159
  45.0 2.7 %collective-permute-start.7 = (bf16[128,512]{1,0:T(8,128)(2,1)S(1)}, bf16[128,512]{1,0:T(8,128)(2,1)S(1)}, u32[]{:S(2)}, u32[]{:S(2)}) collective-permute-start(bf16[128,512]{1,0:T(8,128)(2,1)S(1)} %get-tuple-element.110), channel_id=1, source_target_pairs={{0,12},{4,8},{8,4},{12,0},{16,28},{20,24},{24,20},{28,16},{1,13},{... | collective-permute-start | bytes 393224 | tf_op jit(solution)/shard_map/ppermute | solution.py:507
  50.9 5.3 %project.1 = (f32[128,2048]{1,0:T(8,128)S(1)}, bf16[128,2048]{1,0:T(8,128)(2,1)S(1)}) custom-call(s32[3]{0:T(128)S(1)} %copy-done.8, bf16[256,1024]{1,0:T(8,128)(2,1)S(1)} %get-tuple-element.101.queries, f32[256,2048]{1,0:T(8,128)S(1)} %get-tuple-element.102.local, f32[1,512]{1,0:T(1,128)S(1)} %bitcast.21, bf16[2048,2048]{1,0:T(8,128)(2,1)S(1)} %copy-done, ...), custom_call_target="tpu_custom_call" | custom-call | flops 2800000000 | bytes 10000000 | tf_op jit(solution)/shard_map/project/pallas_call | solution.py:287
  60.5 11.8 %collective-permute-done.16.refs_2_ = bf16[128,2048]{1,0:T(8,128)(2,1)S(1)} collective-permute-done((bf16[128,2048]{1,0:T(8,128)(2,1)S(1)}, bf16[128,2048]{1,0:T(8,128)(2,1)S(1)}, u32[]{:S(2)}, u32[]{:S(2)}) %collective-permute-start.16) | collective-permute-done | bytes 524320 | tf_op jit(solution)/shard_map/ppermute | solution.py:507
  74.7 2.2 %dispatch.1 = (bf16[32,2048]{1,0:T(8,128)(2,1)S(1)}, bf16[32,2048]{1,0:T(8,128)(2,1)S(1)}, bf16[32,2048]{1,0:T(8,128)(2,1)S(1)}, bf16[32,2048]{1,0:T(8,128)(2,1)...) custom-call(s32[3]{0:T(128)S(1)} %copy-done.8, ...), custom_call_target="tpu_custom_call" | custom-call | flops 500000000 | bytes 2000000 | tf_op jit(solution)/shard_map/dispatch/pallas_call | solution.py:394
  77.9 2.3 %collective-permute-start.19 = (bf16[32,2048]{1,0:T(8,128)(2,1)S(1)}, bf16[32,2048]{1,0:T(8,128)(2,1)S(1)}, u32[]{:S(2)}, u32[]{:S(2)}) collective-permute-start(bf16[32,2048]{1,0:T(8,128)(2,1)S(1)} %get-tuple-element.147), channel_id=1, source_target_pairs={{0,8},{4,12},{8,0},{12,4},{16,24},{20,28},{24,16},{28,20},{1,9},{5... | collective-permute-start | bytes 393224 | tf_op jit(solution)/shard_map/ppermute | solution.py:507
  87.8 2.6 %shard_map.156 = (f32[128,2048]{1,0:T(8,128)S(1)}, bf16[128,2048]{1,0:T(8,128)(2,1)S(1)}) custom-call(bf16[704,2048]{1,0:T(8,128)(2,1)S(1)} %get-tuple-element.140.gate, bf16[704,2048]{1,0:T(8,128)(2,1)S(1)} %get-tuple-element.141.widen, bf16[704,2048]{1,0:T(8,128)(2,1)S(1)} %get-tuple-element.142.down, bf16[32,2048]{1,0:T(8,128)(2,1)S(1)} %get-tuple-element.145.refs_0_, ...), custom_call_target="tpu_custom_call" | custom-call | flops 2400000000 | bytes 4000000 | tf_op jit(solution)/shard_map/pallas_call | solution.py:447
  90.7 2.7 %collective-permute-start.29 = (bf16[32,2048]{1,0:T(8,128)(2,1)S(1)}, bf16[32,2048]{1,0:T(8,128)(2,1)S(1)}, u32[]{:S(2)}, u32[]{:S(2)}) collective-permute-start(bf16[32,2048]{1,0:T(8,128)(2,1)S(1)} %get-tuple-element.155), channel_id=1, source_target_pairs={{0,16},{4,20},{8,24},{12,28},{16,0},{20,4},{24,8},{28,12},{1,17},{... | collective-permute-start | bytes 393224 | tf_op jit(solution)/shard_map/ppermute | solution.py:507
  94.7 8.9 %collective-permute-done.29.refs_0_ = bf16[32,2048]{1,0:T(8,128)(2,1)S(1)} collective-permute-done((bf16[32,2048]{1,0:T(8,128)(2,1)S(1)}, bf16[32,2048]{1,0:T(8,128)(2,1)S(1)}, u32[]{:S(2)}, u32[]{:S(2)}) %collective-permute-start.29) | collective-permute-done | bytes 131104 | tf_op jit(solution)/shard_map/ppermute | solution.py:507
  103.6 3.2 %collective-permute-done.30.refs_1_ = bf16[32,2048]{1,0:T(8,128)(2,1)S(1)} collective-permute-done((bf16[32,2048]{1,0:T(8,128)(2,1)S(1)}, bf16[32,2048]{1,0:T(8,128)(2,1)S(1)}, u32[]{:S(2)}, u32[]{:S(2)}) %collective-permute-start.30) | collective-permute-done | bytes 131104 | tf_op jit(solution)/shard_map/ppermute | solution.py:507
  108.3 2.4 %shard_map.158 = (f32[64,2048]{1,0:T(8,128)S(1)}, bf16[64,2048]{1,0:T(8,128)(2,1)S(1)}) custom-call(bf16[704,2048]{1,0:T(8,128)(2,1)S(1)} %get-tuple-element.140.gate, bf16[704,2048]{1,0:T(8,128)(2,1)S(1)} %get-tuple-element.141.widen, bf16[704,2048]{1,0:T(8,128)(2,1)S(1)} %get-tuple-element.142.down, bf16[32,2048]{1,0:T(8,128)(2,1)S(1)} %collective-permute-done.29.refs_0_, ...), custom_call_target="tpu_custom_call" | custom-call | flops 1200000000 | bytes 4000000 | tf_op jit(solution)/shard_map/pallas_call | solution.py:447
  111.0 2.4 %collective-permute-start.36 = (bf16[32,2048]{1,0:T(8,128)(2,1)S(1)}, bf16[32,2048]{1,0:T(8,128)(2,1)S(1)}, u32[]{:S(2)}, u32[]{:S(2)}) collective-permute-start(bf16[32,2048]{1,0:T(8,128)(2,1)S(1)} %get-tuple-element.163), channel_id=1, source_target_pairs={{0,24},{4,28},{8,16},{12,20},{16,8},{20,12},{24,0},{28,4},{1,25},{... | collective-permute-start | bytes 393224 | tf_op jit(solution)/shard_map/ppermute | solution.py:507
  114.9 4.2 %collective-permute-done.36.refs_0_ = bf16[32,2048]{1,0:T(8,128)(2,1)S(1)} collective-permute-done((bf16[32,2048]{1,0:T(8,128)(2,1)S(1)}, bf16[32,2048]{1,0:T(8,128)(2,1)S(1)}, u32[]{:S(2)}, u32[]{:S(2)}) %collective-permute-start.36) | collective-permute-done | bytes 131104 | tf_op jit(solution)/shard_map/ppermute | solution.py:507
  119.1 2.3 %collective-permute-done.37.refs_1_ = bf16[32,2048]{1,0:T(8,128)(2,1)S(1)} collective-permute-done((bf16[32,2048]{1,0:T(8,128)(2,1)S(1)}, bf16[32,2048]{1,0:T(8,128)(2,1)S(1)}, u32[]{:S(2)}, u32[]{:S(2)}) %collective-permute-start.37) | collective-permute-done | bytes 131104 | tf_op jit(solution)/shard_map/ppermute | solution.py:507
  123.0 2.4 %shard_map.160 = (f32[64,2048]{1,0:T(8,128)S(1)}, bf16[64,2048]{1,0:T(8,128)(2,1)S(1)}) custom-call(bf16[704,2048]{1,0:T(8,128)(2,1)S(1)} %get-tuple-element.140.gate, bf16[704,2048]{1,0:T(8,128)(2,1)S(1)} %get-tuple-element.141.widen, bf16[704,2048]{1,0:T(8,128)(2,1)S(1)} %get-tuple-element.142.down, bf16[32,2048]{1,0:T(8,128)(2,1)S(1)} %collective-permute-done.36.refs_0_, ...), custom_call_target="tpu_custom_call" | custom-call | flops 1200000000 | bytes 4000000 | tf_op jit(solution)/shard_map/pallas_call | solution.py:447
  127.1 2.5 %collective-permute-start.27 = (bf16[32,2048]{1,0:T(8,128)(2,1)S(1)}, bf16[32,2048]{1,0:T(8,128)(2,1)S(1)}, u32[]{:S(2)}, u32[]{:S(2)}) collective-permute-start(bf16[32,2048]{1,0:T(8,128)(2,1)S(1)} %get-tuple-element.153), channel_id=1, source_target_pairs={{0,8},{4,12},{8,0},{12,4},{16,24},{20,28},{24,16},{28,20},{1,9},{5... | collective-permute-start | bytes 393224 | tf_op jit(solution)/shard_map/ppermute | solution.py:507
  135.5 4.9 %collective-permute-start.42 = (bf16[32,2048]{1,0:T(8,128)(2,1)S(1)}, bf16[32,2048]{1,0:T(8,128)(2,1)S(1)}, u32[]{:S(2)}, u32[]{:S(2)}) collective-permute-start(bf16[32,2048]{1,0:T(8,128)(2,1)S(1)} %get-tuple-element.170), channel_id=1, source_target_pairs={{0,28},{4,24},{8,20},{12,16},{16,12},{20,8},{24,4},{28,0},{1,29},{... | collective-permute-start | bytes 393224 | tf_op jit(solution)/shard_map/ppermute | solution.py:507
  141.2 7.8 %collective-permute-done.34.refs_4_ = bf16[32,2048]{1,0:T(8,128)(2,1)S(1)} collective-permute-done((bf16[32,2048]{1,0:T(8,128)(2,1)S(1)}, bf16[32,2048]{1,0:T(8,128)(2,1)S(1)}, u32[]{:S(2)}, u32[]{:S(2)}) %collective-permute-start.34) | collective-permute-done | bytes 131104 | tf_op jit(solution)/shard_map/ppermute | solution.py:507
  149.0 2.4 %collective-permute-done.35.refs_5_ = bf16[32,2048]{1,0:T(8,128)(2,1)S(1)} collective-permute-done((bf16[32,2048]{1,0:T(8,128)(2,1)S(1)}, bf16[32,2048]{1,0:T(8,128)(2,1)S(1)}, u32[]{:S(2)}, u32[]{:S(2)}) %collective-permute-start.35) | collective-permute-done | bytes 131104 | tf_op jit(solution)/shard_map/ppermute | solution.py:507
  156.5 6.8 %collective-permute-done.44 = bf16[64,2048]{1,0:T(8,128)(2,1)S(1)} collective-permute-done((bf16[64,2048]{1,0:T(8,128)(2,1)S(1)}, bf16[64,2048]{1,0:T(8,128)(2,1)S(1)}, u32[]{:S(2)}, u32[]{:S(2)}) %collective-permute-start.44) | collective-permute-done | bytes 262176 | tf_op jit(solution)/shard_map/ppermute | solution.py:507
  (138 shorter events, 62.2 us)
Async XLA Ops:
  8.7 8.1 %collective-permute-start.8 = (bf16[136,512]{1,0:T(8,128)(2,1)}, bf16[136,512]{1,0:T(8,128)(2,1)S(1)}, u32[]{:S(2)}, u32[]{:S(2)}) collective-permute-start(bf16[136,512]{1,0:T(8,128)(2,1)} %get-tuple-element.95), channel_id=1, source_target_pairs={{0,4},{4,0},{8,12},{12,8},{16,20},{20,16},{24,28},{28,24},{1,5},{5... | collective-permute-start | bytes 417800 | tf_op jit(solution)/shard_map/ppermute | solution.py:507
  13.3 7.7 %collective-permute-start.10 = (bf16[136,512]{1,0:T(8,128)(2,1)}, bf16[136,512]{1,0:T(8,128)(2,1)S(1)}, u32[]{:S(2)}, u32[]{:S(2)}) collective-permute-start(bf16[136,512]{1,0:T(8,128)(2,1)} %get-tuple-element.97), channel_id=1, source_target_pairs={{0,12},{4,8},{8,4},{12,0},{16,28},{20,24},{24,20},{28,16},{1,13},{... | collective-permute-start | bytes 417800 | tf_op jit(solution)/shard_map/ppermute | solution.py:507
  13.3 20.3 %collective-permute-start.3 = (bf16[64,2048]{1,0:T(8,128)(2,1)S(1)}, bf16[64,2048]{1,0:T(8,128)(2,1)S(1)}, u32[]{:S(2)}, u32[]{:S(2)}) collective-permute-start(bf16[64,2048]{1,0:T(8,128)(2,1)S(1)} %copy-done.7), channel_id=1, source_target_pairs={{0,2},{1,3},{2,0},{3,1},{4,6},{5,7},{6,4},{7,5},{8,10},{9,11},{10,... | collective-permute-start | bytes 786440 | tf_op jit(solution)/shard_map/ppermute | solution.py:507
  15.2 18.4 %collective-permute-start = (bf16[136,512]{1,0:T(8,128)(2,1)S(1)}, bf16[136,512]{1,0:T(8,128)(2,1)S(1)}, u32[]{:S(2)}, u32[]{:S(2)}) collective-permute-start(bf16[136,512]{1,0:T(8,128)(2,1)S(1)} %copy-done.22), channel_id=1, source_target_pairs={{0,4},{4,0},{8,12},{12,8},{16,20},{20,16},{24,28},{28,24},{1,5},{5... | collective-permute-start | bytes 417800 | tf_op jit(solution)/shard_map/ppermute | solution.py:507
  16.7 16.9 %collective-permute-start.1 = (bf16[136,512]{1,0:T(8,128)(2,1)S(1)}, bf16[136,512]{1,0:T(8,128)(2,1)S(1)}, u32[]{:S(2)}, u32[]{:S(2)}) collective-permute-start(bf16[136,512]{1,0:T(8,128)(2,1)S(1)} %copy-done.21), channel_id=1, source_target_pairs={{0,8},{4,12},{8,0},{12,4},{16,24},{20,28},{24,16},{28,20},{1,9},{5... | collective-permute-start | bytes 417800 | tf_op jit(solution)/shard_map/ppermute | solution.py:507
  18.4 15.2 %collective-permute-start.2 = (bf16[136,512]{1,0:T(8,128)(2,1)S(1)}, bf16[136,512]{1,0:T(8,128)(2,1)S(1)}, u32[]{:S(2)}, u32[]{:S(2)}) collective-permute-start(bf16[136,512]{1,0:T(8,128)(2,1)S(1)} %copy-done.20), channel_id=1, source_target_pairs={{0,12},{4,8},{8,4},{12,0},{16,28},{20,24},{24,20},{28,16},{1,13},{... | collective-permute-start | bytes 417800 | tf_op jit(solution)/shard_map/ppermute | solution.py:507
  22.9 13.0 %collective-permute-start.11 = (bf16[128,512]{1,0:T(8,128)(2,1)S(1)}, bf16[128,512]{1,0:T(8,128)(2,1)S(1)}, u32[]{:S(2)}, u32[]{:S(2)}) collective-permute-start(bf16[128,512]{1,0:T(8,128)(2,1)S(1)} %quad_total.3), channel_id=1, source_target_pairs={{0,16},{4,20},{8,24},{12,28},{1,17},{5,21},{9,25},{13,29},{2,18},{... | collective-permute-start | bytes 393224 | tf_op jit(solution)/shard_map/ppermute | solution.py:239
  36.9 8.1 %collective-permute-start.12 = (bf16[128,512]{1,0:T(8,128)(2,1)S(1)}, bf16[128,512]{1,0:T(8,128)(2,1)S(1)}, u32[]{:S(2)}, u32[]{:S(2)}) collective-permute-start(bf16[128,512]{1,0:T(8,128)(2,1)S(1)} %get-tuple-element.112), channel_id=1, source_target_pairs={{0,4},{4,0},{8,12},{12,8},{16,20},{20,16},{24,28},{28,24},{1,5},{5... | collective-permute-start | bytes 393224 | tf_op jit(solution)/shard_map/ppermute | solution.py:507
  38.9 9.6 %collective-permute-start.13 = (bf16[128,512]{1,0:T(8,128)(2,1)S(1)}, bf16[128,512]{1,0:T(8,128)(2,1)S(1)}, u32[]{:S(2)}, u32[]{:S(2)}) collective-permute-start(bf16[128,512]{1,0:T(8,128)(2,1)S(1)} %get-tuple-element.113), channel_id=1, source_target_pairs={{0,8},{4,12},{8,0},{12,4},{16,24},{20,28},{24,16},{28,20},{1,9},{5... | collective-permute-start | bytes 393224 | tf_op jit(solution)/shard_map/ppermute | solution.py:507
  40.5 8.1 %collective-permute-start.14 = (bf16[128,512]{1,0:T(8,128)(2,1)S(1)}, bf16[128,512]{1,0:T(8,128)(2,1)S(1)}, u32[]{:S(2)}, u32[]{:S(2)}) collective-permute-start(bf16[128,512]{1,0:T(8,128)(2,1)S(1)} %get-tuple-element.114), channel_id=1, source_target_pairs={{0,12},{4,8},{8,4},{12,0},{16,28},{20,24},{24,20},{28,16},{1,13},{... | collective-permute-start | bytes 393224 | tf_op jit(solution)/shard_map/ppermute | solution.py:507
  41.4 7.6 %collective-permute-start.5 = (bf16[128,512]{1,0:T(8,128)(2,1)S(1)}, bf16[128,512]{1,0:T(8,128)(2,1)S(1)}, u32[]{:S(2)}, u32[]{:S(2)}) collective-permute-start(bf16[128,512]{1,0:T(8,128)(2,1)S(1)} %get-tuple-element.108), channel_id=1, source_target_pairs={{0,4},{4,0},{8,12},{12,8},{16,20},{20,16},{24,28},{28,24},{1,5},{5... | collective-permute-start | bytes 393224 | tf_op jit(solution)/shard_map/ppermute | solution.py:507
  58.2 14.0 %collective-permute-start.16 = (bf16[128,2048]{1,0:T(8,128)(2,1)S(1)}, bf16[128,2048]{1,0:T(8,128)(2,1)S(1)}, u32[]{:S(2)}, u32[]{:S(2)}) collective-permute-start(bf16[128,2048]{1,0:T(8,128)(2,1)S(1)} %add_convert_fusion), channel_id=1, source_target_pairs={{0,2},{1,3},{2,0},{3,1},{4,6},{5,7},{6,4},{7,5},{8,10},{9,11},{10,... | collective-permute-start | bytes 1572872 | tf_op jit(solution)/shard_map/ppermute | solution.py:507
  90.7 12.9 %collective-permute-start.29 = (bf16[32,2048]{1,0:T(8,128)(2,1)S(1)}, bf16[32,2048]{1,0:T(8,128)(2,1)S(1)}, u32[]{:S(2)}, u32[]{:S(2)}) collective-permute-start(bf16[32,2048]{1,0:T(8,128)(2,1)S(1)} %get-tuple-element.155), channel_id=1, source_target_pairs={{0,16},{4,20},{8,24},{12,28},{16,0},{20,4},{24,8},{28,12},{1,17},{... | collective-permute-start | bytes 393224 | tf_op jit(solution)/shard_map/ppermute | solution.py:507
  93.4 13.3 %collective-permute-start.30 = (bf16[32,2048]{1,0:T(8,128)(2,1)S(1)}, bf16[32,2048]{1,0:T(8,128)(2,1)S(1)}, u32[]{:S(2)}, u32[]{:S(2)}) collective-permute-start(bf16[32,2048]{1,0:T(8,128)(2,1)S(1)} %get-tuple-element.156), channel_id=1, source_target_pairs={{0,20},{4,16},{8,28},{12,24},{16,4},{20,0},{24,12},{28,8},{1,21},{... | collective-permute-start | bytes 393224 | tf_op jit(solution)/shard_map/ppermute | solution.py:507
  111.0 8.1 %collective-permute-start.36 = (bf16[32,2048]{1,0:T(8,128)(2,1)S(1)}, bf16[32,2048]{1,0:T(8,128)(2,1)S(1)}, u32[]{:S(2)}, u32[]{:S(2)}) collective-permute-start(bf16[32,2048]{1,0:T(8,128)(2,1)S(1)} %get-tuple-element.163), channel_id=1, source_target_pairs={{0,24},{4,28},{8,16},{12,20},{16,8},{20,12},{24,0},{28,4},{1,25},{... | collective-permute-start | bytes 393224 | tf_op jit(solution)/shard_map/ppermute | solution.py:507
  113.5 8.0 %collective-permute-start.37 = (bf16[32,2048]{1,0:T(8,128)(2,1)S(1)}, bf16[32,2048]{1,0:T(8,128)(2,1)S(1)}, u32[]{:S(2)}, u32[]{:S(2)}) collective-permute-start(bf16[32,2048]{1,0:T(8,128)(2,1)S(1)} %get-tuple-element.164), channel_id=1, source_target_pairs={{0,28},{4,24},{8,20},{12,16},{16,12},{20,8},{24,4},{28,0},{1,29},{... | collective-permute-start | bytes 393224 | tf_op jit(solution)/shard_map/ppermute | solution.py:507
  125.8 7.7 %collective-permute-start.26 = (bf16[32,2048]{1,0:T(8,128)(2,1)S(1)}, bf16[32,2048]{1,0:T(8,128)(2,1)S(1)}, u32[]{:S(2)}, u32[]{:S(2)}) collective-permute-start(bf16[32,2048]{1,0:T(8,128)(2,1)S(1)} %get-tuple-element.152), channel_id=1, source_target_pairs={{0,4},{4,0},{8,12},{12,8},{16,20},{20,16},{24,28},{28,24},{1,5},{5... | collective-permute-start | bytes 393224 | tf_op jit(solution)/shard_map/ppermute | solution.py:507
  127.1 8.4 %collective-permute-start.27 = (bf16[32,2048]{1,0:T(8,128)(2,1)S(1)}, bf16[32,2048]{1,0:T(8,128)(2,1)S(1)}, u32[]{:S(2)}, u32[]{:S(2)}) collective-permute-start(bf16[32,2048]{1,0:T(8,128)(2,1)S(1)} %get-tuple-element.153), channel_id=1, source_target_pairs={{0,8},{4,12},{8,0},{12,4},{16,24},{20,28},{24,16},{28,20},{1,9},{5... | collective-permute-start | bytes 393224 | tf_op jit(solution)/shard_map/ppermute | solution.py:507
  129.6 11.6 %collective-permute-start.28 = (bf16[32,2048]{1,0:T(8,128)(2,1)S(1)}, bf16[32,2048]{1,0:T(8,128)(2,1)S(1)}, u32[]{:S(2)}, u32[]{:S(2)}) collective-permute-start(bf16[32,2048]{1,0:T(8,128)(2,1)S(1)} %get-tuple-element.154), channel_id=1, source_target_pairs={{0,12},{4,8},{8,4},{12,0},{16,28},{20,24},{24,20},{28,16},{1,13},{... | collective-permute-start | bytes 393224 | tf_op jit(solution)/shard_map/ppermute | solution.py:507
  130.5 18.5 %collective-permute-start.34 = (bf16[32,2048]{1,0:T(8,128)(2,1)S(1)}, bf16[32,2048]{1,0:T(8,128)(2,1)S(1)}, u32[]{:S(2)}, u32[]{:S(2)}) collective-permute-start(bf16[32,2048]{1,0:T(8,128)(2,1)S(1)} %get-tuple-element.161), channel_id=1, source_target_pairs={{0,16},{4,20},{8,24},{12,28},{16,0},{20,4},{24,8},{28,12},{1,17},{... | collective-permute-start | bytes 393224 | tf_op jit(solution)/shard_map/ppermute | solution.py:507
  132.4 18.9 %collective-permute-start.35 = (bf16[32,2048]{1,0:T(8,128)(2,1)S(1)}, bf16[32,2048]{1,0:T(8,128)(2,1)S(1)}, u32[]{:S(2)}, u32[]{:S(2)}) collective-permute-start(bf16[32,2048]{1,0:T(8,128)(2,1)S(1)} %get-tuple-element.162), channel_id=1, source_target_pairs={{0,20},{4,16},{8,28},{12,24},{16,4},{20,0},{24,12},{28,8},{1,21},{... | collective-permute-start | bytes 393224 | tf_op jit(solution)/shard_map/ppermute | solution.py:507
  133.5 17.9 %collective-permute-start.41 = (bf16[32,2048]{1,0:T(8,128)(2,1)S(1)}, bf16[32,2048]{1,0:T(8,128)(2,1)S(1)}, u32[]{:S(2)}, u32[]{:S(2)}) collective-permute-start(bf16[32,2048]{1,0:T(8,128)(2,1)S(1)} %get-tuple-element.169), channel_id=1, source_target_pairs={{0,24},{4,28},{8,16},{12,20},{16,8},{20,12},{24,0},{28,4},{1,25},{... | collective-permute-start | bytes 393224 | tf_op jit(solution)/shard_map/ppermute | solution.py:507
  135.5 15.8 %collective-permute-start.42 = (bf16[32,2048]{1,0:T(8,128)(2,1)S(1)}, bf16[32,2048]{1,0:T(8,128)(2,1)S(1)}, u32[]{:S(2)}, u32[]{:S(2)}) collective-permute-start(bf16[32,2048]{1,0:T(8,128)(2,1)S(1)} %get-tuple-element.170), channel_id=1, source_target_pairs={{0,28},{4,24},{8,20},{12,16},{16,12},{20,8},{24,4},{28,0},{1,29},{... | collective-permute-start | bytes 393224 | tf_op jit(solution)/shard_map/ppermute | solution.py:507
  154.9 8.4 %collective-permute-start.44 = (bf16[64,2048]{1,0:T(8,128)(2,1)S(1)}, bf16[64,2048]{1,0:T(8,128)(2,1)S(1)}, u32[]{:S(2)}, u32[]{:S(2)}) collective-permute-start(bf16[64,2048]{1,0:T(8,128)(2,1)S(1)} %slice.17), channel_id=1, source_target_pairs={{0,2},{1,3},{2,0},{3,1},{4,6},{5,7},{6,4},{7,5},{8,10},{9,11},{10,... | collective-permute-start | bytes 786440 | tf_op jit(solution)/shard_map/ppermute | solution.py:507
  (44 other events, 503.7 us)
where the time goes:
time: 167 us; the launch traced here: 164 us
  waiting for transfers between devices  66.7 us (40%)
  starting transfers between devices  58.4 us (35%)
  Pallas kernels  35.7 us (21%)
  other arithmetic  1.68 us (1%)
    ppermute x43, waiting for transfers between devices, swap(): return lax.ppermute(value, axis, xor_perm(axis, k))  66.7 us
    ppermute x43, starting transfers between devices, swap(): return lax.ppermute(value, axis, xor_perm(axis, k))  52.4 us
    pallas_call x2, Pallas kernels, device_states(): pl.pallas_call(functools.partial(state_kernel, first, count), in_specs=[S...  7.88 us
    pallas_call x3, Pallas kernels, expert(): pl.pallas_call(functools.partial(expert_kernel, count), in_specs=[VMEM] *...  7.35 us
    ppermute x2, starting transfers between devices, quad_entry(): start = lax.ppermute(total, 'sp', perm)  6.07 us
    pallas_call x1, Pallas kernels, local_attention(): pl.pallas_call(local_kernel, grid=(heads,), in_specs=[pl.BlockSpec(low.sh...  5.85 us
    pallas_call x1, Pallas kernels, project(): pl.pallas_call(functools.partial(project_kernel, count, heads, groups), g...  5.26 us
    pallas_call x4, Pallas kernels, quad_prefix(): pl.pallas_call(functools.partial(prefix_kernel, count, emit), in_specs=[S...  3.83 us
  transfers between devices with their start and end apart: 45, of which 24 were waited for; matrix products, arithmetic and copies ran while one was open for 0% of the time, Pallas kernels for 7%

commit v1 on v0

--- a/solution.py
+++ b/solution.py
@@ -64,7 +64,8 @@
 
 
 def state_kernel(first, count, idx, low, matrix, bias, shift, key_rows, values, *rest):
-    outs, (keys, vals, state, decays, sems) = rest[:QUAD], rest[QUAD:]
+    outs = rest[:QUAD]
+    keys, vals, state, decays, sems = rest[QUAD:]
     length = low.shape[1]
     piece = HK // QUAD
     copies = []
@@ -108,7 +109,7 @@
     rows = count * (HK // QUAD) + 8
     return pl.pallas_call(
         functools.partial(state_kernel, first, count),
-        in_specs=[SMEM, VMEM, VMEM, VMEM, VMEM, HBM, HBM],
+        in_specs=[SMEM] + [VMEM] * 4 + [HBM] * 2,
         out_specs=[VMEM] * QUAD,
         out_shape=[jax.ShapeDtypeStruct((rows, HV), BF16)] * QUAD,
         scratch_shapes=[
@@ -123,7 +124,8 @@
     )(idx, low, matrix, bias, shift, key_rows, values)
 
 
-def local_kernel(low, matrix, bias, shift, queries, key_rows, values, out, query_out):
+def local_kernel(low, matrix, bias, shift, queries, key_rows, values, *refs):
+    out, query_out = refs[-2:]
     length = low.shape[1]
     logs = head_log_decay(low[...], matrix[...], bias[...], shift[0], 0)
     below = tri(BLK, lambda r, c: c <= r)
@@ -154,32 +156,45 @@
         before = before + final
 
 
-def local_attention(heads, low, matrix, bias, shift, queries, key_rows, values):
+def local_attention(first, count, heads, sofar, low, matrix, bias, shift, *arrays):
     length = low.shape[1]
+    queries, key_rows, values = arrays
+    sofar = list(sofar or ())
+    out_specs = [
+        pl.BlockSpec((length, HV), lambda h: (0, first + h)),
+        pl.BlockSpec((length, HK), lambda h: (0, first + h)),
+    ]
     return pl.pallas_call(
         local_kernel,
-        grid=(heads,),
+        grid=(count,),
         in_specs=[
             pl.BlockSpec(low.shape, lambda h: (0, 0)),
-            pl.BlockSpec((low.shape[0], HK), lambda h: (0, h)),
-            pl.BlockSpec((1, HK), lambda h: (0, h)),
-            pl.BlockSpec((1, 1, length), lambda h: (h, 0, 0)),
-            pl.BlockSpec((length, HK), lambda h: (0, h)),
-            pl.BlockSpec((length, HK), lambda h: (0, h)),
-            pl.BlockSpec((length, HV), lambda h: (0, h)),
-        ],
-        out_specs=[
-            pl.BlockSpec((length, HV), lambda h: (0, h)),
-            pl.BlockSpec((length, HK), lambda h: (0, h)),
-        ],
+            pl.BlockSpec((low.shape[0], HK), lambda h: (0, first + h)),
+            pl.BlockSpec((1, HK), lambda h: (0, first + h)),
+            pl.BlockSpec((1, 1, length), lambda h: (first + h, 0, 0)),
+            pl.BlockSpec((length, HK), lambda h: (0, first + h)),
+            pl.BlockSpec((length, HK), lambda h: (0, first + h)),
+            pl.BlockSpec((length, HV), lambda h: (0, first + h)),
+        ]
+        + [pl.BlockSpec(memory_space=pl.ANY)] * len(sofar),
+        out_specs=out_specs,
         out_shape=[
             jax.ShapeDtypeStruct((length, heads * HV), F32),
             jax.ShapeDtypeStruct((length, heads * HK), BF16),
         ],
+        input_output_aliases={7 + i: i for i in range(len(sofar))},
         compiler_params=params(24),
-        cost_estimate=cost(heads * 4e8, heads * 1.2e6),
-        name="local_attention",
-    )(low, matrix, bias, shift.reshape(heads, 1, length), queries, key_rows, values)
+        cost_estimate=cost(count * 4e8, count * 1.2e6),
+    )(
+        low,
+        matrix,
+        bias,
+        shift.reshape(heads, 1, length),
+        queries,
+        key_rows,
+        values,
+        *sofar,
+    )
 
 
 def prefix_kernel(count, emit, idx, start, *refs):
@@ -346,23 +361,29 @@
 def route_kernel(n, half, idx, routes, weights, select, high, low):
     me, core = idx[0], idx[1]
     length = routes.shape[1]
-    earlier = tri(length, lambda r, c: r < c).astype(F32).astype(BF16)
-    first, second = routes[0:1, :], routes[1:2, :]
-    expert = me ^ lax.broadcasted_iota(jnp.int32, (n, length), 0)
-    is_first, is_second = first == expert, second == expert
+    earlier = tri(length, lambda r, c: c < r).astype(F32).astype(BF16)
+    chosen = jnp.transpose(routes[...].astype(F32)).astype(jnp.int32)
+    weight = jnp.transpose(weights[...])
+    expert = me ^ lax.broadcasted_iota(jnp.int32, (length, n), 1)
+    is_first, is_second = chosen[:, 0:1] == expert, chosen[:, 1:2] == expert
     member = jnp.where(is_first | is_second, 1.0, 0.0)
-    rank = jnp.dot(member.astype(BF16), earlier, preferred_element_type=F32)
-    slot = jnp.where(member > 0.0, rank.astype(jnp.int32), -1)
-    weight = jnp.where(is_first, weights[0:1, :], weights[1:2, :])
-    for k in range(n):
-        wanted = core * half + lax.broadcasted_iota(jnp.int32, (half, length), 0)
-        hit = slot[k : k + 1, :] == wanted
-        span = slice(k * half, (k + 1) * half)
-        select[span, :] = jnp.where(hit, 1.0, 0.0).astype(BF16)
-        value = jnp.where(hit, weight[k : k + 1, :], 0.0)
-        top = value.astype(BF16)
-        high[span, :] = top
-        low[span, :] = (value - top.astype(F32)).astype(BF16)
+    rank = jnp.dot(earlier, member.astype(BF16), preferred_element_type=F32)
+    slot = jnp.where(member > 0.0, rank, -1.0)
+    value = jnp.where(is_first, weight[:, 0:1], weight[:, 1:2])
+    top = value.astype(BF16)
+    rest = (value - top.astype(F32)).astype(BF16)
+    column = lax.broadcasted_iota(jnp.int32, (n, n * half), 1)
+    owner = lax.broadcasted_iota(jnp.int32, (n, n * half), 0)
+    spread = jnp.where(column // half == owner, 1.0, 0.0).astype(BF16)
+
+    def widen(array):
+        return jnp.dot(array, spread, preferred_element_type=F32)
+
+    wanted = core * half + lax.broadcasted_iota(jnp.int32, (length, n * half), 1) % half
+    hit = widen(slot.astype(BF16)) == wanted.astype(F32)
+    select[...] = jnp.where(hit, 1.0, 0.0).astype(BF16)
+    high[...] = jnp.where(hit, widen(top), 0.0).astype(BF16)
+    low[...] = jnp.where(hit, widen(rest), 0.0).astype(BF16)
 
 
 def slot_tables(n, half, idx, routes, weights):
@@ -371,7 +392,7 @@
         functools.partial(route_kernel, n, half),
         in_specs=[SMEM, VMEM, VMEM],
         out_specs=[VMEM] * 3,
-        out_shape=[jax.ShapeDtypeStruct((n * half, length), BF16)] * 3,
+        out_shape=[jax.ShapeDtypeStruct((length, n * half), BF16)] * 3,
         compiler_params=params(16),
         cost_estimate=cost(1e8, 5e5),
         name="slot_tables",
@@ -379,14 +400,14 @@
 
 
 def dispatch_kernel(n, half, groups, idx, select, mine, theirs, *refs):
-    outs, group = refs[:n], refs[n]
-    rows = mine.shape[0] // groups
-    for span, own, other in block_spans(idx, groups, rows):
-        group[own, :] = mine[span, :]
-        group[other, :] = theirs[span, :]
+    outs, table = refs[:n], refs[n]
+    split = mine.shape[0]
+    for span, own, other in block_spans(idx, groups, split // groups):
+        table[span, :] = select[own, :]
+        table[split + span.start : split + span.stop, :] = select[other, :]
+    picked = contract0(table[:split, :], mine[...]) + contract0(table[split:, :], theirs[...])
     for k in range(n):
-        chosen = select[k * half : (k + 1) * half, :]
-        outs[k][...] = jnp.dot(chosen, group[...], preferred_element_type=F32).astype(BF16)
+        outs[k][...] = picked[k * half : (k + 1) * half, :].astype(BF16)
 
 
 def dispatch(n, half, groups, idx, select, mine, theirs):
@@ -396,7 +417,7 @@
         in_specs=[SMEM] + [VMEM] * 3,
         out_specs=[VMEM] * n,
         out_shape=[jax.ShapeDtypeStruct((half, width), BF16)] * n,
-        scratch_shapes=[pltpu.VMEM((select.shape[1], width), BF16)],
+        scratch_shapes=[pltpu.VMEM(select.shape, BF16)],
         compiler_params=params(16),
         cost_estimate=cost(5e8, 2e6),
         name="dispatch",
@@ -477,17 +498,22 @@
 
 
 def combine_kernel(n, groups, idx, high, low, *refs):
-    ins, (keep, send, total) = refs[:n], refs[n:]
+    ins, (keep, send, table) = refs[:n], refs[n:]
     rows = jnp.concatenate([piece[...] for piece in ins], axis=0)
-    total[...] = contract0(high[...], rows) + contract0(low[...], rows)
-    for span, own, other in block_spans(idx, groups, keep.shape[0] // groups):
-        keep[span, :] = total[own, :]
-        send[span, :] = total[other, :].astype(BF16)
+    split = keep.shape[0]
+    for part, source in enumerate((high, low)):
+        for span, own, other in block_spans(idx, groups, split // groups):
+            table[part, span, :] = source[own, :]
+            table[part, split + span.start : split + span.stop, :] = source[other, :]
+    total = jnp.dot(table[0], rows, preferred_element_type=F32)
+    total = total + jnp.dot(table[1], rows, preferred_element_type=F32)
+    keep[...] = total[:split, :]
+    send[...] = total[split:, :].astype(BF16)
 
 
 def combine(n, groups, idx, high, low, pieces):
     width = pieces[0].shape[1]
-    length = high.shape[1]
+    length = high.shape[0]
     return pl.pallas_call(
         functools.partial(combine_kernel, n, groups),
         in_specs=[SMEM] + [VMEM] * (2 + n),
@@ -496,7 +522,7 @@
             jax.ShapeDtypeStruct((length // 2, width), F32),
             jax.ShapeDtypeStruct((length // 2, width), BF16),
         ],
-        scratch_shapes=[pltpu.VMEM((length, width), F32)],
+        scratch_shapes=[pltpu.VMEM((2,) + high.shape, BF16)],
         compiler_params=params(16),
         cost_estimate=cost(1e9, 3e6),
         name="combine",
@@ -555,19 +581,29 @@
         gathered.append(exchange(states))
     stream_in, _ = lax.optimization_barrier((stream_in, states))
     streams = [stream_in] + [swap(stream_in, "tp", 2 * k) for k in range(1, groups)]
-    local, late_queries = local_attention(
-        heads, low, decay_matrix, bias, shift, queries, key_rows, values
-    )
+    sofar = None
+    for first in range(0, heads, count):
+        sofar = local_attention(
+            first,
+            count,
+            heads,
+            sofar,
+            low,
+            decay_matrix,
+            bias,
+            shift,
+            queries,
+            key_rows,
+            values,
+        )
+    local, late_queries = sofar
     select, high, low_part = slot_tables(n, half, idx, routes.T, route_weights.T)
-    gathered[0], streams, local, late_queries = lax.optimization_barrier(
-        (gathered[0], streams, local, late_queries)
-    )
     carried = []
     for part, pieces in enumerate(gathered):
         entry = quad_entry(count, idx, pieces)
         carried += exchange(quad_prefix(count, True, idx, entry, pieces))
-    carried, select, high, low_part = lax.optimization_barrier(
-        (carried, select, high, low_part)
+    carried, streams, select, high, low_part = lax.optimization_barrier(
+        (carried, streams, select, high, low_part)
     )
     keep, send = project(
         count,
@@ -618,7 +654,7 @@
 
 def expert_chunks(n):
     middle = (QUAD + n) // 2
-    return [range(QUAD), range(QUAD, middle), range(middle, n)]
+    return [range(QUAD, middle), range(QUAD), range(middle, n)]
 
 
 def solution(mesh):

time: 167 us -> 159 us (0.952); the launches traced: 164 us -> 158 us
  waiting for transfers between devices: 66.7 us -> 61.9 us
    ppermute x43, waiting for transfers between devices: 66.7 us -> 61.9 us  [swap(): return lax.ppermute(value, axis, xor_perm(axis, k))]
    ppermute x43, starting transfers between devices: 52.4 us -> 49.3 us  [swap(): return lax.ppermute(value, axis, xor_perm(axis, k))]
    ppermute x2, starting transfers between devices: 6.07 us -> 8.49 us  [quad_entry(): start = lax.ppermute(total, 'sp', perm)]
    pallas_call x1 -> x2, Pallas kernels: 5.85 us -> 5.9 us  [local_attention(): pl.pallas_call(local_kernel, grid=(count,), in_specs=[pl.BlockSpec(low.sh...]
  transfers between devices with their start and end apart: 45 -> 45, of which waited for: 24 -> 23; matrix products, arithmetic and copies ran while one was open for 0% -> 0% of each run, Pallas kernels for 7% -> 10%
where the time goes in v1:
time: 159 us; the launch traced here: 158 us
  waiting for transfers between devices  61.9 us (39%)
  starting transfers between devices  57.8 us (36%)
  Pallas kernels  35.3 us (22%)
  other arithmetic  1.71 us (1%)
    ppermute x43, waiting for transfers between devices, swap(): return lax.ppermute(value, axis, xor_perm(axis, k))  61.9 us
    ppermute x43, starting transfers between devices, swap(): return lax.ppermute(value, axis, xor_perm(axis, k))  49.3 us
    ppermute x2, starting transfers between devices, quad_entry(): start = lax.ppermute(total, 'sp', perm)  8.49 us
    pallas_call x2, Pallas kernels, device_states(): pl.pallas_call(functools.partial(state_kernel, first, count), in_specs=[S...  7.82 us
    pallas_call x3, Pallas kernels, expert(): pl.pallas_call(functools.partial(expert_kernel, count), in_specs=[VMEM] *...  7.35 us
    pallas_call x2, Pallas kernels, local_attention(): pl.pallas_call(local_kernel, grid=(count,), in_specs=[pl.BlockSpec(low.sh...  5.9 us
    pallas_call x1, Pallas kernels, project(): pl.pallas_call(functools.partial(project_kernel, count, heads, groups), g...  5.08 us
    pallas_call x4, Pallas kernels, quad_prefix(): pl.pallas_call(functools.partial(prefix_kernel, count, emit), in_specs=[S...  3.83 us
  transfers between devices with their start and end apart: 45, of which 23 were waited for; matrix products, arithmetic and copies ran while one was open for 0% of the time, Pallas kernels for 10%

profile of v1, /device:TPU:0, one launch (start us, length us, event | category | flops | bytes accessed | tf_op | source)
XLA Modules:
  0.0 158.2 jit_solution(10830800285774596734)
XLA Ops:
  0.7 3.8 %shard_map.156 = (bf16[136,512]{1,0:T(8,128)(2,1)}, bf16[136,512]{1,0:T(8,128)(2,1)}, bf16[136,512]{1,0:T(8,128)(2,1)}, bf16[136,512]{1,0:T(8,128)(2,1)}) custom-call(s32[3]{0:T(128)} %pad_add_fusion.idx, bf16[16,256]{1,0:T(8,128)(2,1)} %bitcast.22, bf16[16,1024]{1,0:T(8,128)(2,1)} %matrix.8, f32[1,1024]{1,0:T(1,128)} %bitcast.27, f32[4,256]{1,0:T(4,128)} %bitcast.34, ...), custom_call_target="tpu_custom_call" | custom-call | flops 800000000 | bytes 1000000 | tf_op jit(solution)/shard_map/pallas_call | solution.py:110
  4.6 3.0 %collective-permute-start = (bf16[136,512]{1,0:T(8,128)(2,1)}, bf16[136,512]{1,0:T(8,128)(2,1)S(1)}, u32[]{:S(2)}, u32[]{:S(2)}) collective-permute-start(bf16[136,512]{1,0:T(8,128)(2,1)} %get-tuple-element.92), channel_id=1, source_target_pairs={{0,4},{4,0},{8,12},{12,8},{16,20},{20,16},{24,28},{28,24},{1,5},{5... | collective-permute-start | bytes 417800 | tf_op jit(solution)/shard_map/ppermute | solution.py:533
  9.2 4.0 %shard_map.157 = (bf16[136,512]{1,0:T(8,128)(2,1)}, bf16[136,512]{1,0:T(8,128)(2,1)}, bf16[136,512]{1,0:T(8,128)(2,1)}, bf16[136,512]{1,0:T(8,128)(2,1)}) custom-call(s32[3]{0:T(128)} %pad_add_fusion.idx, bf16[16,256]{1,0:T(8,128)(2,1)} %bitcast.23, bf16[16,1024]{1,0:T(8,128)(2,1)} %matrix.8, f32[1,1024]{1,0:T(1,128)} %bitcast.28, f32[4,256]{1,0:T(4,128)} %bitcast.35, ...), custom_call_target="tpu_custom_call" | custom-call | flops 800000000 | bytes 1000000 | tf_op jit(solution)/shard_map/pallas_call | solution.py:110
  17.8 4.9 %collective-permute-start.3 = (bf16[128,512]{1,0:T(8,128)(2,1)S(1)}, bf16[128,512]{1,0:T(8,128)(2,1)S(1)}, u32[]{:S(2)}, u32[]{:S(2)}) collective-permute-start(bf16[128,512]{1,0:T(8,128)(2,1)S(1)} %quad_total.2), channel_id=1, source_target_pairs={{0,16},{4,20},{8,24},{12,28},{1,17},{5,21},{9,25},{13,29},{2,18},{... | collective-permute-start | bytes 393224 | tf_op jit(solution)/shard_map/ppermute | solution.py:254
  26.2 3.6 %collective-permute-start.10 = (bf16[128,512]{1,0:T(8,128)(2,1)S(1)}, bf16[128,512]{1,0:T(8,128)(2,1)S(1)}, u32[]{:S(2)}, u32[]{:S(2)}) collective-permute-start(bf16[128,512]{1,0:T(8,128)(2,1)S(1)} %quad_total.3), channel_id=1, source_target_pairs={{0,16},{4,20},{8,24},{12,28},{1,17},{5,21},{9,25},{13,29},{2,18},{... | collective-permute-start | bytes 393224 | tf_op jit(solution)/shard_map/ppermute | solution.py:254
  32.9 2.5 %collective-permute-start.5 = (bf16[128,512]{1,0:T(8,128)(2,1)S(1)}, bf16[128,512]{1,0:T(8,128)(2,1)S(1)}, u32[]{:S(2)}, u32[]{:S(2)}) collective-permute-start(bf16[128,512]{1,0:T(8,128)(2,1)S(1)} %get-tuple-element.97), channel_id=1, source_target_pairs={{0,8},{4,12},{8,0},{12,4},{16,24},{20,28},{24,16},{28,20},{1,9},{5... | collective-permute-start | bytes 393224 | tf_op jit(solution)/shard_map/ppermute | solution.py:533
  42.0 2.9 %shard_map.154 = (f32[256,2048]{1,0:T(8,128)S(1)}, bf16[256,1024]{1,0:T(8,128)(2,1)S(1)}) custom-call(bf16[16,256]{1,0:T(8,128)(2,1)S(1)} %bitcast.24, bf16[16,1024]{1,0:T(8,128)(2,1)S(1)} %copy-done.11, f32[1,1024]{1,0:T(1,128)S(1)} %bitcast.29, f32[4,1,256]{2,1,0:T(1,128)S(1)} %copy.20.shift, bf16[256,1024]{1,0:T(8,128)(2,1)S(1)} %copy-done.8, ...), custom_call_target="tpu_custom_call" | custom-call | flops 800000000 | bytes 2400000 | tf_op jit(solution)/shard_map/pallas_call | solution.py:167
  44.9 3.0 %shard_map.155 = (f32[256,2048]{1,0:T(8,128)S(1)}, bf16[256,1024]{1,0:T(8,128)(2,1)S(1)}) custom-call(bf16[16,256]{1,0:T(8,128)(2,1)S(1)} %bitcast.25, bf16[16,1024]{1,0:T(8,128)(2,1)S(1)} %copy-done.11, f32[1,1024]{1,0:T(1,128)S(1)} %bitcast.30, f32[4,1,256]{2,1,0:T(1,128)S(1)} %copy.20.shift, ...), custom_call_target="tpu_custom_call", output_to_operand_aliasing={{0}: (7, {}), {1}: (8, {})} | custom-call | flops 800000000 | bytes 2400000 | tf_op jit(solution)/shard_map/pallas_call | solution.py:167
  48.0 5.1 %project.1 = (f32[128,2048]{1,0:T(8,128)S(1)}, bf16[128,2048]{1,0:T(8,128)(2,1)S(1)}) custom-call(s32[3]{0:T(128)S(1)} %copy-done.12, bf16[256,1024]{1,0:T(8,128)(2,1)S(1)} %get-tuple-element.89.queries, f32[256,2048]{1,0:T(8,128)S(1)} %get-tuple-element.90.local, f32[1,512]{1,0:T(1,128)S(1)} %bitcast.31, bf16[2048,2048]{1,0:T(8,128)(2,1)S(1)} %copy-done, ...), custom_call_target="tpu_custom_call" | custom-call | flops 2800000000 | bytes 10000000 | tf_op jit(solution)/shard_map/project/pallas_call | solution.py:302
  57.6 11.6 %collective-permute-done.16.refs_2_ = bf16[128,2048]{1,0:T(8,128)(2,1)S(1)} collective-permute-done((bf16[128,2048]{1,0:T(8,128)(2,1)S(1)}, bf16[128,2048]{1,0:T(8,128)(2,1)S(1)}, u32[]{:S(2)}, u32[]{:S(2)}) %collective-permute-start.16) | collective-permute-done | bytes 524320 | tf_op jit(solution)/shard_map/ppermute | solution.py:533
  75.0 9.2 %collective-permute-done.21.refs_0_ = bf16[32,2048]{1,0:T(8,128)(2,1)S(1)} collective-permute-done((bf16[32,2048]{1,0:T(8,128)(2,1)S(1)}, bf16[32,2048]{1,0:T(8,128)(2,1)S(1)}, u32[]{:S(2)}, u32[]{:S(2)}) %collective-permute-start.21) | collective-permute-done | bytes 131104 | tf_op jit(solution)/shard_map/ppermute | solution.py:533
  84.2 2.7 %collective-permute-done.22.refs_1_ = bf16[32,2048]{1,0:T(8,128)(2,1)S(1)} collective-permute-done((bf16[32,2048]{1,0:T(8,128)(2,1)S(1)}, bf16[32,2048]{1,0:T(8,128)(2,1)S(1)}, u32[]{:S(2)}, u32[]{:S(2)}) %collective-permute-start.22) | collective-permute-done | bytes 131104 | tf_op jit(solution)/shard_map/ppermute | solution.py:533
  88.3 2.4 %shard_map.158 = (f32[64,2048]{1,0:T(8,128)S(1)}, bf16[64,2048]{1,0:T(8,128)(2,1)S(1)}) custom-call(bf16[704,2048]{1,0:T(8,128)(2,1)S(1)} %get-tuple-element.134.gate, bf16[704,2048]{1,0:T(8,128)(2,1)S(1)} %get-tuple-element.135.widen, bf16[704,2048]{1,0:T(8,128)(2,1)S(1)} %get-tuple-element.136.down, bf16[32,2048]{1,0:T(8,128)(2,1)S(1)} %collective-permute-done.21.refs_0_, ...), custom_call_target="tpu_custom_call" | custom-call | flops 1200000000 | bytes 4000000 | tf_op jit(solution)/shard_map/pallas_call | solution.py:468
  102.6 2.6 %shard_map.160 = (f32[128,2048]{1,0:T(8,128)S(1)}, bf16[128,2048]{1,0:T(8,128)(2,1)S(1)}) custom-call(bf16[704,2048]{1,0:T(8,128)(2,1)S(1)} %get-tuple-element.134.gate, bf16[704,2048]{1,0:T(8,128)(2,1)S(1)} %get-tuple-element.135.widen, bf16[704,2048]{1,0:T(8,128)(2,1)S(1)} %get-tuple-element.136.down, bf16[32,2048]{1,0:T(8,128)(2,1)S(1)} %get-tuple-element.149.refs_0_, ...), custom_call_target="tpu_custom_call" | custom-call | flops 2400000000 | bytes 4000000 | tf_op jit(solution)/shard_map/pallas_call | solution.py:468
  107.1 3.3 %collective-permute-start.37 = (bf16[32,2048]{1,0:T(8,128)(2,1)S(1)}, bf16[32,2048]{1,0:T(8,128)(2,1)S(1)}, u32[]{:S(2)}, u32[]{:S(2)}) collective-permute-start(bf16[32,2048]{1,0:T(8,128)(2,1)S(1)} %get-tuple-element.160), channel_id=1, source_target_pairs={{0,28},{4,24},{8,20},{12,16},{16,12},{20,8},{24,4},{28,0},{1,29},{... | collective-permute-start | bytes 393224 | tf_op jit(solution)/shard_map/ppermute | solution.py:533
  110.5 3.4 %collective-permute-done.36.refs_0_ = bf16[32,2048]{1,0:T(8,128)(2,1)S(1)} collective-permute-done((bf16[32,2048]{1,0:T(8,128)(2,1)S(1)}, bf16[32,2048]{1,0:T(8,128)(2,1)S(1)}, u32[]{:S(2)}, u32[]{:S(2)}) %collective-permute-start.36) | collective-permute-done | bytes 131104 | tf_op jit(solution)/shard_map/ppermute | solution.py:533
  113.9 2.9 %collective-permute-done.37.refs_1_ = bf16[32,2048]{1,0:T(8,128)(2,1)S(1)} collective-permute-done((bf16[32,2048]{1,0:T(8,128)(2,1)S(1)}, bf16[32,2048]{1,0:T(8,128)(2,1)S(1)}, u32[]{:S(2)}, u32[]{:S(2)}) %collective-permute-start.37) | collective-permute-done | bytes 131104 | tf_op jit(solution)/shard_map/ppermute | solution.py:533
  121.2 3.7 %collective-permute-start.34 = (bf16[32,2048]{1,0:T(8,128)(2,1)S(1)}, bf16[32,2048]{1,0:T(8,128)(2,1)S(1)}, u32[]{:S(2)}, u32[]{:S(2)}) collective-permute-start(bf16[32,2048]{1,0:T(8,128)(2,1)S(1)} %get-tuple-element.147), channel_id=1, source_target_pairs={{0,16},{4,20},{8,24},{12,28},{16,0},{20,4},{24,8},{28,12},{1,17},{... | collective-permute-start | bytes 393224 | tf_op jit(solution)/shard_map/ppermute | solution.py:533
  126.4 3.2 %collective-permute-start.32 = (bf16[32,2048]{1,0:T(8,128)(2,1)S(1)}, bf16[32,2048]{1,0:T(8,128)(2,1)S(1)}, u32[]{:S(2)}, u32[]{:S(2)}) collective-permute-start(bf16[32,2048]{1,0:T(8,128)(2,1)S(1)} %get-tuple-element.157), channel_id=1, source_target_pairs={{0,8},{4,12},{8,0},{12,4},{16,24},{20,28},{24,16},{28,20},{1,9},{5... | collective-permute-start | bytes 393224 | tf_op jit(solution)/shard_map/ppermute | solution.py:533
  129.6 5.1 %collective-permute-done.34.refs_4_ = bf16[32,2048]{1,0:T(8,128)(2,1)S(1)} collective-permute-done((bf16[32,2048]{1,0:T(8,128)(2,1)S(1)}, bf16[32,2048]{1,0:T(8,128)(2,1)S(1)}, u32[]{:S(2)}, u32[]{:S(2)}) %collective-permute-start.34) | collective-permute-done | bytes 131104 | tf_op jit(solution)/shard_map/ppermute | solution.py:533
  134.7 2.8 %collective-permute-start.41 = (bf16[32,2048]{1,0:T(8,128)(2,1)S(1)}, bf16[32,2048]{1,0:T(8,128)(2,1)S(1)}, u32[]{:S(2)}, u32[]{:S(2)}) collective-permute-start(bf16[32,2048]{1,0:T(8,128)(2,1)S(1)} %get-tuple-element.165), channel_id=1, source_target_pairs={{0,24},{4,28},{8,16},{12,20},{16,8},{20,12},{24,0},{28,4},{1,25},{... | collective-permute-start | bytes 393224 | tf_op jit(solution)/shard_map/ppermute | solution.py:533
  137.9 3.3 %collective-permute-start.42 = (bf16[32,2048]{1,0:T(8,128)(2,1)S(1)}, bf16[32,2048]{1,0:T(8,128)(2,1)S(1)}, u32[]{:S(2)}, u32[]{:S(2)}) collective-permute-start(bf16[32,2048]{1,0:T(8,128)(2,1)S(1)} %get-tuple-element.166), channel_id=1, source_target_pairs={{0,28},{4,24},{8,20},{12,16},{16,12},{20,8},{24,4},{28,0},{1,29},{... | collective-permute-start | bytes 393224 | tf_op jit(solution)/shard_map/ppermute | solution.py:533
  142.7 2.9 %collective-permute-done.42.refs_7_ = bf16[32,2048]{1,0:T(8,128)(2,1)S(1)} collective-permute-done((bf16[32,2048]{1,0:T(8,128)(2,1)S(1)}, bf16[32,2048]{1,0:T(8,128)(2,1)S(1)}, u32[]{:S(2)}, u32[]{:S(2)}) %collective-permute-start.42) | collective-permute-done | bytes 131104 | tf_op jit(solution)/shard_map/ppermute | solution.py:533
  150.6 6.8 %collective-permute-done.44 = bf16[64,2048]{1,0:T(8,128)(2,1)S(1)} collective-permute-done((bf16[64,2048]{1,0:T(8,128)(2,1)S(1)}, bf16[64,2048]{1,0:T(8,128)(2,1)S(1)}, u32[]{:S(2)}, u32[]{:S(2)}) %collective-permute-start.44) | collective-permute-done | bytes 262176 | tf_op jit(solution)/shard_map/ppermute | solution.py:533
  (133 shorter events, 58.7 us)
Async XLA Ops:
  4.6 12.2 %collective-permute-start = (bf16[136,512]{1,0:T(8,128)(2,1)}, bf16[136,512]{1,0:T(8,128)(2,1)S(1)}, u32[]{:S(2)}, u32[]{:S(2)}) collective-permute-start(bf16[136,512]{1,0:T(8,128)(2,1)} %get-tuple-element.92), channel_id=1, source_target_pairs={{0,4},{4,0},{8,12},{12,8},{16,20},{20,16},{24,28},{28,24},{1,5},{5... | collective-permute-start | bytes 417800 | tf_op jit(solution)/shard_map/ppermute | solution.py:533
  7.6 9.2 %collective-permute-start.1 = (bf16[136,512]{1,0:T(8,128)(2,1)}, bf16[136,512]{1,0:T(8,128)(2,1)S(1)}, u32[]{:S(2)}, u32[]{:S(2)}) collective-permute-start(bf16[136,512]{1,0:T(8,128)(2,1)} %get-tuple-element.93), channel_id=1, source_target_pairs={{0,8},{4,12},{8,0},{12,4},{16,24},{20,28},{24,16},{28,20},{1,9},{5... | collective-permute-start | bytes 417800 | tf_op jit(solution)/shard_map/ppermute | solution.py:533
  13.2 11.1 %collective-permute-start.7 = (bf16[136,512]{1,0:T(8,128)(2,1)}, bf16[136,512]{1,0:T(8,128)(2,1)S(1)}, u32[]{:S(2)}, u32[]{:S(2)}) collective-permute-start(bf16[136,512]{1,0:T(8,128)(2,1)} %get-tuple-element.101), channel_id=1, source_target_pairs={{0,4},{4,0},{8,12},{12,8},{16,20},{20,16},{24,28},{28,24},{1,5},{5... | collective-permute-start | bytes 417800 | tf_op jit(solution)/shard_map/ppermute | solution.py:533
  15.2 9.1 %collective-permute-start.8 = (bf16[136,512]{1,0:T(8,128)(2,1)}, bf16[136,512]{1,0:T(8,128)(2,1)S(1)}, u32[]{:S(2)}, u32[]{:S(2)}) collective-permute-start(bf16[136,512]{1,0:T(8,128)(2,1)} %get-tuple-element.102), channel_id=1, source_target_pairs={{0,8},{4,12},{8,0},{12,4},{16,24},{20,28},{24,16},{28,20},{1,9},{5... | collective-permute-start | bytes 417800 | tf_op jit(solution)/shard_map/ppermute | solution.py:533
  17.8 12.0 %collective-permute-start.3 = (bf16[128,512]{1,0:T(8,128)(2,1)S(1)}, bf16[128,512]{1,0:T(8,128)(2,1)S(1)}, u32[]{:S(2)}, u32[]{:S(2)}) collective-permute-start(bf16[128,512]{1,0:T(8,128)(2,1)S(1)} %quad_total.2), channel_id=1, source_target_pairs={{0,16},{4,20},{8,24},{12,28},{1,17},{5,21},{9,25},{13,29},{2,18},{... | collective-permute-start | bytes 393224 | tf_op jit(solution)/shard_map/ppermute | solution.py:254
  22.7 15.3 %collective-permute-start.14 = (bf16[64,2048]{1,0:T(8,128)(2,1)S(1)}, bf16[64,2048]{1,0:T(8,128)(2,1)S(1)}, u32[]{:S(2)}, u32[]{:S(2)}) collective-permute-start(bf16[64,2048]{1,0:T(8,128)(2,1)S(1)} %copy-done.10), channel_id=1, source_target_pairs={{0,2},{1,3},{2,0},{3,1},{4,6},{5,7},{6,4},{7,5},{8,10},{9,11},{10,... | collective-permute-start | bytes 786440 | tf_op jit(solution)/shard_map/ppermute | solution.py:533
  26.2 9.5 %collective-permute-start.10 = (bf16[128,512]{1,0:T(8,128)(2,1)S(1)}, bf16[128,512]{1,0:T(8,128)(2,1)S(1)}, u32[]{:S(2)}, u32[]{:S(2)}) collective-permute-start(bf16[128,512]{1,0:T(8,128)(2,1)S(1)} %quad_total.3), channel_id=1, source_target_pairs={{0,16},{4,20},{8,24},{12,28},{1,17},{5,21},{9,25},{13,29},{2,18},{... | collective-permute-start | bytes 393224 | tf_op jit(solution)/shard_map/ppermute | solution.py:254
  30.7 9.2 %collective-permute-start.4 = (bf16[128,512]{1,0:T(8,128)(2,1)S(1)}, bf16[128,512]{1,0:T(8,128)(2,1)S(1)}, u32[]{:S(2)}, u32[]{:S(2)}) collective-permute-start(bf16[128,512]{1,0:T(8,128)(2,1)S(1)} %get-tuple-element.96), channel_id=1, source_target_pairs={{0,4},{4,0},{8,12},{12,8},{16,20},{20,16},{24,28},{28,24},{1,5},{5... | collective-permute-start | bytes 393224 | tf_op jit(solution)/shard_map/ppermute | solution.py:533
  32.9 15.0 %collective-permute-start.5 = (bf16[128,512]{1,0:T(8,128)(2,1)S(1)}, bf16[128,512]{1,0:T(8,128)(2,1)S(1)}, u32[]{:S(2)}, u32[]{:S(2)}) collective-permute-start(bf16[128,512]{1,0:T(8,128)(2,1)S(1)} %get-tuple-element.97), channel_id=1, source_target_pairs={{0,8},{4,12},{8,0},{12,4},{16,24},{20,28},{24,16},{28,20},{1,9},{5... | collective-permute-start | bytes 393224 | tf_op jit(solution)/shard_map/ppermute | solution.py:533
  35.4 12.5 %collective-permute-start.6 = (bf16[128,512]{1,0:T(8,128)(2,1)S(1)}, bf16[128,512]{1,0:T(8,128)(2,1)S(1)}, u32[]{:S(2)}, u32[]{:S(2)}) collective-permute-start(bf16[128,512]{1,0:T(8,128)(2,1)S(1)} %get-tuple-element.98), channel_id=1, source_target_pairs={{0,12},{4,8},{8,4},{12,0},{16,28},{20,24},{24,20},{28,16},{1,13},{... | collective-permute-start | bytes 393224 | tf_op jit(solution)/shard_map/ppermute | solution.py:533
  36.7 11.2 %collective-permute-start.11 = (bf16[128,512]{1,0:T(8,128)(2,1)S(1)}, bf16[128,512]{1,0:T(8,128)(2,1)S(1)}, u32[]{:S(2)}, u32[]{:S(2)}) collective-permute-start(bf16[128,512]{1,0:T(8,128)(2,1)S(1)} %get-tuple-element.105), channel_id=1, source_target_pairs={{0,4},{4,0},{8,12},{12,8},{16,20},{20,16},{24,28},{28,24},{1,5},{5... | collective-permute-start | bytes 393224 | tf_op jit(solution)/shard_map/ppermute | solution.py:533
  38.0 9.9 %collective-permute-start.12 = (bf16[128,512]{1,0:T(8,128)(2,1)S(1)}, bf16[128,512]{1,0:T(8,128)(2,1)S(1)}, u32[]{:S(2)}, u32[]{:S(2)}) collective-permute-start(bf16[128,512]{1,0:T(8,128)(2,1)S(1)} %get-tuple-element.106), channel_id=1, source_target_pairs={{0,8},{4,12},{8,0},{12,4},{16,24},{20,28},{24,16},{28,20},{1,9},{5... | collective-permute-start | bytes 393224 | tf_op jit(solution)/shard_map/ppermute | solution.py:533
  55.2 14.0 %collective-permute-start.16 = (bf16[128,2048]{1,0:T(8,128)(2,1)S(1)}, bf16[128,2048]{1,0:T(8,128)(2,1)S(1)}, u32[]{:S(2)}, u32[]{:S(2)}) collective-permute-start(bf16[128,2048]{1,0:T(8,128)(2,1)S(1)} %add_convert_fusion), channel_id=1, source_target_pairs={{0,2},{1,3},{2,0},{3,1},{4,6},{5,7},{6,4},{7,5},{8,10},{9,11},{10,... | collective-permute-start | bytes 1572872 | tf_op jit(solution)/shard_map/ppermute | solution.py:533
  73.0 11.2 %collective-permute-start.21 = (bf16[32,2048]{1,0:T(8,128)(2,1)S(1)}, bf16[32,2048]{1,0:T(8,128)(2,1)S(1)}, u32[]{:S(2)}, u32[]{:S(2)}) collective-permute-start(bf16[32,2048]{1,0:T(8,128)(2,1)S(1)} %get-tuple-element.143), channel_id=1, source_target_pairs={{0,16},{4,20},{8,24},{12,28},{16,0},{20,4},{24,8},{28,12},{1,17},{... | collective-permute-start | bytes 393224 | tf_op jit(solution)/shard_map/ppermute | solution.py:533
  73.0 13.9 %collective-permute-start.22 = (bf16[32,2048]{1,0:T(8,128)(2,1)S(1)}, bf16[32,2048]{1,0:T(8,128)(2,1)S(1)}, u32[]{:S(2)}, u32[]{:S(2)}) collective-permute-start(bf16[32,2048]{1,0:T(8,128)(2,1)S(1)} %get-tuple-element.144), channel_id=1, source_target_pairs={{0,20},{4,16},{8,28},{12,24},{16,4},{20,0},{24,12},{28,8},{1,21},{... | collective-permute-start | bytes 393224 | tf_op jit(solution)/shard_map/ppermute | solution.py:533
  92.3 8.3 %collective-permute-start.20 = (bf16[32,2048]{1,0:T(8,128)(2,1)S(1)}, bf16[32,2048]{1,0:T(8,128)(2,1)S(1)}, u32[]{:S(2)}, u32[]{:S(2)}) collective-permute-start(bf16[32,2048]{1,0:T(8,128)(2,1)S(1)} %get-tuple-element.142), channel_id=1, source_target_pairs={{0,12},{4,8},{8,4},{12,0},{16,28},{20,24},{24,20},{28,16},{1,13},{... | collective-permute-start | bytes 393224 | tf_op jit(solution)/shard_map/ppermute | solution.py:533
  107.1 9.8 %collective-permute-start.37 = (bf16[32,2048]{1,0:T(8,128)(2,1)S(1)}, bf16[32,2048]{1,0:T(8,128)(2,1)S(1)}, u32[]{:S(2)}, u32[]{:S(2)}) collective-permute-start(bf16[32,2048]{1,0:T(8,128)(2,1)S(1)} %get-tuple-element.160), channel_id=1, source_target_pairs={{0,28},{4,24},{8,20},{12,16},{16,12},{20,8},{24,4},{28,0},{1,29},{... | collective-permute-start | bytes 393224 | tf_op jit(solution)/shard_map/ppermute | solution.py:533
  120.8 8.8 %collective-permute-start.40 = (bf16[64,2048]{1,0:T(8,128)(2,1)S(1)}, bf16[64,2048]{1,0:T(8,128)(2,1)S(1)}, u32[]{:S(2)}, u32[]{:S(2)}) collective-permute-start(bf16[64,2048]{1,0:T(8,128)(2,1)S(1)} %get-tuple-element.164), channel_id=1, source_target_pairs={{0,1},{1,0},{2,3},{3,2},{4,5},{5,4},{6,7},{7,6},{8,9},{9,8},{10,11... | collective-permute-start | bytes 786440 | tf_op jit(solution)/shard_map/ppermute | solution.py:533
  121.2 13.5 %collective-permute-start.34 = (bf16[32,2048]{1,0:T(8,128)(2,1)S(1)}, bf16[32,2048]{1,0:T(8,128)(2,1)S(1)}, u32[]{:S(2)}, u32[]{:S(2)}) collective-permute-start(bf16[32,2048]{1,0:T(8,128)(2,1)S(1)} %get-tuple-element.147), channel_id=1, source_target_pairs={{0,16},{4,20},{8,24},{12,28},{16,0},{20,4},{24,8},{28,12},{1,17},{... | collective-permute-start | bytes 393224 | tf_op jit(solution)/shard_map/ppermute | solution.py:533
  124.9 13.0 %collective-permute-start.35 = (bf16[32,2048]{1,0:T(8,128)(2,1)S(1)}, bf16[32,2048]{1,0:T(8,128)(2,1)S(1)}, u32[]{:S(2)}, u32[]{:S(2)}) collective-permute-start(bf16[32,2048]{1,0:T(8,128)(2,1)S(1)} %get-tuple-element.148), channel_id=1, source_target_pairs={{0,20},{4,16},{8,28},{12,24},{16,4},{20,0},{24,12},{28,8},{1,21},{... | collective-permute-start | bytes 393224 | tf_op jit(solution)/shard_map/ppermute | solution.py:533
  125.1 16.1 %collective-permute-start.31 = (bf16[32,2048]{1,0:T(8,128)(2,1)S(1)}, bf16[32,2048]{1,0:T(8,128)(2,1)S(1)}, u32[]{:S(2)}, u32[]{:S(2)}) collective-permute-start(bf16[32,2048]{1,0:T(8,128)(2,1)S(1)} %get-tuple-element.156), channel_id=1, source_target_pairs={{0,4},{4,0},{8,12},{12,8},{16,20},{20,16},{24,28},{28,24},{1,5},{5... | collective-permute-start | bytes 393224 | tf_op jit(solution)/shard_map/ppermute | solution.py:533
  126.4 14.9 %collective-permute-start.32 = (bf16[32,2048]{1,0:T(8,128)(2,1)S(1)}, bf16[32,2048]{1,0:T(8,128)(2,1)S(1)}, u32[]{:S(2)}, u32[]{:S(2)}) collective-permute-start(bf16[32,2048]{1,0:T(8,128)(2,1)S(1)} %get-tuple-element.157), channel_id=1, source_target_pairs={{0,8},{4,12},{8,0},{12,4},{16,24},{20,28},{24,16},{28,20},{1,9},{5... | collective-permute-start | bytes 393224 | tf_op jit(solution)/shard_map/ppermute | solution.py:533
  129.6 11.6 %collective-permute-start.33 = (bf16[32,2048]{1,0:T(8,128)(2,1)S(1)}, bf16[32,2048]{1,0:T(8,128)(2,1)S(1)}, u32[]{:S(2)}, u32[]{:S(2)}) collective-permute-start(bf16[32,2048]{1,0:T(8,128)(2,1)S(1)} %get-tuple-element.158), channel_id=1, source_target_pairs={{0,12},{4,8},{8,4},{12,0},{16,28},{20,24},{24,20},{28,16},{1,13},{... | collective-permute-start | bytes 393224 | tf_op jit(solution)/shard_map/ppermute | solution.py:533
  149.0 8.4 %collective-permute-start.44 = (bf16[64,2048]{1,0:T(8,128)(2,1)S(1)}, bf16[64,2048]{1,0:T(8,128)(2,1)S(1)}, u32[]{:S(2)}, u32[]{:S(2)}) collective-permute-start(bf16[64,2048]{1,0:T(8,128)(2,1)S(1)} %slice.17), channel_id=1, source_target_pairs={{0,2},{1,3},{2,0},{3,1},{4,6},{5,7},{6,4},{7,5},{8,10},{9,11},{10,... | collective-permute-start | bytes 786440 | tf_op jit(solution)/shard_map/ppermute | solution.py:533
  (41 other events, 492.1 us)

commit v2 on v1

v2 whole, which is shorter than its diff:
```python
import functools
import jax
import jax.numpy as jnp
from jax import lax
from jax.experimental import pallas as pl
from jax.experimental.pallas import tpu as pltpu
from jax.sharding import PartitionSpec as P


HK = 256
HV = 512
TOP = 2
BLK = 128
TEMPER = 16.0
EPSILON = 1e-06
F32 = jnp.float32
BF16 = jnp.bfloat16
VMEM = pl.BlockSpec(memory_space=pltpu.VMEM)
SMEM = pl.BlockSpec(memory_space=pltpu.SMEM)
HBM = pl.BlockSpec(memory_space=pltpu.HBM)
QUAD = 4


def cost(flops, moved):
    return pl.CostEstimate(flops=int(flops), bytes_accessed=int(moved), transcendentals=0)


def params(mib):
    return pltpu.CompilerParams(vmem_limit_bytes=mib * 1024 * 1024)


def place():
    tp = lax.axis_index("tp")
    return lax.axis_index("sp"), tp % 2, tp // 2


def xor_perm(axis, k):
    return [(i, i ^ k) for i in range(lax.axis_size(axis))]


def tri(n, fn):
    row = lax.broadcasted_iota(jnp.int32, (n, n), 0)
    col = lax.broadcasted_iota(jnp.int32, (n, n), 1)
    return fn(row, col)


def contract0(a, b):
    return lax.dot_general(a, b, (((0,), (0,)), ((), ())), preferred_element_type=F32)


def contract1(a, b):
    return lax.dot_general(a, b, (((1,), (1,)), ((), ())), preferred_element_type=F32)


def split_dot(ones, value):
    total = None
    for _ in range(3):
        part = value.astype(BF16)
        value = value - part.astype(F32)
        term = jnp.dot(ones, part, preferred_element_type=F32)
        total = term if total is None else total + term
    return total


def head_log_decay(low, matrix, bias, shift, head):
    pre = contract0(low, matrix) + bias
    logged = (jnp.minimum(pre, 0.0) - jnp.log1p(jnp.exp(-jnp.abs(pre)))) / TEMPER
    return logged + jnp.transpose(shift)[:, head : head + 1]


def state_kernel(first, count, low, matrix, bias, shift, key_rows, values, *rest):
    outs = rest[:QUAD]
    keys, vals, state, decays, sems = rest[QUAD:]
    length = low.shape[1]
    piece = HK // QUAD
    copies = []
    for h in range(count):
        at = first + h
        pair = (
            pltpu.make_async_copy(
                key_rows.at[:, at * HK : (at + 1) * HK], keys.at[h], sems.at[0, h]
            ),
            pltpu.make_async_copy(
                values.at[:, at * HV : (at + 1) * HV], vals.at[h], sems.at[1, h]
            ),
        )
        for copy in pair:
            copy.start()
        copies.append(pair)
    after = tri(length, lambda r, c: c > r).astype(F32).astype(BF16)
    me = place()[0] % QUAD
    decays[...] = jnp.zeros_like(decays)
    for h in range(count):
        span = slice((first + h) * HK, (first + h + 1) * HK)
        logs = head_log_decay(low[...], matrix[:, span], bias[:, span], shift[...], first + h)
        suffix = split_dot(after, logs)
        total = jnp.exp(suffix[0:1, :] + logs[0:1, :])
        high = total.astype(BF16).astype(F32)
        decays[h : h + 1, 0:HK] = high
        decays[h : h + 1, HK : 2 * HK] = total - high
        for copy in copies[h]:
            copy.wait()
        end_keys = (keys[h].astype(F32) * jnp.exp(suffix)).astype(BF16)
        state[...] = contract0(end_keys, vals[h])
        for k in range(QUAD):
            start = pl.multiple_of((me ^ k) * piece, piece)
            outs[k][h * piece : (h + 1) * piece, :] = state[pl.ds(start, piece), :].astype(BF16)
    for k in range(QUAD):
        outs[k][count * piece :, :] = decays[...].astype(BF16)


def device_states(first, count, low, matrix, bias, shift, key_rows, values):
    length = key_rows.shape[0]
    rows = count * (HK // QUAD) + 8
    return pl.pallas_call(
        functools.partial(state_kernel, first, count),
        in_specs=[VMEM] * 4 + [HBM] * 2,
        out_specs=[VMEM] * QUAD,
        out_shape=[jax.ShapeDtypeStruct((rows, HV), BF16)] * QUAD,
        scratch_shapes=[
            pltpu.VMEM((count, length, HK), BF16),
            pltpu.VMEM((count, length, HV), BF16),
            pltpu.VMEM((HK, HV), F32),
            pltpu.VMEM((8, HV), F32),
            pltpu.SemaphoreType.DMA((2, count)),
        ],
        compiler_params=params(60),
        cost_estimate=cost(count * 4e8, count * 5e5),
    )(low, matrix, bias, shift, key_rows, values)


def local_kernel(first, count, low, matrix, bias, shift, queries, key_rows, values, *refs):
    out, query_out = refs[-2:]
    length = low.shape[1]
    below = tri(BLK, lambda r, c: c <= r)
    lower = below.astype(F32).astype(BF16)
    scale = HK ** (-0.5)
    for h in range(count):
        narrow, wide = slice(h * HK, (h + 1) * HK), slice(h * HV, (h + 1) * HV)
        logs = head_log_decay(
            low[...], matrix[:, narrow], bias[:, narrow], shift[...], first + h
        )
        before = jnp.zeros((1, HK), F32)
        earlier = []
        for b in range(length // BLK):
            rows = slice(b * BLK, (b + 1) * BLK)
            inside = split_dot(lower, logs[rows])
            final = inside[BLK - 1 : BLK, :]
            middle = inside[BLK // 2 - 1 : BLK // 2, :]
            query = queries[rows, narrow].astype(F32) * scale
            keys = key_rows[rows, narrow].astype(F32)
            grown = query * jnp.exp(inside)
            near_query = (query * jnp.exp(inside - middle)).astype(BF16)
            near_key = (keys * jnp.exp(middle - inside)).astype(BF16)
            scores = jnp.where(below, contract1(near_query, near_key), 0.0).astype(BF16)
            total = jnp.dot(scores, values[rows, wide], preferred_element_type=F32)
            here = grown.astype(BF16)
            for past_keys, past in earlier:
                cross = contract1(here, past_keys.astype(BF16)).astype(BF16)
                total = total + jnp.dot(cross, values[past, wide], preferred_element_type=F32)
            out[rows, wide] = total
            query_out[rows, narrow] = (grown * jnp.exp(before)).astype(BF16)
            if b + 1 < length // BLK:
                earlier = [(old * jnp.exp(final), past) for old, past in earlier]
                earlier.append((keys * jnp.exp(final - inside), rows))
                before = before + final


def local_attention(first, count, low, matrix, bias, shift, queries, key_rows, values):
    length = low.shape[1]
    block = first // count

    def part(width):
        return pl.BlockSpec((length, count * width), lambda i: (0, block))

    return pl.pallas_call(
        functools.partial(local_kernel, first, count),
        grid=(1,),
        in_specs=[
            pl.BlockSpec(low.shape, lambda i: (0, 0)),
            pl.BlockSpec((low.shape[0], count * HK), lambda i: (0, block)),
            pl.BlockSpec((1, count * HK), lambda i: (0, block)),
            pl.BlockSpec(shift.shape, lambda i: (0, 0)),
            part(HK),
            part(HK),
            part(HV),
        ],
        out_specs=[
            pl.BlockSpec((length, count * HV), lambda i: (0, 0)),
            pl.BlockSpec((length, count * HK), lambda i: (0, 0)),
        ],
        out_shape=[
            jax.ShapeDtypeStruct((length, count * HV), F32),
            jax.ShapeDtypeStruct((length, count * HK), BF16),
        ],
        compiler_params=params(24),
        cost_estimate=cost(count * 4e8, count * 1.2e6),
    )(low, matrix, bias, shift, queries, key_rows, values)


def prefix_kernel(count, emit, primed, *refs):
    start, refs = (refs[0], refs[1:]) if primed else (None, refs)
    ins, outs = refs[:QUAD], refs[QUAD:]
    me = place()[0] % QUAD
    piece = HK // QUAD
    rows = count * piece
    tails = jnp.concatenate([ref[rows : rows + 8, :].astype(F32) for ref in ins], axis=0)
    across = jnp.transpose(tails[:, :HK] + tails[:, HK:])
    parts = [across[i * piece : (i + 1) * piece, :] for i in range(QUAD)]
    mine = parts[0]
    for i in range(1, QUAD):
        mine = jnp.where(me == i, parts[i], mine)
    decay = [mine[:, k * 8 : k * 8 + count] for k in range(QUAD)]
    spot = [me ^ k for k in range(QUAD)]
    ends = spot if emit else [jnp.int32(QUAD)]

    def between(low, end):
        factor = jnp.ones_like(decay[0])
        for k in range(QUAD):
            inside = jnp.logical_and(spot[k] > low, spot[k] < end)
            factor = jnp.where(inside, factor * decay[k], factor)
        return factor

    weights = [
        [jnp.where(spot[k] < end, between(spot[k], end), 0.0) for k in range(QUAD)]
        + ([between(-1, end)] if primed else [])
        for end in ends
    ]
    for h in range(count):
        span = slice(h * piece, (h + 1) * piece)
        sources = [ref[span, :].astype(F32) for ref in ins]
        if primed:
            sources.append(start[span, :].astype(F32))
        for out, factors in zip(outs, weights):
            total = None
            for source, factor in zip(sources, factors):
                term = source * factor[:, h : h + 1]
                total = term if total is None else total + term
            out[span, :] = total.astype(BF16)


def quad_prefix(count, emit, start, pieces):
    rows = count * (HK // QUAD)
    outs = QUAD if emit else 1
    primed = [] if start is None else [start]
    return pl.pallas_call(
        functools.partial(prefix_kernel, count, emit, start is not None),
        in_specs=[VMEM] * (QUAD + len(primed)),
        out_specs=[VMEM] * outs,
        out_shape=[jax.ShapeDtypeStruct((rows, HV), BF16)] * outs,
        compiler_params=params(24),
        cost_estimate=cost(1e8, 1e6),
        name="quad_prefix" if emit else "quad_total",
    )(*primed, *pieces)


def quad_entry(count, pieces):
    start = None
    quads = lax.axis_size("sp") // QUAD
    entry = None
    for g in range(quads - 1):
        (total,) = quad_prefix(count, False, start, pieces)
        perm = [(g * QUAD + i, (g + 1) * QUAD + i) for i in range(QUAD)]
        start = lax.ppermute(total, "sp", perm)
        entry = start if entry is None else entry + start
    return entry


def block_spans(groups, rows):
    _, core, line = place()
    for k in range(groups):
        base = (line ^ k) * 2
        own = pl.ds(pl.multiple_of((base + core) * rows, rows), rows)
        other = pl.ds(pl.multiple_of((base + 1 - core) * rows, rows), rows)
        yield slice(k * rows, (k + 1) * rows), own, other


def project_kernel(count, groups, gain, matrix, *refs):
    mixed, keep, send, carried = refs[-4:]
    chunks = len(refs[:-4]) // (2 + QUAD)
    local, queries, pieces = refs[:chunks], refs[chunks : 2 * chunks], refs[2 * chunks : -4]
    me, my_core, my_line = place()
    me = me % QUAD
    piece = HK // QUAD
    split = keep.shape[0]
    rows = split // groups
    for part in range(chunks):
        for h in range(count):
            span = slice(h * piece, (h + 1) * piece)
            for k in range(QUAD):
                start = pl.multiple_of((me ^ k) * piece, piece)
                carried[pl.ds(start, piece), :] = pieces[part * QUAD + k][span, :]
            narrow, wide = slice(h * HK, (h + 1) * HK), slice(h * HV, (h + 1) * HV)
            out = local[part][:, wide] + jnp.dot(
                queries[part][:, narrow], carried[...], preferred_element_type=F32
            )
            spread = lax.rsqrt(jnp.mean(out * out, axis=-1, keepdims=True) + EPSILON)
            value = (out * spread * gain[...]).astype(BF16)
            at = (part * count + h) * HV
            for b in range(2 * groups):
                line, core = b // 2, b % 2
                there = (line ^ my_line) + (core ^ my_core) * groups
                there = pl.multiple_of(there * rows, rows)
                mixed[pl.ds(there, rows), at : at + HV] = value[b * rows : (b + 1) * rows, :]
    keep[...] = jnp.dot(mixed[:split, :], matrix[...], preferred_element_type=F32)
    send[...] = jnp.dot(mixed[split:, :], matrix[...], preferred_element_type=F32).astype(BF16)


def project_rest_kernel(mixed, matrix, keep, send):
    split = keep.shape[0]
    total = jnp.dot(mixed[...], matrix[...], preferred_element_type=F32)
    keep[...] = total[:split, :]
    send[...] = total[split:, :].astype(BF16)


def project(count, groups, gain, matrix, local, pieces):
    outs = [array for array, _ in local] + [array for _, array in local]
    length = outs[0].shape[0]
    depth, width = matrix.shape
    cut = width // 2
    small = [
        jax.ShapeDtypeStruct((length // 2, cut), F32),
        jax.ShapeDtypeStruct((length // 2, cut), BF16),
    ]
    whole = [pl.BlockSpec((length // 2, cut), lambda i: (0, 0))] * 2
    mixed, keep, send = pl.pallas_call(
        functools.partial(project_kernel, count, groups),
        grid=(1,),
        in_specs=[VMEM, pl.BlockSpec((depth, cut), lambda i: (0, 0))]
        + [VMEM] * (len(outs) + len(pieces)),
        out_specs=[pl.BlockSpec((length, depth), lambda i: (0, 0))] + whole,
        out_shape=[jax.ShapeDtypeStruct((length, depth), BF16)] + small,
        scratch_shapes=[pltpu.VMEM((HK, HV), BF16)],
        compiler_params=params(28),
        cost_estimate=cost(2e9, 8e6),
        name="project",
    )(gain, matrix, *outs, *pieces)
    rest = pl.pallas_call(
        project_rest_kernel,
        grid=(1,),
        in_specs=[
            pl.BlockSpec((length, depth), lambda i: (0, 0)),
            pl.BlockSpec((depth, cut), lambda i: (0, 1)),
        ],
        out_specs=whole,
        out_shape=small,
        compiler_params=params(28),
        cost_estimate=cost(1e9, 6e6),
        name="project_rest",
    )(mixed, matrix)
    return (keep, send), rest


def norm_kernel(groups, gain, *refs):
    keeps, received, streams = refs[:2], refs[2:4], refs[4 : 4 + groups]
    arrived = refs[4 + groups : 4 + groups + 2 * (groups - 1)]
    normed, mid = refs[-2:]
    rows, width = mid.shape
    cut = width // 2
    for k in range(groups):
        span = slice(k * rows, (k + 1) * rows)
        values, square = [], None
        for side in range(2):
            columns = slice(side * cut, (side + 1) * cut)
            value = keeps[side][span, :] + received[side][span, :].astype(F32)
            for j in range(1, groups):
                there = k ^ j
                part = arrived[side * (groups - 1) + j - 1]
                value = value + part[there * rows : (there + 1) * rows, :].astype(F32)
            value = value + streams[k][:, columns].astype(F32)
            if k == 0:
                mid[:, columns] = value
            term = jnp.sum(value * value, axis=-1, keepdims=True)
            square = term if square is None else square + term
            values.append((columns, value))
        spread = lax.rsqrt(square / width + EPSILON)
        for columns, value in values:
            normed[span, columns] = (value * spread * gain[:, columns]).astype(BF16)


def midstream_norm(groups, gain, keeps, received, streams, arrived):
    rows, width = streams[0].shape
    arrays = [*keeps, *received, *streams, *arrived]
    return pl.pallas_call(
        functools.partial(norm_kernel, groups),
        in_specs=[VMEM] * (1 + len(arrays)),
        out_specs=[VMEM] * 2,
        out_shape=[
            jax.ShapeDtypeStruct((groups * rows, width), BF16),
            jax.ShapeDtypeStruct((rows, width), F32),
        ],
        compiler_params=params(24),
        cost_estimate=cost(1e7, 3e6),
        name="midstream_norm",
    )(gain, *arrays)


def route_kernel(n, half, groups, routes, weights, select, high, low, table):
    me, core, _ = place()
    length = routes.shape[1]
    earlier = tri(length, lambda r, c: c < r).astype(F32).astype(BF16)
    chosen = jnp.transpose(routes[...].astype(F32)).astype(jnp.int32)
    weight = jnp.transpose(weights[...])
    expert = me ^ lax.broadcasted_iota(jnp.int32, (length, n), 1)
    is_first, is_second = chosen[:, 0:1] == expert, chosen[:, 1:2] == expert
    member = jnp.where(is_first | is_second, 1.0, 0.0)
    rank = jnp.dot(earlier, member.astype(BF16), preferred_element_type=F32)
    slot = jnp.where(member > 0.0, rank, -1.0)
    value = jnp.where(is_first, weight[:, 0:1], weight[:, 1:2])
    top = value.astype(BF16)
    rest = (value - top.astype(F32)).astype(BF16)
    column = lax.broadcasted_iota(jnp.int32, (n, n * half), 1)
    owner = lax.broadcasted_iota(jnp.int32, (n, n * half), 0)
    spread = jnp.where(column // half == owner, 1.0, 0.0).astype(BF16)

    def widen(array):
        return jnp.dot(array, spread, preferred_element_type=F32)

    wanted = core * half + lax.broadcasted_iota(jnp.int32, (length, n * half), 1) % half
    hit = widen(slot.astype(BF16)) == wanted.astype(F32)
    table[0] = jnp.where(hit, 1.0, 0.0)
    table[1] = jnp.where(hit, widen(top), 0.0)
    table[2] = jnp.where(hit, widen(rest), 0.0)
    split = length // 2
    ordered = []
    for span, own, other in block_spans(groups, split // groups):
        below = slice(split + span.start, split + span.stop)
        for out, source in ((high, 1), (low, 2)):
            out[span, :] = table[source, own, :].astype(BF16)
            out[below, :] = table[source, other, :].astype(BF16)
        ordered.append((table[0, own, :], table[0, other, :]))
    chosen = jnp.concatenate([own for own, _ in ordered] + [other for _, other in ordered])
    select[...] = jnp.transpose(chosen).astype(BF16)


def slot_tables(n, half, groups, routes, weights):
    length = routes.shape[1]
    return pl.pallas_call(
        functools.partial(route_kernel, n, half, groups),
        in_specs=[VMEM, VMEM],
        out_specs=[VMEM] * 3,
        out_shape=[
            jax.ShapeDtypeStruct((n * half, length), BF16),
            jax.ShapeDtypeStruct((length, n * half), BF16),
            jax.ShapeDtypeStruct((length, n * half), BF16),
        ],
        scratch_shapes=[pltpu.VMEM((3, length, n * half), F32)],
        compiler_params=params(16),
        cost_estimate=cost(1e8, 5e5),
        name="slot_tables",
    )(routes, weights)


def dispatch_kernel(n, half, select, mine, theirs, *outs):
    split = mine.shape[0]
    picked = jnp.dot(select[:, :split], mine[...], preferred_element_type=F32)
    picked = picked + jnp.dot(select[:, split:], theirs[...], preferred_element_type=F32)
    for k in range(n):
        outs[k][...] = picked[k * half : (k + 1) * half, :].astype(BF16)


def dispatch(n, half, select, mine, theirs):
    width = mine.shape[1]
    return pl.pallas_call(
        functools.partial(dispatch_kernel, n, half),
        in_specs=[VMEM] * 3,
        out_specs=[VMEM] * n,
        out_shape=[jax.ShapeDtypeStruct((half, width), BF16)] * n,
        compiler_params=params(16),
        cost_estimate=cost(5e8, 2e6),
        name="dispatch",
    )(select, mine, theirs)


def fetch_kernel(*refs):
    half = (len(refs) - 1) // 2
    ins, outs, sems = refs[:half], refs[half:-1], refs[-1]
    copies = [
        pltpu.make_async_copy(src, dst, sems.at[i])
        for i, (src, dst) in enumerate(zip(ins, outs))
    ]
    for copy in copies:
        copy.start()
    for copy in copies:
        copy.wait()


def fetch(*arrays):
    return pl.pallas_call(
        fetch_kernel,
        in_specs=[HBM] * len(arrays),
        out_specs=[VMEM] * len(arrays),
        out_shape=[jax.ShapeDtypeStruct(a.shape, a.dtype) for a in arrays],
        scratch_shapes=[pltpu.SemaphoreType.DMA((len(arrays),))],
        compiler_params=params(16),
        cost_estimate=cost(2e9, 1e7),
        name="fetch",
    )(*arrays)


def expert_kernel(count, gate, widen, down, *refs):
    ins, (keep, send) = refs[: 2 * count], refs[2 * count :]
    rows = jnp.concatenate([piece[...] for piece in ins], axis=0)
    gated = contract1(rows, gate[...])
    lifted = contract1(rows, widen[...])
    hidden = (gated * jax.nn.sigmoid(gated) * lifted).astype(BF16)
    out = jnp.dot(hidden, down[...], preferred_element_type=F32)
    split = keep.shape[0]
    keep[...] = out[:split, :]
    send[...] = out[split:, :].astype(BF16)


def expert(weights, mine, theirs):
    count = len(mine)
    half, width = mine[0].shape
    return pl.pallas_call(
        functools.partial(expert_kernel, count),
        in_specs=[VMEM] * (3 + 2 * count),
        out_specs=[VMEM] * 2,
        out_shape=[
            jax.ShapeDtypeStruct((count * half, width), F32),
            jax.ShapeDtypeStruct((count * half, width), BF16),
        ],
        compiler_params=params(24),
        cost_estimate=cost(6e8 * count, 4e6),
    )(*weights, *mine, *theirs)


def merge_kernel(count, keep, received, *outs):
    half = outs[0].shape[0]
    for k in range(count):
        span = slice(k * half, (k + 1) * half)
        outs[k][...] = (keep[span, :] + received[span, :].astype(F32)).astype(BF16)


def merge(count, half, keep, received):
    width = keep.shape[1]
    return pl.pallas_call(
        functools.partial(merge_kernel, count),
        in_specs=[VMEM] * 2,
        out_specs=[VMEM] * count,
        out_shape=[jax.ShapeDtypeStruct((half, width), BF16)] * count,
        compiler_params=params(16),
        cost_estimate=cost(1e7, 4e6),
    )(keep, received)


def combine_kernel(n, high, low, *refs):
    ins, (keep, send) = refs[:n], refs[n:]
    rows = jnp.concatenate([piece[...] for piece in ins], axis=0)
    total = jnp.dot(high[...], rows, preferred_element_type=F32)
    total = total + jnp.dot(low[...], rows, preferred_element_type=F32)
    split = keep.shape[0]
    keep[...] = total[:split, :]
    send[...] = total[split:, :].astype(BF16)


def combine(n, high, low, pieces):
    width = pieces[0].shape[1]
    length = high.shape[0]
    return pl.pallas_call(
        functools.partial(combine_kernel, n),
        in_specs=[VMEM] * (2 + n),
        out_specs=[VMEM] * 2,
        out_shape=[
            jax.ShapeDtypeStruct((length // 2, width), F32),
            jax.ShapeDtypeStruct((length // 2, width), BF16),
        ],
        compiler_params=params(16),
        cost_estimate=cost(1e9, 3e6),
        name="combine",
    )(high, low, *pieces)


def swap(value, axis, k):
    return lax.ppermute(value, axis, xor_perm(axis, k))


def exchange(pieces):
    return [pieces[0]] + [swap(pieces[k], "sp", k) for k in range(1, len(pieces))]


def body(
    stream_in,
    queries,
    key_rows,
    values,
    decay_low,
    decay_matrix,
    decay_bias,
    decay_shift,
    head_gain,
    output_matrix,
    feed_gain,
    routes,
    route_weights,
    expert_gate,
    specialist_widen,
    expert_down,
):
    length = queries.shape[0]
    heads = queries.shape[1] // HK
    n = lax.axis_size("sp")
    head_devices = lax.axis_size("tp")
    groups = head_devices // 2
    rows = length // head_devices
    half = TOP * length // n // 2
    bias = decay_bias.reshape(1, -1)

    low, shift = decay_low.T, decay_shift.T
    count = heads // 2 if heads % 2 == 0 else heads

    gathered, states = [], None
    for part, first in enumerate(range(0, heads, count)):
        low_here = low
        if states is not None:
            low_here, states = lax.optimization_barrier((low, states))
        states = device_states(
            first, count, low_here, decay_matrix, bias, shift, key_rows, values
        )
        gathered.append(exchange(states))
    stream_in, _ = lax.optimization_barrier((stream_in, states))
    streams = [stream_in] + [swap(stream_in, "tp", 2 * k) for k in range(1, groups)]
    local = [
        local_attention(
            first, count, low, decay_matrix, bias, shift, queries, key_rows, values
        )
        for first in range(0, heads, count)
    ]
    select, high, low_part = slot_tables(
        n, half, groups, routes.T, route_weights.T
    )
    carried = []
    for part, pieces in enumerate(gathered):
        entry = quad_entry(count, pieces)
        carried += exchange(quad_prefix(count, True, entry, pieces))
    sides = project(
        count, groups, head_gain.reshape(1, -1), output_matrix, local, carried
    )
    received, shared = [], []
    for keep, send in sides:
        received.append(swap(send, "tp", 1))
        shared.append((keep + received[-1].astype(F32)).astype(BF16))
    arrived = [swap(value, "tp", 2 * k) for value in shared for k in range(1, groups)]
    weights, _ = lax.optimization_barrier(
        ((expert_gate[0].T, specialist_widen[0].T, expert_down[0]), shared)
    )
    weights = fetch(*weights)
    arrived, weights, select, high, low_part = lax.optimization_barrier(
        (arrived, weights, select, high, low_part)
    )
    normed, mid = midstream_norm(
        groups,
        feed_gain.reshape(1, -1),
        [keep for keep, _ in sides],
        received,
        streams,
        arrived,
    )
    theirs = swap(normed, "tp", 1)
    slots = dispatch(n, half, select, normed, theirs)
    slots = exchange(slots)
    back, previous = {}, None
    for part, ks in enumerate(expert_chunks(n)):
        mine = [slots[k] for k in ks]
        if previous is not None:
            mine, previous = lax.optimization_barrier((mine, previous))
        theirs = [swap(slot, "tp", 1) for slot in mine]
        kept, sent = expert(weights, mine, theirs)
        received = swap(sent, "tp", 1)
        merged = merge(len(ks), half, kept, received)
        previous = sent if part == 1 else merged
        for k, piece in zip(ks, merged):
            back[k] = piece if k == 0 else swap(piece, "sp", k)
    back = [back[k] for k in range(n)]
    keep, send = combine(n, high, low_part, back)
    summed = keep + swap(send, "tp", 1).astype(F32)
    total = mid + summed[:rows]
    for k in range(1, groups):
        part = summed[k * rows : (k + 1) * rows].astype(BF16)
        total = total + swap(part, "tp", 2 * k).astype(F32)
    return total.astype(BF16)


def expert_chunks(n):
    middle = (QUAD + n) // 2
    return [range(QUAD, middle), range(QUAD), range(middle, n)]


def solution(mesh):
    return jax.shard_map(
        body,
        mesh=mesh,
        in_specs=(
            P(("sp", "tp"), None),
            P("sp", "tp"),
            P("sp", "tp"),
            P("sp", "tp"),
            P("sp", None),
            P(None, "tp"),
            P("tp"),
            P("sp", "tp"),
            P(),
            P("tp", None),
            P(),
            P("sp", None),
            P("sp", None),
            P("sp", None, "tp"),
            P("sp", None, "tp"),
            P("sp", "tp", None),
        ),
        out_specs=P(("sp", "tp"), None),
        check_vma=False,
    )
```

time: 159 us -> 159 us (level)
  waiting for transfers between devices: 61.9 us -> 69.3 us
  Pallas kernels: 35.3 us -> 29 us
    ppermute x43 -> x45, waiting for transfers between devices: 61.9 us -> 69.3 us  [swap(): return lax.ppermute(value, axis, xor_perm(axis, k))]
    pallas_call x12 -> x13, Pallas kernels: 26.4 us -> 20.2 us  [the longest x2 7.61 us: device_states(): pl.pallas_call(functools.partial(state_kernel, first, count), in_specs=[V...]
    ppermute x43 -> x45, starting transfers between devices: 49.3 us -> 46.9 us  [swap(): return lax.ppermute(value, axis, xor_perm(axis, k))]
    ppermute x2, starting transfers between devices: 8.49 us -> 10.2 us  [quad_entry(): start = lax.ppermute(total, 'sp', perm)]
  transfers between devices with their start and end apart: 45 -> 47, of which waited for: 23 -> 21; matrix products, arithmetic and copies ran while one was open for 0% -> 0% of each run, Pallas kernels for 10% -> 11%
where the time goes in v2:
time: 159 us
  waiting for transfers between devices  69.3 us (44%)
  starting transfers between devices  57 us (36%)
  Pallas kernels  29 us (18%)
  local copies, waits for them, and re-layouts  1.95 us (1%)
    ppermute x45, waiting for transfers between devices, swap(): return lax.ppermute(value, axis, xor_perm(axis, k))  69.3 us
    ppermute x45, starting transfers between devices, swap(): return lax.ppermute(value, axis, xor_perm(axis, k))  46.9 us
    ppermute x2, starting transfers between devices, quad_entry(): start = lax.ppermute(total, 'sp', perm)  10.2 us
    pallas_call x2, Pallas kernels, device_states(): pl.pallas_call(functools.partial(state_kernel, first, count), in_specs=[V...  7.61 us
    pallas_call x3, Pallas kernels, expert(): pl.pallas_call(functools.partial(expert_kernel, count), in_specs=[VMEM] *...  7.35 us
    pallas_call x2, Pallas kernels, local_attention(): pl.pallas_call(functools.partial(local_kernel, first, count), grid=(1,),...  5.11 us
  transfers between devices with their start and end apart: 47, of which 21 were waited for; matrix products, arithmetic and copies ran while one was open for 0% of the time, Pallas kernels for 11%

profile of v2, /device:TPU:0, one launch (start us, length us, event | category | flops | bytes accessed | tf_op | source)
XLA Modules:
  0.0 158.8 jit_solution(17438956479813545281)
XLA Ops:
  0.0 3.8 %shard_map.156 = (bf16[136,512]{1,0:T(8,128)(2,1)}, bf16[136,512]{1,0:T(8,128)(2,1)}, bf16[136,512]{1,0:T(8,128)(2,1)}, bf16[136,512]{1,0:T(8,128)(2,1)}) custom-call(bf16[16,256]{1,0:T(8,128)(2,1)} %bitcast.19, bf16[16,1024]{1,0:T(8,128)(2,1)} %matrix.9, f32[1,1024]{1,0:T(1,128)} %bitcast.23, f32[4,256]{1,0:T(4,128)} %bitcast.27, ...), custom_call_target="tpu_custom_call" | custom-call | flops 800000000 | bytes 1000000 | tf_op jit(solution)/shard_map/pallas_call | solution.py:115
  3.9 3.0 %collective-permute-start = (bf16[136,512]{1,0:T(8,128)(2,1)}, bf16[136,512]{1,0:T(8,128)(2,1)S(1)}, u32[]{:S(2)}, u32[]{:S(2)}) collective-permute-start(bf16[136,512]{1,0:T(8,128)(2,1)} %get-tuple-element.86), channel_id=1, source_target_pairs={{0,4},{4,0},{8,12},{12,8},{16,20},{20,16},{24,28},{28,24},{1,5},{5... | collective-permute-start | bytes 417800 | tf_op jit(solution)/shard_map/ppermute | solution.py:576
  8.5 3.8 %shard_map.157 = (bf16[136,512]{1,0:T(8,128)(2,1)}, bf16[136,512]{1,0:T(8,128)(2,1)}, bf16[136,512]{1,0:T(8,128)(2,1)}, bf16[136,512]{1,0:T(8,128)(2,1)}) custom-call(bf16[16,256]{1,0:T(8,128)(2,1)} %bitcast.20, bf16[16,1024]{1,0:T(8,128)(2,1)} %matrix.9, f32[1,1024]{1,0:T(1,128)} %bitcast.24, f32[4,256]{1,0:T(4,128)} %bitcast.28, ...), custom_call_target="tpu_custom_call" | custom-call | flops 800000000 | bytes 1000000 | tf_op jit(solution)/shard_map/pallas_call | solution.py:115
  16.3 5.2 %collective-permute-start.3 = (bf16[128,512]{1,0:T(8,128)(2,1)S(1)}, bf16[128,512]{1,0:T(8,128)(2,1)S(1)}, u32[]{:S(2)}, u32[]{:S(2)}) collective-permute-start(bf16[128,512]{1,0:T(8,128)(2,1)S(1)} %quad_total.2), channel_id=1, source_target_pairs={{0,16},{4,20},{8,24},{12,28},{1,17},{5,21},{9,25},{13,29},{2,18},{... | collective-permute-start | bytes 393224 | tf_op jit(solution)/shard_map/ppermute | solution.py:264
  23.5 5.0 %collective-permute-start.10 = (bf16[128,512]{1,0:T(8,128)(2,1)S(1)}, bf16[128,512]{1,0:T(8,128)(2,1)S(1)}, u32[]{:S(2)}, u32[]{:S(2)}) collective-permute-start(bf16[128,512]{1,0:T(8,128)(2,1)S(1)} %quad_total.3), channel_id=1, source_target_pairs={{0,16},{4,20},{8,24},{12,28},{1,17},{5,21},{9,25},{13,29},{2,18},{... | collective-permute-start | bytes 393224 | tf_op jit(solution)/shard_map/ppermute | solution.py:264
  29.9 2.8 %collective-permute-start.5 = (bf16[128,512]{1,0:T(8,128)(2,1)S(1)}, bf16[128,512]{1,0:T(8,128)(2,1)S(1)}, u32[]{:S(2)}, u32[]{:S(2)}) collective-permute-start(bf16[128,512]{1,0:T(8,128)(2,1)S(1)} %get-tuple-element.91), channel_id=1, source_target_pairs={{0,8},{4,12},{8,0},{12,4},{16,24},{20,28},{24,16},{28,20},{1,9},{5... | collective-permute-start | bytes 393224 | tf_op jit(solution)/shard_map/ppermute | solution.py:576
  39.5 2.6 %shard_map.155 = (f32[256,1024]{1,0:T(8,128)S(1)}, bf16[256,512]{1,0:T(8,128)(2,1)S(1)}) custom-call(bf16[16,256]{1,0:T(8,128)(2,1)S(1)} %bitcast.21, bf16[16,1024]{1,0:T(8,128)(2,1)S(1)} %copy-done.13, f32[1,1024]{1,0:T(1,128)S(1)} %bitcast.25, f32[4,256]{1,0:T(4,128)S(1)} %bitcast.29, bf16[256,1024]{1,0:T(8,128)(2,1)S(1)} %copy-done.11, ...), custom_call_target="tpu_custom_call" | custom-call | flops 800000000 | bytes 2400000 | tf_op jit(solution)/shard_map/pallas_call | solution.py:176
  42.1 2.6 %shard_map.154 = (f32[256,1024]{1,0:T(8,128)S(1)}, bf16[256,512]{1,0:T(8,128)(2,1)S(1)}) custom-call(bf16[16,256]{1,0:T(8,128)(2,1)S(1)} %bitcast.22, bf16[16,1024]{1,0:T(8,128)(2,1)S(1)} %copy-done.13, f32[1,1024]{1,0:T(1,128)S(1)} %bitcast.26, f32[4,256]{1,0:T(4,128)S(1)} %bitcast.30, bf16[256,1024]{1,0:T(8,128)(2,1)S(1)} %copy-done.11, ...), custom_call_target="tpu_custom_call" | custom-call | flops 800000000 | bytes 2400000 | tf_op jit(solution)/shard_map/pallas_call | solution.py:176
  55.3 3.7 %collective-permute-done.18.refs_7_ = bf16[128,1024]{1,0:T(8,128)(2,1)S(1)} collective-permute-done((bf16[128,1024]{1,0:T(8,128)(2,1)S(1)}, bf16[128,1024]{1,0:T(8,128)(2,1)S(1)}, u32[]{:S(2)}, u32[]{:S(2)}) %collective-permute-start.18) | collective-permute-done | bytes 262176 | tf_op jit(solution)/shard_map/ppermute | solution.py:576
  59.0 5.6 %collective-permute-done.17.refs_6_ = bf16[128,1024]{1,0:T(8,128)(2,1)S(1)} collective-permute-done((bf16[128,1024]{1,0:T(8,128)(2,1)S(1)}, bf16[128,1024]{1,0:T(8,128)(2,1)S(1)}, u32[]{:S(2)}, u32[]{:S(2)}) %collective-permute-start.17) | collective-permute-done | bytes 262176 | tf_op jit(solution)/shard_map/ppermute | solution.py:576
  64.6 4.8 %collective-permute-done.16.refs_5_ = bf16[64,2048]{1,0:T(8,128)(2,1)S(1)} collective-permute-done((bf16[64,2048]{1,0:T(8,128)(2,1)S(1)}, bf16[64,2048]{1,0:T(8,128)(2,1)S(1)}, u32[]{:S(2)}, u32[]{:S(2)}) %collective-permute-start.16) | collective-permute-done | bytes 262176 | tf_op jit(solution)/shard_map/ppermute | solution.py:576
  74.9 9.1 %collective-permute-done.23.refs_0_ = bf16[32,2048]{1,0:T(8,128)(2,1)S(1)} collective-permute-done((bf16[32,2048]{1,0:T(8,128)(2,1)S(1)}, bf16[32,2048]{1,0:T(8,128)(2,1)S(1)}, u32[]{:S(2)}, u32[]{:S(2)}) %collective-permute-start.23) | collective-permute-done | bytes 131104 | tf_op jit(solution)/shard_map/ppermute | solution.py:576
  84.0 2.8 %collective-permute-done.24.refs_1_ = bf16[32,2048]{1,0:T(8,128)(2,1)S(1)} collective-permute-done((bf16[32,2048]{1,0:T(8,128)(2,1)S(1)}, bf16[32,2048]{1,0:T(8,128)(2,1)S(1)}, u32[]{:S(2)}, u32[]{:S(2)}) %collective-permute-start.24) | collective-permute-done | bytes 131104 | tf_op jit(solution)/shard_map/ppermute | solution.py:576
  88.2 2.4 %shard_map.158 = (f32[64,2048]{1,0:T(8,128)S(1)}, bf16[64,2048]{1,0:T(8,128)(2,1)S(1)}) custom-call(bf16[704,2048]{1,0:T(8,128)(2,1)S(1)} %get-tuple-element.122.gate, bf16[704,2048]{1,0:T(8,128)(2,1)S(1)} %get-tuple-element.123.widen, bf16[704,2048]{1,0:T(8,128)(2,1)S(1)} %get-tuple-element.124.down, bf16[32,2048]{1,0:T(8,128)(2,1)S(1)} %collective-permute-done.23.refs_0_, ...), custom_call_target="tpu_custom_call" | custom-call | flops 1200000000 | bytes 4000000 | tf_op jit(solution)/shard_map/pallas_call | solution.py:516
  101.5 3.1 %collective-permute-start.38 = (bf16[32,2048]{1,0:T(8,128)(2,1)S(1)}, bf16[32,2048]{1,0:T(8,128)(2,1)S(1)}, u32[]{:S(2)}, u32[]{:S(2)}) collective-permute-start(bf16[32,2048]{1,0:T(8,128)(2,1)S(1)} %get-tuple-element.147), channel_id=1, source_target_pairs={{0,24},{4,28},{8,16},{12,20},{16,8},{20,12},{24,0},{28,4},{1,25},{... | collective-permute-start | bytes 393224 | tf_op jit(solution)/shard_map/ppermute | solution.py:576
  106.2 2.6 %shard_map.160 = (f32[128,2048]{1,0:T(8,128)S(1)}, bf16[128,2048]{1,0:T(8,128)(2,1)S(1)}) custom-call(bf16[704,2048]{1,0:T(8,128)(2,1)S(1)} %get-tuple-element.122.gate, bf16[704,2048]{1,0:T(8,128)(2,1)S(1)} %get-tuple-element.123.widen, bf16[704,2048]{1,0:T(8,128)(2,1)S(1)} %get-tuple-element.124.down, bf16[32,2048]{1,0:T(8,128)(2,1)S(1)} %get-tuple-element.137.refs_0_, ...), custom_call_target="tpu_custom_call" | custom-call | flops 2400000000 | bytes 4000000 | tf_op jit(solution)/shard_map/pallas_call | solution.py:516
  108.9 3.5 %collective-permute-done.39.refs_1_ = bf16[32,2048]{1,0:T(8,128)(2,1)S(1)} collective-permute-done((bf16[32,2048]{1,0:T(8,128)(2,1)S(1)}, bf16[32,2048]{1,0:T(8,128)(2,1)S(1)}, u32[]{:S(2)}, u32[]{:S(2)}) %collective-permute-start.39) | collective-permute-done | bytes 131104 | tf_op jit(solution)/shard_map/ppermute | solution.py:576
  114.0 2.4 %shard_map.162 = (f32[64,2048]{1,0:T(8,128)S(1)}, bf16[64,2048]{1,0:T(8,128)(2,1)S(1)}) custom-call(bf16[704,2048]{1,0:T(8,128)(2,1)S(1)} %get-tuple-element.122.gate, bf16[704,2048]{1,0:T(8,128)(2,1)S(1)} %get-tuple-element.123.widen, bf16[704,2048]{1,0:T(8,128)(2,1)S(1)} %get-tuple-element.124.down, bf16[32,2048]{1,0:T(8,128)(2,1)S(1)} %collective-permute-done.38.refs_0_, ...), custom_call_target="tpu_custom_call" | custom-call | flops 1200000000 | bytes 4000000 | tf_op jit(solution)/shard_map/pallas_call | solution.py:516
  116.8 4.8 %collective-permute-start.36 = (bf16[32,2048]{1,0:T(8,128)(2,1)S(1)}, bf16[32,2048]{1,0:T(8,128)(2,1)S(1)}, u32[]{:S(2)}, u32[]{:S(2)}) collective-permute-start(bf16[32,2048]{1,0:T(8,128)(2,1)S(1)} %get-tuple-element.135), channel_id=1, source_target_pairs={{0,16},{4,20},{8,24},{12,28},{16,0},{20,4},{24,8},{28,12},{1,17},{... | collective-permute-start | bytes 393224 | tf_op jit(solution)/shard_map/ppermute | solution.py:576
  123.8 2.6 %collective-permute-start.44 = (bf16[32,2048]{1,0:T(8,128)(2,1)S(1)}, bf16[32,2048]{1,0:T(8,128)(2,1)S(1)}, u32[]{:S(2)}, u32[]{:S(2)}) collective-permute-start(bf16[32,2048]{1,0:T(8,128)(2,1)S(1)} %get-tuple-element.154), channel_id=1, source_target_pairs={{0,28},{4,24},{8,20},{12,16},{16,12},{20,8},{24,4},{28,0},{1,29},{... | collective-permute-start | bytes 393224 | tf_op jit(solution)/shard_map/ppermute | solution.py:576
  128.1 9.1 %collective-permute-done.36.refs_4_ = bf16[32,2048]{1,0:T(8,128)(2,1)S(1)} collective-permute-done((bf16[32,2048]{1,0:T(8,128)(2,1)S(1)}, bf16[32,2048]{1,0:T(8,128)(2,1)S(1)}, u32[]{:S(2)}, u32[]{:S(2)}) %collective-permute-start.36) | collective-permute-done | bytes 131104 | tf_op jit(solution)/shard_map/ppermute | solution.py:576
  137.2 3.7 %collective-permute-done.37.refs_5_ = bf16[32,2048]{1,0:T(8,128)(2,1)S(1)} collective-permute-done((bf16[32,2048]{1,0:T(8,128)(2,1)S(1)}, bf16[32,2048]{1,0:T(8,128)(2,1)S(1)}, u32[]{:S(2)}, u32[]{:S(2)}) %collective-permute-start.37) | collective-permute-done | bytes 131104 | tf_op jit(solution)/shard_map/ppermute | solution.py:576
  142.3 4.4 %collective-permute-done.35.refs_3_ = bf16[32,2048]{1,0:T(8,128)(2,1)S(1)} collective-permute-done((bf16[32,2048]{1,0:T(8,128)(2,1)S(1)}, bf16[32,2048]{1,0:T(8,128)(2,1)S(1)}, u32[]{:S(2)}, u32[]{:S(2)}) %collective-permute-start.35) | collective-permute-done | bytes 131104 | tf_op jit(solution)/shard_map/ppermute | solution.py:576
  151.2 6.8 %collective-permute-done.46 = bf16[64,2048]{1,0:T(8,128)(2,1)S(1)} collective-permute-done((bf16[64,2048]{1,0:T(8,128)(2,1)S(1)}, bf16[64,2048]{1,0:T(8,128)(2,1)S(1)}, u32[]{:S(2)}, u32[]{:S(2)}) %collective-permute-start.46) | collective-permute-done | bytes 262176 | tf_op jit(solution)/shard_map/ppermute | solution.py:576
  (134 shorter events, 57.9 us)
Async XLA Ops:
  3.9 12.0 %collective-permute-start = (bf16[136,512]{1,0:T(8,128)(2,1)}, bf16[136,512]{1,0:T(8,128)(2,1)S(1)}, u32[]{:S(2)}, u32[]{:S(2)}) collective-permute-start(bf16[136,512]{1,0:T(8,128)(2,1)} %get-tuple-element.86), channel_id=1, source_target_pairs={{0,4},{4,0},{8,12},{12,8},{16,20},{20,16},{24,28},{28,24},{1,5},{5... | collective-permute-start | bytes 417800 | tf_op jit(solution)/shard_map/ppermute | solution.py:576
  6.9 9.0 %collective-permute-start.1 = (bf16[136,512]{1,0:T(8,128)(2,1)}, bf16[136,512]{1,0:T(8,128)(2,1)S(1)}, u32[]{:S(2)}, u32[]{:S(2)}) collective-permute-start(bf16[136,512]{1,0:T(8,128)(2,1)} %get-tuple-element.87), channel_id=1, source_target_pairs={{0,8},{4,12},{8,0},{12,4},{16,24},{20,28},{24,16},{28,20},{1,9},{5... | collective-permute-start | bytes 417800 | tf_op jit(solution)/shard_map/ppermute | solution.py:576
  12.3 9.1 %collective-permute-start.7 = (bf16[136,512]{1,0:T(8,128)(2,1)}, bf16[136,512]{1,0:T(8,128)(2,1)S(1)}, u32[]{:S(2)}, u32[]{:S(2)}) collective-permute-start(bf16[136,512]{1,0:T(8,128)(2,1)} %get-tuple-element.95), channel_id=1, source_target_pairs={{0,4},{4,0},{8,12},{12,8},{16,20},{20,16},{24,28},{28,24},{1,5},{5... | collective-permute-start | bytes 417800 | tf_op jit(solution)/shard_map/ppermute | solution.py:576
  16.3 12.2 %collective-permute-start.3 = (bf16[128,512]{1,0:T(8,128)(2,1)S(1)}, bf16[128,512]{1,0:T(8,128)(2,1)S(1)}, u32[]{:S(2)}, u32[]{:S(2)}) collective-permute-start(bf16[128,512]{1,0:T(8,128)(2,1)S(1)} %quad_total.2), channel_id=1, source_target_pairs={{0,16},{4,20},{8,24},{12,28},{1,17},{5,21},{9,25},{13,29},{2,18},{... | collective-permute-start | bytes 393224 | tf_op jit(solution)/shard_map/ppermute | solution.py:264
  23.5 9.3 %collective-permute-start.10 = (bf16[128,512]{1,0:T(8,128)(2,1)S(1)}, bf16[128,512]{1,0:T(8,128)(2,1)S(1)}, u32[]{:S(2)}, u32[]{:S(2)}) collective-permute-start(bf16[128,512]{1,0:T(8,128)(2,1)S(1)} %quad_total.3), channel_id=1, source_target_pairs={{0,16},{4,20},{8,24},{12,28},{1,17},{5,21},{9,25},{13,29},{2,18},{... | collective-permute-start | bytes 393224 | tf_op jit(solution)/shard_map/ppermute | solution.py:264
  29.1 8.7 %collective-permute-start.4 = (bf16[128,512]{1,0:T(8,128)(2,1)S(1)}, bf16[128,512]{1,0:T(8,128)(2,1)S(1)}, u32[]{:S(2)}, u32[]{:S(2)}) collective-permute-start(bf16[128,512]{1,0:T(8,128)(2,1)S(1)} %get-tuple-element.90), channel_id=1, source_target_pairs={{0,4},{4,0},{8,12},{12,8},{16,20},{20,16},{24,28},{28,24},{1,5},{5... | collective-permute-start | bytes 393224 | tf_op jit(solution)/shard_map/ppermute | solution.py:576
  29.9 14.7 %collective-permute-start.5 = (bf16[128,512]{1,0:T(8,128)(2,1)S(1)}, bf16[128,512]{1,0:T(8,128)(2,1)S(1)}, u32[]{:S(2)}, u32[]{:S(2)}) collective-permute-start(bf16[128,512]{1,0:T(8,128)(2,1)S(1)} %get-tuple-element.91), channel_id=1, source_target_pairs={{0,8},{4,12},{8,0},{12,4},{16,24},{20,28},{24,16},{28,20},{1,9},{5... | collective-permute-start | bytes 393224 | tf_op jit(solution)/shard_map/ppermute | solution.py:576
  32.7 11.9 %collective-permute-start.6 = (bf16[128,512]{1,0:T(8,128)(2,1)S(1)}, bf16[128,512]{1,0:T(8,128)(2,1)S(1)}, u32[]{:S(2)}, u32[]{:S(2)}) collective-permute-start(bf16[128,512]{1,0:T(8,128)(2,1)S(1)} %get-tuple-element.92), channel_id=1, source_target_pairs={{0,12},{4,8},{8,4},{12,0},{16,28},{20,24},{24,20},{28,16},{1,13},{... | collective-permute-start | bytes 393224 | tf_op jit(solution)/shard_map/ppermute | solution.py:576
  34.3 10.4 %collective-permute-start.11 = (bf16[128,512]{1,0:T(8,128)(2,1)S(1)}, bf16[128,512]{1,0:T(8,128)(2,1)S(1)}, u32[]{:S(2)}, u32[]{:S(2)}) collective-permute-start(bf16[128,512]{1,0:T(8,128)(2,1)S(1)} %get-tuple-element.99), channel_id=1, source_target_pairs={{0,4},{4,0},{8,12},{12,8},{16,20},{20,16},{24,28},{28,24},{1,5},{5... | collective-permute-start | bytes 393224 | tf_op jit(solution)/shard_map/ppermute | solution.py:576
  35.8 8.9 %collective-permute-start.12 = (bf16[128,512]{1,0:T(8,128)(2,1)S(1)}, bf16[128,512]{1,0:T(8,128)(2,1)S(1)}, u32[]{:S(2)}, u32[]{:S(2)}) collective-permute-start(bf16[128,512]{1,0:T(8,128)(2,1)S(1)} %get-tuple-element.100), channel_id=1, source_target_pairs={{0,8},{4,12},{8,0},{12,4},{16,24},{20,28},{24,16},{28,20},{1,9},{5... | collective-permute-start | bytes 393224 | tf_op jit(solution)/shard_map/ppermute | solution.py:576
  49.8 9.2 %collective-permute-start.18 = (bf16[128,1024]{1,0:T(8,128)(2,1)S(1)}, bf16[128,1024]{1,0:T(8,128)(2,1)S(1)}, u32[]{:S(2)}, u32[]{:S(2)}) collective-permute-start(bf16[128,1024]{1,0:T(8,128)(2,1)S(1)} %add_convert_fusion), channel_id=1, source_target_pairs={{0,2},{1,3},{2,0},{3,1},{4,6},{5,7},{6,4},{7,5},{8,10},{9,11},{10,... | collective-permute-start | bytes 786440 | tf_op jit(solution)/shard_map/ppermute | solution.py:576
  51.4 13.2 %collective-permute-start.17 = (bf16[128,1024]{1,0:T(8,128)(2,1)S(1)}, bf16[128,1024]{1,0:T(8,128)(2,1)S(1)}, u32[]{:S(2)}, u32[]{:S(2)}) collective-permute-start(bf16[128,1024]{1,0:T(8,128)(2,1)S(1)} %add_convert_fusion.1), channel_id=1, source_target_pairs={{0,2},{1,3},{2,0},{3,1},{4,6},{5,7},{6,4},{7,5},{8,10},{9,11},{10,... | collective-permute-start | bytes 786440 | tf_op jit(solution)/shard_map/ppermute | solution.py:576
  52.0 17.4 %collective-permute-start.16 = (bf16[64,2048]{1,0:T(8,128)(2,1)S(1)}, bf16[64,2048]{1,0:T(8,128)(2,1)S(1)}, u32[]{:S(2)}, u32[]{:S(2)}) collective-permute-start(bf16[64,2048]{1,0:T(8,128)(2,1)S(1)} %copy-done.7), channel_id=1, source_target_pairs={{0,2},{1,3},{2,0},{3,1},{4,6},{5,7},{6,4},{7,5},{8,10},{9,11},{10,... | collective-permute-start | bytes 786440 | tf_op jit(solution)/shard_map/ppermute | solution.py:576
  72.5 11.5 %collective-permute-start.23 = (bf16[32,2048]{1,0:T(8,128)(2,1)S(1)}, bf16[32,2048]{1,0:T(8,128)(2,1)S(1)}, u32[]{:S(2)}, u32[]{:S(2)}) collective-permute-start(bf16[32,2048]{1,0:T(8,128)(2,1)S(1)} %get-tuple-element.131), channel_id=1, source_target_pairs={{0,16},{4,20},{8,24},{12,28},{16,0},{20,4},{24,8},{28,12},{1,17},{... | collective-permute-start | bytes 393224 | tf_op jit(solution)/shard_map/ppermute | solution.py:576
  73.8 13.0 %collective-permute-start.24 = (bf16[32,2048]{1,0:T(8,128)(2,1)S(1)}, bf16[32,2048]{1,0:T(8,128)(2,1)S(1)}, u32[]{:S(2)}, u32[]{:S(2)}) collective-permute-start(bf16[32,2048]{1,0:T(8,128)(2,1)S(1)} %get-tuple-element.132), channel_id=1, source_target_pairs={{0,20},{4,16},{8,28},{12,24},{16,4},{20,0},{24,12},{28,8},{1,21},{... | collective-permute-start | bytes 393224 | tf_op jit(solution)/shard_map/ppermute | solution.py:576
  92.2 8.3 %collective-permute-start.22 = (bf16[32,2048]{1,0:T(8,128)(2,1)S(1)}, bf16[32,2048]{1,0:T(8,128)(2,1)S(1)}, u32[]{:S(2)}, u32[]{:S(2)}) collective-permute-start(bf16[32,2048]{1,0:T(8,128)(2,1)S(1)} %get-tuple-element.130), channel_id=1, source_target_pairs={{0,12},{4,8},{8,4},{12,0},{16,28},{20,24},{24,20},{28,16},{1,13},{... | collective-permute-start | bytes 393224 | tf_op jit(solution)/shard_map/ppermute | solution.py:576
  104.6 7.8 %collective-permute-start.39 = (bf16[32,2048]{1,0:T(8,128)(2,1)S(1)}, bf16[32,2048]{1,0:T(8,128)(2,1)S(1)}, u32[]{:S(2)}, u32[]{:S(2)}) collective-permute-start(bf16[32,2048]{1,0:T(8,128)(2,1)S(1)} %get-tuple-element.148), channel_id=1, source_target_pairs={{0,28},{4,24},{8,20},{12,16},{16,12},{20,8},{24,4},{28,0},{1,29},{... | collective-permute-start | bytes 393224 | tf_op jit(solution)/shard_map/ppermute | solution.py:576
  108.9 17.6 %collective-permute-start.32 = (bf16[128,2048]{1,0:T(8,128)(2,1)S(1)}, bf16[128,2048]{1,0:T(8,128)(2,1)S(1)}, u32[]{:S(2)}, u32[]{:S(2)}) collective-permute-start(bf16[128,2048]{1,0:T(8,128)(2,1)S(1)} %get-tuple-element.142), channel_id=1, source_target_pairs={{0,1},{1,0},{2,3},{3,2},{4,5},{5,4},{6,7},{7,6},{8,9},{9,8},{10,11... | collective-permute-start | bytes 1572872 | tf_op jit(solution)/shard_map/ppermute | solution.py:576
  116.8 20.4 %collective-permute-start.36 = (bf16[32,2048]{1,0:T(8,128)(2,1)S(1)}, bf16[32,2048]{1,0:T(8,128)(2,1)S(1)}, u32[]{:S(2)}, u32[]{:S(2)}) collective-permute-start(bf16[32,2048]{1,0:T(8,128)(2,1)S(1)} %get-tuple-element.135), channel_id=1, source_target_pairs={{0,16},{4,20},{8,24},{12,28},{16,0},{20,4},{24,8},{28,12},{1,17},{... | collective-permute-start | bytes 393224 | tf_op jit(solution)/shard_map/ppermute | solution.py:576
  121.6 19.3 %collective-permute-start.37 = (bf16[32,2048]{1,0:T(8,128)(2,1)S(1)}, bf16[32,2048]{1,0:T(8,128)(2,1)S(1)}, u32[]{:S(2)}, u32[]{:S(2)}) collective-permute-start(bf16[32,2048]{1,0:T(8,128)(2,1)S(1)} %get-tuple-element.136), channel_id=1, source_target_pairs={{0,20},{4,16},{8,28},{12,24},{16,4},{20,0},{24,12},{28,8},{1,21},{... | collective-permute-start | bytes 393224 | tf_op jit(solution)/shard_map/ppermute | solution.py:576
  122.5 18.3 %collective-permute-start.43 = (bf16[32,2048]{1,0:T(8,128)(2,1)S(1)}, bf16[32,2048]{1,0:T(8,128)(2,1)S(1)}, u32[]{:S(2)}, u32[]{:S(2)}) collective-permute-start(bf16[32,2048]{1,0:T(8,128)(2,1)S(1)} %get-tuple-element.153), channel_id=1, source_target_pairs={{0,24},{4,28},{8,16},{12,20},{16,8},{20,12},{24,0},{28,4},{1,25},{... | collective-permute-start | bytes 393224 | tf_op jit(solution)/shard_map/ppermute | solution.py:576
  123.8 17.1 %collective-permute-start.44 = (bf16[32,2048]{1,0:T(8,128)(2,1)S(1)}, bf16[32,2048]{1,0:T(8,128)(2,1)S(1)}, u32[]{:S(2)}, u32[]{:S(2)}) collective-permute-start(bf16[32,2048]{1,0:T(8,128)(2,1)S(1)} %get-tuple-element.154), channel_id=1, source_target_pairs={{0,28},{4,24},{8,20},{12,16},{16,12},{20,8},{24,4},{28,0},{1,29},{... | collective-permute-start | bytes 393224 | tf_op jit(solution)/shard_map/ppermute | solution.py:576
  126.5 14.4 %collective-permute-start.33 = (bf16[32,2048]{1,0:T(8,128)(2,1)S(1)}, bf16[32,2048]{1,0:T(8,128)(2,1)S(1)}, u32[]{:S(2)}, u32[]{:S(2)}) collective-permute-start(bf16[32,2048]{1,0:T(8,128)(2,1)S(1)} %get-tuple-element.144), channel_id=1, source_target_pairs={{0,4},{4,0},{8,12},{12,8},{16,20},{20,16},{24,28},{28,24},{1,5},{5... | collective-permute-start | bytes 393224 | tf_op jit(solution)/shard_map/ppermute | solution.py:576
  149.6 8.4 %collective-permute-start.46 = (bf16[64,2048]{1,0:T(8,128)(2,1)S(1)}, bf16[64,2048]{1,0:T(8,128)(2,1)S(1)}, u32[]{:S(2)}, u32[]{:S(2)}) collective-permute-start(bf16[64,2048]{1,0:T(8,128)(2,1)S(1)} %slice.17), channel_id=1, source_target_pairs={{0,2},{1,3},{2,0},{3,1},{4,6},{5,7},{6,4},{7,5},{8,10},{9,11},{10,... | collective-permute-start | bytes 786440 | tf_op jit(solution)/shard_map/ppermute | solution.py:576
  (42 other events, 459.5 us)

commit v3 on v2

--- a/solution.py
+++ b/solution.py
@@ -555,21 +555,48 @@
     send[...] = total[split:, :].astype(BF16)
 
 
-def combine(n, high, low, pieces):
-    width = pieces[0].shape[1]
-    length = high.shape[0]
+def combine(n, side, high, low, pieces):
+    half, width = pieces[0].shape
+    length, slots = high.shape
+    cut = width // 2
+    table = pl.BlockSpec((length, slots), lambda i: (0, 0))
     return pl.pallas_call(
         functools.partial(combine_kernel, n),
-        in_specs=[VMEM] * (2 + n),
-        out_specs=[VMEM] * 2,
+        grid=(1,),
+        in_specs=[table] * 2 + [pl.BlockSpec((half, cut), lambda i: (0, side))] * n,
+        out_specs=[pl.BlockSpec((length // 2, cut), lambda i: (0, 0))] * 2,
         out_shape=[
-            jax.ShapeDtypeStruct((length // 2, width), F32),
-            jax.ShapeDtypeStruct((length // 2, width), BF16),
+            jax.ShapeDtypeStruct((length // 2, cut), F32),
+            jax.ShapeDtypeStruct((length // 2, cut), BF16),
         ],
         compiler_params=params(16),
-        cost_estimate=cost(1e9, 3e6),
-        name="combine",
+        cost_estimate=cost(5e8, 2e6),
     )(high, low, *pieces)
+
+
+def final_kernel(groups, mid, *refs):
+    keeps, received, parts, out = refs[:2], refs[2:4], refs[4:-1], refs[-1]
+    rows, width = mid.shape
+    cut = width // 2
+    for side in range(2):
+        columns = slice(side * cut, (side + 1) * cut)
+        total = mid[:, columns] + keeps[side][:rows, :] + received[side][:rows, :].astype(F32)
+        for k in range(groups - 1):
+            total = total + parts[side * (groups - 1) + k][...].astype(F32)
+        out[:, columns] = total.astype(BF16)
+
+
+def final(groups, mid, keeps, received, parts):
+    arrays = [*keeps, *received, *parts]
+    return pl.pallas_call(
+        functools.partial(final_kernel, groups),
+        in_specs=[VMEM] * (1 + len(arrays)),
+        out_specs=VMEM,
+        out_shape=jax.ShapeDtypeStruct(mid.shape, BF16),
+        compiler_params=params(16),
+        cost_estimate=cost(1e6, 2e6),
+        name="final",
+    )(mid, *arrays)
 
 
 def swap(value, axis, k):
@@ -673,13 +700,17 @@
         for k, piece in zip(ks, merged):
             back[k] = piece if k == 0 else swap(piece, "sp", k)
     back = [back[k] for k in range(n)]
-    keep, send = combine(n, high, low_part, back)
-    summed = keep + swap(send, "tp", 1).astype(F32)
-    total = mid + summed[:rows]
-    for k in range(1, groups):
-        part = summed[k * rows : (k + 1) * rows].astype(BF16)
-        total = total + swap(part, "tp", 2 * k).astype(F32)
-    return total.astype(BF16)
+    keeps, received, parts = [], [], []
+    for side in range(2):
+        keep, send = combine(n, side, high, low_part, back)
+        other = swap(send, "tp", 1)
+        for k in range(1, groups):
+            span = slice(k * rows, (k + 1) * rows)
+            part = (keep[span] + other[span].astype(F32)).astype(BF16)
+            parts.append(swap(part, "tp", 2 * k))
+        keeps.append(keep)
+        received.append(other)
+    return final(groups, mid, keeps, received, parts)
 
 
 def expert_chunks(n):

time: 159 us -> 158 us (level)
  waiting for transfers between devices: 69.3 us -> 67.2 us
    ppermute x45 -> x47, waiting for transfers between devices: 69.3 us -> 67.2 us  [swap(): return lax.ppermute(value, axis, xor_perm(axis, k))]
    ppermute x45 -> x47, starting transfers between devices: 46.9 us -> 48 us  [swap(): return lax.ppermute(value, axis, xor_perm(axis, k))]
  transfers between devices with their start and end apart: 47 -> 49, of which waited for: 21 -> 22; matrix products, arithmetic and copies ran while one was open for 0% -> 0% of each run, Pallas kernels for 11% -> 11%
where the time goes in v3:
time: 158 us
  waiting for transfers between devices  67.2 us (43%)
  starting transfers between devices  58.2 us (37%)
  Pallas kernels  30 us (19%)
  local copies, waits for them, and re-layouts  1.92 us (1%)
    ppermute x47, waiting for transfers between devices, swap(): return lax.ppermute(value, axis, xor_perm(axis, k))  67.2 us
    ppermute x47, starting transfers between devices, swap(): return lax.ppermute(value, axis, xor_perm(axis, k))  48 us
    ppermute x2, starting transfers between devices, quad_entry(): start = lax.ppermute(total, 'sp', perm)  10.2 us
    pallas_call x2, Pallas kernels, device_states(): pl.pallas_call(functools.partial(state_kernel, first, count), in_specs=[V...  7.61 us
    pallas_call x3, Pallas kernels, expert(): pl.pallas_call(functools.partial(expert_kernel, count), in_specs=[VMEM] *...  7.35 us
    pallas_call x2, Pallas kernels, local_attention(): pl.pallas_call(functools.partial(local_kernel, first, count), grid=(1,),...  5.11 us
  transfers between devices with their start and end apart: 49, of which 22 were waited for; matrix products, arithmetic and copies ran while one was open for 0% of the time, Pallas kernels for 11%

profile of v3, /device:TPU:0, one launch (start us, length us, event | category | flops | bytes accessed | tf_op | source)
XLA Modules:
  0.0 158.1 jit_solution(10333617310023084348)
XLA Ops:
  0.0 3.8 %shard_map.156 = (bf16[136,512]{1,0:T(8,128)(2,1)}, bf16[136,512]{1,0:T(8,128)(2,1)}, bf16[136,512]{1,0:T(8,128)(2,1)}, bf16[136,512]{1,0:T(8,128)(2,1)}) custom-call(bf16[16,256]{1,0:T(8,128)(2,1)} %bitcast.19, bf16[16,1024]{1,0:T(8,128)(2,1)} %matrix.9, f32[1,1024]{1,0:T(1,128)} %bitcast.23, f32[4,256]{1,0:T(4,128)} %bitcast.27, ...), custom_call_target="tpu_custom_call" | custom-call | flops 800000000 | bytes 1000000 | tf_op jit(solution)/shard_map/pallas_call | solution.py:115
  3.9 3.0 %collective-permute-start = (bf16[136,512]{1,0:T(8,128)(2,1)}, bf16[136,512]{1,0:T(8,128)(2,1)S(1)}, u32[]{:S(2)}, u32[]{:S(2)}) collective-permute-start(bf16[136,512]{1,0:T(8,128)(2,1)} %get-tuple-element.88), channel_id=1, source_target_pairs={{0,4},{4,0},{8,12},{12,8},{16,20},{20,16},{24,28},{28,24},{1,5},{5... | collective-permute-start | bytes 417800 | tf_op jit(solution)/shard_map/ppermute | solution.py:603
  8.5 3.8 %shard_map.157 = (bf16[136,512]{1,0:T(8,128)(2,1)}, bf16[136,512]{1,0:T(8,128)(2,1)}, bf16[136,512]{1,0:T(8,128)(2,1)}, bf16[136,512]{1,0:T(8,128)(2,1)}) custom-call(bf16[16,256]{1,0:T(8,128)(2,1)} %bitcast.20, bf16[16,1024]{1,0:T(8,128)(2,1)} %matrix.9, f32[1,1024]{1,0:T(1,128)} %bitcast.24, f32[4,256]{1,0:T(4,128)} %bitcast.28, ...), custom_call_target="tpu_custom_call" | custom-call | flops 800000000 | bytes 1000000 | tf_op jit(solution)/shard_map/pallas_call | solution.py:115
  16.3 5.2 %collective-permute-start.3 = (bf16[128,512]{1,0:T(8,128)(2,1)S(1)}, bf16[128,512]{1,0:T(8,128)(2,1)S(1)}, u32[]{:S(2)}, u32[]{:S(2)}) collective-permute-start(bf16[128,512]{1,0:T(8,128)(2,1)S(1)} %quad_total.2), channel_id=1, source_target_pairs={{0,16},{4,20},{8,24},{12,28},{1,17},{5,21},{9,25},{13,29},{2,18},{... | collective-permute-start | bytes 393224 | tf_op jit(solution)/shard_map/ppermute | solution.py:264
  23.5 5.0 %collective-permute-start.10 = (bf16[128,512]{1,0:T(8,128)(2,1)S(1)}, bf16[128,512]{1,0:T(8,128)(2,1)S(1)}, u32[]{:S(2)}, u32[]{:S(2)}) collective-permute-start(bf16[128,512]{1,0:T(8,128)(2,1)S(1)} %quad_total.3), channel_id=1, source_target_pairs={{0,16},{4,20},{8,24},{12,28},{1,17},{5,21},{9,25},{13,29},{2,18},{... | collective-permute-start | bytes 393224 | tf_op jit(solution)/shard_map/ppermute | solution.py:264
  29.9 2.8 %collective-permute-start.5 = (bf16[128,512]{1,0:T(8,128)(2,1)S(1)}, bf16[128,512]{1,0:T(8,128)(2,1)S(1)}, u32[]{:S(2)}, u32[]{:S(2)}) collective-permute-start(bf16[128,512]{1,0:T(8,128)(2,1)S(1)} %get-tuple-element.93), channel_id=1, source_target_pairs={{0,8},{4,12},{8,0},{12,4},{16,24},{20,28},{24,16},{28,20},{1,9},{5... | collective-permute-start | bytes 393224 | tf_op jit(solution)/shard_map/ppermute | solution.py:603
  39.5 2.6 %shard_map.155 = (f32[256,1024]{1,0:T(8,128)S(1)}, bf16[256,512]{1,0:T(8,128)(2,1)S(1)}) custom-call(bf16[16,256]{1,0:T(8,128)(2,1)S(1)} %bitcast.21, bf16[16,1024]{1,0:T(8,128)(2,1)S(1)} %copy-done.13, f32[1,1024]{1,0:T(1,128)S(1)} %bitcast.25, f32[4,256]{1,0:T(4,128)S(1)} %bitcast.29, bf16[256,1024]{1,0:T(8,128)(2,1)S(1)} %copy-done.11, ...), custom_call_target="tpu_custom_call" | custom-call | flops 800000000 | bytes 2400000 | tf_op jit(solution)/shard_map/pallas_call | solution.py:176
  42.1 2.6 %shard_map.154 = (f32[256,1024]{1,0:T(8,128)S(1)}, bf16[256,512]{1,0:T(8,128)(2,1)S(1)}) custom-call(bf16[16,256]{1,0:T(8,128)(2,1)S(1)} %bitcast.22, bf16[16,1024]{1,0:T(8,128)(2,1)S(1)} %copy-done.13, f32[1,1024]{1,0:T(1,128)S(1)} %bitcast.26, f32[4,256]{1,0:T(4,128)S(1)} %bitcast.30, bf16[256,1024]{1,0:T(8,128)(2,1)S(1)} %copy-done.11, ...), custom_call_target="tpu_custom_call" | custom-call | flops 800000000 | bytes 2400000 | tf_op jit(solution)/shard_map/pallas_call | solution.py:176
  55.3 3.7 %collective-permute-done.18.refs_7_ = bf16[128,1024]{1,0:T(8,128)(2,1)S(1)} collective-permute-done((bf16[128,1024]{1,0:T(8,128)(2,1)S(1)}, bf16[128,1024]{1,0:T(8,128)(2,1)S(1)}, u32[]{:S(2)}, u32[]{:S(2)}) %collective-permute-start.18) | collective-permute-done | bytes 262176 | tf_op jit(solution)/shard_map/ppermute | solution.py:603
  59.0 5.6 %collective-permute-done.17.refs_6_ = bf16[128,1024]{1,0:T(8,128)(2,1)S(1)} collective-permute-done((bf16[128,1024]{1,0:T(8,128)(2,1)S(1)}, bf16[128,1024]{1,0:T(8,128)(2,1)S(1)}, u32[]{:S(2)}, u32[]{:S(2)}) %collective-permute-start.17) | collective-permute-done | bytes 262176 | tf_op jit(solution)/shard_map/ppermute | solution.py:603
  64.6 4.8 %collective-permute-done.16.refs_5_ = bf16[64,2048]{1,0:T(8,128)(2,1)S(1)} collective-permute-done((bf16[64,2048]{1,0:T(8,128)(2,1)S(1)}, bf16[64,2048]{1,0:T(8,128)(2,1)S(1)}, u32[]{:S(2)}, u32[]{:S(2)}) %collective-permute-start.16) | collective-permute-done | bytes 262176 | tf_op jit(solution)/shard_map/ppermute | solution.py:603
  74.9 9.1 %collective-permute-done.23.refs_0_ = bf16[32,2048]{1,0:T(8,128)(2,1)S(1)} collective-permute-done((bf16[32,2048]{1,0:T(8,128)(2,1)S(1)}, bf16[32,2048]{1,0:T(8,128)(2,1)S(1)}, u32[]{:S(2)}, u32[]{:S(2)}) %collective-permute-start.23) | collective-permute-done | bytes 131104 | tf_op jit(solution)/shard_map/ppermute | solution.py:603
  84.0 2.8 %collective-permute-done.24.refs_1_ = bf16[32,2048]{1,0:T(8,128)(2,1)S(1)} collective-permute-done((bf16[32,2048]{1,0:T(8,128)(2,1)S(1)}, bf16[32,2048]{1,0:T(8,128)(2,1)S(1)}, u32[]{:S(2)}, u32[]{:S(2)}) %collective-permute-start.24) | collective-permute-done | bytes 131104 | tf_op jit(solution)/shard_map/ppermute | solution.py:603
  88.2 2.4 %shard_map.158 = (f32[64,2048]{1,0:T(8,128)S(1)}, bf16[64,2048]{1,0:T(8,128)(2,1)S(1)}) custom-call(bf16[704,2048]{1,0:T(8,128)(2,1)S(1)} %get-tuple-element.124.gate, bf16[704,2048]{1,0:T(8,128)(2,1)S(1)} %get-tuple-element.125.widen, bf16[704,2048]{1,0:T(8,128)(2,1)S(1)} %get-tuple-element.126.down, bf16[32,2048]{1,0:T(8,128)(2,1)S(1)} %collective-permute-done.23.refs_0_, ...), custom_call_target="tpu_custom_call" | custom-call | flops 1200000000 | bytes 4000000 | tf_op jit(solution)/shard_map/pallas_call | solution.py:516
  101.5 3.1 %collective-permute-start.38 = (bf16[32,2048]{1,0:T(8,128)(2,1)S(1)}, bf16[32,2048]{1,0:T(8,128)(2,1)S(1)}, u32[]{:S(2)}, u32[]{:S(2)}) collective-permute-start(bf16[32,2048]{1,0:T(8,128)(2,1)S(1)} %get-tuple-element.149), channel_id=1, source_target_pairs={{0,24},{4,28},{8,16},{12,20},{16,8},{20,12},{24,0},{28,4},{1,25},{... | collective-permute-start | bytes 393224 | tf_op jit(solution)/shard_map/ppermute | solution.py:603
  106.2 2.6 %shard_map.160 = (f32[128,2048]{1,0:T(8,128)S(1)}, bf16[128,2048]{1,0:T(8,128)(2,1)S(1)}) custom-call(bf16[704,2048]{1,0:T(8,128)(2,1)S(1)} %get-tuple-element.124.gate, bf16[704,2048]{1,0:T(8,128)(2,1)S(1)} %get-tuple-element.125.widen, bf16[704,2048]{1,0:T(8,128)(2,1)S(1)} %get-tuple-element.126.down, bf16[32,2048]{1,0:T(8,128)(2,1)S(1)} %get-tuple-element.139.refs_0_, ...), custom_call_target="tpu_custom_call" | custom-call | flops 2400000000 | bytes 4000000 | tf_op jit(solution)/shard_map/pallas_call | solution.py:516
  108.9 3.5 %collective-permute-done.39.refs_1_ = bf16[32,2048]{1,0:T(8,128)(2,1)S(1)} collective-permute-done((bf16[32,2048]{1,0:T(8,128)(2,1)S(1)}, bf16[32,2048]{1,0:T(8,128)(2,1)S(1)}, u32[]{:S(2)}, u32[]{:S(2)}) %collective-permute-start.39) | collective-permute-done | bytes 131104 | tf_op jit(solution)/shard_map/ppermute | solution.py:603
  114.0 2.4 %shard_map.162 = (f32[64,2048]{1,0:T(8,128)S(1)}, bf16[64,2048]{1,0:T(8,128)(2,1)S(1)}) custom-call(bf16[704,2048]{1,0:T(8,128)(2,1)S(1)} %get-tuple-element.124.gate, bf16[704,2048]{1,0:T(8,128)(2,1)S(1)} %get-tuple-element.125.widen, bf16[704,2048]{1,0:T(8,128)(2,1)S(1)} %get-tuple-element.126.down, bf16[32,2048]{1,0:T(8,128)(2,1)S(1)} %collective-permute-done.38.refs_0_, ...), custom_call_target="tpu_custom_call" | custom-call | flops 1200000000 | bytes 4000000 | tf_op jit(solution)/shard_map/pallas_call | solution.py:516
  116.8 4.8 %collective-permute-start.36 = (bf16[32,2048]{1,0:T(8,128)(2,1)S(1)}, bf16[32,2048]{1,0:T(8,128)(2,1)S(1)}, u32[]{:S(2)}, u32[]{:S(2)}) collective-permute-start(bf16[32,2048]{1,0:T(8,128)(2,1)S(1)} %get-tuple-element.137), channel_id=1, source_target_pairs={{0,16},{4,20},{8,24},{12,28},{16,0},{20,4},{24,8},{28,12},{1,17},{... | collective-permute-start | bytes 393224 | tf_op jit(solution)/shard_map/ppermute | solution.py:603
  123.8 2.6 %collective-permute-start.44 = (bf16[32,2048]{1,0:T(8,128)(2,1)S(1)}, bf16[32,2048]{1,0:T(8,128)(2,1)S(1)}, u32[]{:S(2)}, u32[]{:S(2)}) collective-permute-start(bf16[32,2048]{1,0:T(8,128)(2,1)S(1)} %get-tuple-element.156), channel_id=1, source_target_pairs={{0,28},{4,24},{8,20},{12,16},{16,12},{20,8},{24,4},{28,0},{1,29},{... | collective-permute-start | bytes 393224 | tf_op jit(solution)/shard_map/ppermute | solution.py:603
  128.1 9.1 %collective-permute-done.36.refs_4_ = bf16[32,2048]{1,0:T(8,128)(2,1)S(1)} collective-permute-done((bf16[32,2048]{1,0:T(8,128)(2,1)S(1)}, bf16[32,2048]{1,0:T(8,128)(2,1)S(1)}, u32[]{:S(2)}, u32[]{:S(2)}) %collective-permute-start.36) | collective-permute-done | bytes 131104 | tf_op jit(solution)/shard_map/ppermute | solution.py:603
  137.2 3.7 %collective-permute-done.37.refs_5_ = bf16[32,2048]{1,0:T(8,128)(2,1)S(1)} collective-permute-done((bf16[32,2048]{1,0:T(8,128)(2,1)S(1)}, bf16[32,2048]{1,0:T(8,128)(2,1)S(1)}, u32[]{:S(2)}, u32[]{:S(2)}) %collective-permute-start.37) | collective-permute-done | bytes 131104 | tf_op jit(solution)/shard_map/ppermute | solution.py:603
  142.3 4.4 %collective-permute-done.35.refs_3_ = bf16[32,2048]{1,0:T(8,128)(2,1)S(1)} collective-permute-done((bf16[32,2048]{1,0:T(8,128)(2,1)S(1)}, bf16[32,2048]{1,0:T(8,128)(2,1)S(1)}, u32[]{:S(2)}, u32[]{:S(2)}) %collective-permute-start.35) | collective-permute-done | bytes 131104 | tf_op jit(solution)/shard_map/ppermute | solution.py:603
  151.1 4.2 %collective-permute-done.48.refs_5_ = bf16[64,1024]{1,0:T(8,128)(2,1)S(1)} collective-permute-done((bf16[64,1024]{1,0:T(8,128)(2,1)S(1)}, bf16[64,1024]{1,0:T(8,128)(2,1)S(1)}, u32[]{:S(2)}, u32[]{:S(2)}) %collective-permute-start.48) | collective-permute-done | bytes 131104 | tf_op jit(solution)/shard_map/ppermute | solution.py:603
  (139 shorter events, 59.8 us)
Async XLA Ops:
  3.9 12.0 %collective-permute-start = (bf16[136,512]{1,0:T(8,128)(2,1)}, bf16[136,512]{1,0:T(8,128)(2,1)S(1)}, u32[]{:S(2)}, u32[]{:S(2)}) collective-permute-start(bf16[136,512]{1,0:T(8,128)(2,1)} %get-tuple-element.88), channel_id=1, source_target_pairs={{0,4},{4,0},{8,12},{12,8},{16,20},{20,16},{24,28},{28,24},{1,5},{5... | collective-permute-start | bytes 417800 | tf_op jit(solution)/shard_map/ppermute | solution.py:603
  6.9 9.0 %collective-permute-start.1 = (bf16[136,512]{1,0:T(8,128)(2,1)}, bf16[136,512]{1,0:T(8,128)(2,1)S(1)}, u32[]{:S(2)}, u32[]{:S(2)}) collective-permute-start(bf16[136,512]{1,0:T(8,128)(2,1)} %get-tuple-element.89), channel_id=1, source_target_pairs={{0,8},{4,12},{8,0},{12,4},{16,24},{20,28},{24,16},{28,20},{1,9},{5... | collective-permute-start | bytes 417800 | tf_op jit(solution)/shard_map/ppermute | solution.py:603
  12.3 9.1 %collective-permute-start.7 = (bf16[136,512]{1,0:T(8,128)(2,1)}, bf16[136,512]{1,0:T(8,128)(2,1)S(1)}, u32[]{:S(2)}, u32[]{:S(2)}) collective-permute-start(bf16[136,512]{1,0:T(8,128)(2,1)} %get-tuple-element.97), channel_id=1, source_target_pairs={{0,4},{4,0},{8,12},{12,8},{16,20},{20,16},{24,28},{28,24},{1,5},{5... | collective-permute-start | bytes 417800 | tf_op jit(solution)/shard_map/ppermute | solution.py:603
  16.3 12.2 %collective-permute-start.3 = (bf16[128,512]{1,0:T(8,128)(2,1)S(1)}, bf16[128,512]{1,0:T(8,128)(2,1)S(1)}, u32[]{:S(2)}, u32[]{:S(2)}) collective-permute-start(bf16[128,512]{1,0:T(8,128)(2,1)S(1)} %quad_total.2), channel_id=1, source_target_pairs={{0,16},{4,20},{8,24},{12,28},{1,17},{5,21},{9,25},{13,29},{2,18},{... | collective-permute-start | bytes 393224 | tf_op jit(solution)/shard_map/ppermute | solution.py:264
  23.5 9.3 %collective-permute-start.10 = (bf16[128,512]{1,0:T(8,128)(2,1)S(1)}, bf16[128,512]{1,0:T(8,128)(2,1)S(1)}, u32[]{:S(2)}, u32[]{:S(2)}) collective-permute-start(bf16[128,512]{1,0:T(8,128)(2,1)S(1)} %quad_total.3), channel_id=1, source_target_pairs={{0,16},{4,20},{8,24},{12,28},{1,17},{5,21},{9,25},{13,29},{2,18},{... | collective-permute-start | bytes 393224 | tf_op jit(solution)/shard_map/ppermute | solution.py:264
  29.1 8.7 %collective-permute-start.4 = (bf16[128,512]{1,0:T(8,128)(2,1)S(1)}, bf16[128,512]{1,0:T(8,128)(2,1)S(1)}, u32[]{:S(2)}, u32[]{:S(2)}) collective-permute-start(bf16[128,512]{1,0:T(8,128)(2,1)S(1)} %get-tuple-element.92), channel_id=1, source_target_pairs={{0,4},{4,0},{8,12},{12,8},{16,20},{20,16},{24,28},{28,24},{1,5},{5... | collective-permute-start | bytes 393224 | tf_op jit(solution)/shard_map/ppermute | solution.py:603
  29.9 14.7 %collective-permute-start.5 = (bf16[128,512]{1,0:T(8,128)(2,1)S(1)}, bf16[128,512]{1,0:T(8,128)(2,1)S(1)}, u32[]{:S(2)}, u32[]{:S(2)}) collective-permute-start(bf16[128,512]{1,0:T(8,128)(2,1)S(1)} %get-tuple-element.93), channel_id=1, source_target_pairs={{0,8},{4,12},{8,0},{12,4},{16,24},{20,28},{24,16},{28,20},{1,9},{5... | collective-permute-start | bytes 393224 | tf_op jit(solution)/shard_map/ppermute | solution.py:603
  32.7 11.9 %collective-permute-start.6 = (bf16[128,512]{1,0:T(8,128)(2,1)S(1)}, bf16[128,512]{1,0:T(8,128)(2,1)S(1)}, u32[]{:S(2)}, u32[]{:S(2)}) collective-permute-start(bf16[128,512]{1,0:T(8,128)(2,1)S(1)} %get-tuple-element.94), channel_id=1, source_target_pairs={{0,12},{4,8},{8,4},{12,0},{16,28},{20,24},{24,20},{28,16},{1,13},{... | collective-permute-start | bytes 393224 | tf_op jit(solution)/shard_map/ppermute | solution.py:603
  34.3 10.4 %collective-permute-start.11 = (bf16[128,512]{1,0:T(8,128)(2,1)S(1)}, bf16[128,512]{1,0:T(8,128)(2,1)S(1)}, u32[]{:S(2)}, u32[]{:S(2)}) collective-permute-start(bf16[128,512]{1,0:T(8,128)(2,1)S(1)} %get-tuple-element.101), channel_id=1, source_target_pairs={{0,4},{4,0},{8,12},{12,8},{16,20},{20,16},{24,28},{28,24},{1,5},{5... | collective-permute-start | bytes 393224 | tf_op jit(solution)/shard_map/ppermute | solution.py:603
  35.8 8.9 %collective-permute-start.12 = (bf16[128,512]{1,0:T(8,128)(2,1)S(1)}, bf16[128,512]{1,0:T(8,128)(2,1)S(1)}, u32[]{:S(2)}, u32[]{:S(2)}) collective-permute-start(bf16[128,512]{1,0:T(8,128)(2,1)S(1)} %get-tuple-element.102), channel_id=1, source_target_pairs={{0,8},{4,12},{8,0},{12,4},{16,24},{20,28},{24,16},{28,20},{1,9},{5... | collective-permute-start | bytes 393224 | tf_op jit(solution)/shard_map/ppermute | solution.py:603
  49.8 9.2 %collective-permute-start.18 = (bf16[128,1024]{1,0:T(8,128)(2,1)S(1)}, bf16[128,1024]{1,0:T(8,128)(2,1)S(1)}, u32[]{:S(2)}, u32[]{:S(2)}) collective-permute-start(bf16[128,1024]{1,0:T(8,128)(2,1)S(1)} %add_convert_fusion), channel_id=1, source_target_pairs={{0,2},{1,3},{2,0},{3,1},{4,6},{5,7},{6,4},{7,5},{8,10},{9,11},{10,... | collective-permute-start | bytes 786440 | tf_op jit(solution)/shard_map/ppermute | solution.py:603
  51.4 13.2 %collective-permute-start.17 = (bf16[128,1024]{1,0:T(8,128)(2,1)S(1)}, bf16[128,1024]{1,0:T(8,128)(2,1)S(1)}, u32[]{:S(2)}, u32[]{:S(2)}) collective-permute-start(bf16[128,1024]{1,0:T(8,128)(2,1)S(1)} %add_convert_fusion.1), channel_id=1, source_target_pairs={{0,2},{1,3},{2,0},{3,1},{4,6},{5,7},{6,4},{7,5},{8,10},{9,11},{10,... | collective-permute-start | bytes 786440 | tf_op jit(solution)/shard_map/ppermute | solution.py:603
  52.0 17.4 %collective-permute-start.16 = (bf16[64,2048]{1,0:T(8,128)(2,1)S(1)}, bf16[64,2048]{1,0:T(8,128)(2,1)S(1)}, u32[]{:S(2)}, u32[]{:S(2)}) collective-permute-start(bf16[64,2048]{1,0:T(8,128)(2,1)S(1)} %copy-done.7), channel_id=1, source_target_pairs={{0,2},{1,3},{2,0},{3,1},{4,6},{5,7},{6,4},{7,5},{8,10},{9,11},{10,... | collective-permute-start | bytes 786440 | tf_op jit(solution)/shard_map/ppermute | solution.py:603
  72.5 11.5 %collective-permute-start.23 = (bf16[32,2048]{1,0:T(8,128)(2,1)S(1)}, bf16[32,2048]{1,0:T(8,128)(2,1)S(1)}, u32[]{:S(2)}, u32[]{:S(2)}) collective-permute-start(bf16[32,2048]{1,0:T(8,128)(2,1)S(1)} %get-tuple-element.133), channel_id=1, source_target_pairs={{0,16},{4,20},{8,24},{12,28},{16,0},{20,4},{24,8},{28,12},{1,17},{... | collective-permute-start | bytes 393224 | tf_op jit(solution)/shard_map/ppermute | solution.py:603
  73.8 13.0 %collective-permute-start.24 = (bf16[32,2048]{1,0:T(8,128)(2,1)S(1)}, bf16[32,2048]{1,0:T(8,128)(2,1)S(1)}, u32[]{:S(2)}, u32[]{:S(2)}) collective-permute-start(bf16[32,2048]{1,0:T(8,128)(2,1)S(1)} %get-tuple-element.134), channel_id=1, source_target_pairs={{0,20},{4,16},{8,28},{12,24},{16,4},{20,0},{24,12},{28,8},{1,21},{... | collective-permute-start | bytes 393224 | tf_op jit(solution)/shard_map/ppermute | solution.py:603
  92.2 8.4 %collective-permute-start.22 = (bf16[32,2048]{1,0:T(8,128)(2,1)S(1)}, bf16[32,2048]{1,0:T(8,128)(2,1)S(1)}, u32[]{:S(2)}, u32[]{:S(2)}) collective-permute-start(bf16[32,2048]{1,0:T(8,128)(2,1)S(1)} %get-tuple-element.132), channel_id=1, source_target_pairs={{0,12},{4,8},{8,4},{12,0},{16,28},{20,24},{24,20},{28,16},{1,13},{... | collective-permute-start | bytes 393224 | tf_op jit(solution)/shard_map/ppermute | solution.py:603
  101.5 7.4 %collective-permute-start.38 = (bf16[32,2048]{1,0:T(8,128)(2,1)S(1)}, bf16[32,2048]{1,0:T(8,128)(2,1)S(1)}, u32[]{:S(2)}, u32[]{:S(2)}) collective-permute-start(bf16[32,2048]{1,0:T(8,128)(2,1)S(1)} %get-tuple-element.149), channel_id=1, source_target_pairs={{0,24},{4,28},{8,16},{12,20},{16,8},{20,12},{24,0},{28,4},{1,25},{... | collective-permute-start | bytes 393224 | tf_op jit(solution)/shard_map/ppermute | solution.py:603
  104.6 7.8 %collective-permute-start.39 = (bf16[32,2048]{1,0:T(8,128)(2,1)S(1)}, bf16[32,2048]{1,0:T(8,128)(2,1)S(1)}, u32[]{:S(2)}, u32[]{:S(2)}) collective-permute-start(bf16[32,2048]{1,0:T(8,128)(2,1)S(1)} %get-tuple-element.150), channel_id=1, source_target_pairs={{0,28},{4,24},{8,20},{12,16},{16,12},{20,8},{24,4},{28,0},{1,29},{... | collective-permute-start | bytes 393224 | tf_op jit(solution)/shard_map/ppermute | solution.py:603
  108.9 17.6 %collective-permute-start.32 = (bf16[128,2048]{1,0:T(8,128)(2,1)S(1)}, bf16[128,2048]{1,0:T(8,128)(2,1)S(1)}, u32[]{:S(2)}, u32[]{:S(2)}) collective-permute-start(bf16[128,2048]{1,0:T(8,128)(2,1)S(1)} %get-tuple-element.144), channel_id=1, source_target_pairs={{0,1},{1,0},{2,3},{3,2},{4,5},{5,4},{6,7},{7,6},{8,9},{9,8},{10,11... | collective-permute-start | bytes 1572872 | tf_op jit(solution)/shard_map/ppermute | solution.py:603
  116.8 20.4 %collective-permute-start.36 = (bf16[32,2048]{1,0:T(8,128)(2,1)S(1)}, bf16[32,2048]{1,0:T(8,128)(2,1)S(1)}, u32[]{:S(2)}, u32[]{:S(2)}) collective-permute-start(bf16[32,2048]{1,0:T(8,128)(2,1)S(1)} %get-tuple-element.137), channel_id=1, source_target_pairs={{0,16},{4,20},{8,24},{12,28},{16,0},{20,4},{24,8},{28,12},{1,17},{... | collective-permute-start | bytes 393224 | tf_op jit(solution)/shard_map/ppermute | solution.py:603
  121.6 19.3 %collective-permute-start.37 = (bf16[32,2048]{1,0:T(8,128)(2,1)S(1)}, bf16[32,2048]{1,0:T(8,128)(2,1)S(1)}, u32[]{:S(2)}, u32[]{:S(2)}) collective-permute-start(bf16[32,2048]{1,0:T(8,128)(2,1)S(1)} %get-tuple-element.138), channel_id=1, source_target_pairs={{0,20},{4,16},{8,28},{12,24},{16,4},{20,0},{24,12},{28,8},{1,21},{... | collective-permute-start | bytes 393224 | tf_op jit(solution)/shard_map/ppermute | solution.py:603
  122.5 18.3 %collective-permute-start.43 = (bf16[32,2048]{1,0:T(8,128)(2,1)S(1)}, bf16[32,2048]{1,0:T(8,128)(2,1)S(1)}, u32[]{:S(2)}, u32[]{:S(2)}) collective-permute-start(bf16[32,2048]{1,0:T(8,128)(2,1)S(1)} %get-tuple-element.155), channel_id=1, source_target_pairs={{0,24},{4,28},{8,16},{12,20},{16,8},{20,12},{24,0},{28,4},{1,25},{... | collective-permute-start | bytes 393224 | tf_op jit(solution)/shard_map/ppermute | solution.py:603
  123.8 17.1 %collective-permute-start.44 = (bf16[32,2048]{1,0:T(8,128)(2,1)S(1)}, bf16[32,2048]{1,0:T(8,128)(2,1)S(1)}, u32[]{:S(2)}, u32[]{:S(2)}) collective-permute-start(bf16[32,2048]{1,0:T(8,128)(2,1)S(1)} %get-tuple-element.156), channel_id=1, source_target_pairs={{0,28},{4,24},{8,20},{12,16},{16,12},{20,8},{24,4},{28,0},{1,29},{... | collective-permute-start | bytes 393224 | tf_op jit(solution)/shard_map/ppermute | solution.py:603
  126.5 14.4 %collective-permute-start.33 = (bf16[32,2048]{1,0:T(8,128)(2,1)S(1)}, bf16[32,2048]{1,0:T(8,128)(2,1)S(1)}, u32[]{:S(2)}, u32[]{:S(2)}) collective-permute-start(bf16[32,2048]{1,0:T(8,128)(2,1)S(1)} %get-tuple-element.146), channel_id=1, source_target_pairs={{0,4},{4,0},{8,12},{12,8},{16,20},{20,16},{24,28},{28,24},{1,5},{5... | collective-permute-start | bytes 393224 | tf_op jit(solution)/shard_map/ppermute | solution.py:603
  (44 other events, 467.6 us)

commit v4 on v3

--- a/solution.py
+++ b/solution.py
@@ -69,39 +69,24 @@
 
 
 def state_kernel(first, count, low, matrix, bias, shift, key_rows, values, *rest):
-    outs = rest[:QUAD]
-    keys, vals, state, decays, sems = rest[QUAD:]
+    outs, (state, decays) = rest[:QUAD], rest[QUAD:]
     length = low.shape[1]
     piece = HK // QUAD
-    copies = []
-    for h in range(count):
-        at = first + h
-        pair = (
-            pltpu.make_async_copy(
-                key_rows.at[:, at * HK : (at + 1) * HK], keys.at[h], sems.at[0, h]
-            ),
-            pltpu.make_async_copy(
-                values.at[:, at * HV : (at + 1) * HV], vals.at[h], sems.at[1, h]
-            ),
-        )
-        for copy in pair:
-            copy.start()
-        copies.append(pair)
     after = tri(length, lambda r, c: c > r).astype(F32).astype(BF16)
     me = place()[0] % QUAD
     decays[...] = jnp.zeros_like(decays)
     for h in range(count):
-        span = slice((first + h) * HK, (first + h + 1) * HK)
-        logs = head_log_decay(low[...], matrix[:, span], bias[:, span], shift[...], first + h)
+        narrow, wide = slice(h * HK, (h + 1) * HK), slice(h * HV, (h + 1) * HV)
+        logs = head_log_decay(
+            low[...], matrix[:, narrow], bias[:, narrow], shift[...], first + h
+        )
         suffix = split_dot(after, logs)
         total = jnp.exp(suffix[0:1, :] + logs[0:1, :])
         high = total.astype(BF16).astype(F32)
         decays[h : h + 1, 0:HK] = high
         decays[h : h + 1, HK : 2 * HK] = total - high
-        for copy in copies[h]:
-            copy.wait()
-        end_keys = (keys[h].astype(F32) * jnp.exp(suffix)).astype(BF16)
-        state[...] = contract0(end_keys, vals[h])
+        end_keys = (key_rows[:, narrow].astype(F32) * jnp.exp(suffix)).astype(BF16)
+        state[...] = contract0(end_keys, values[:, wide])
         for k in range(QUAD):
             start = pl.multiple_of((me ^ k) * piece, piece)
             outs[k][h * piece : (h + 1) * piece, :] = state[pl.ds(start, piece), :].astype(BF16)
@@ -112,18 +97,28 @@
 def device_states(first, count, low, matrix, bias, shift, key_rows, values):
     length = key_rows.shape[0]
     rows = count * (HK // QUAD) + 8
+    block = first // count
+
+    def whole(array):
+        return pl.BlockSpec(array.shape, lambda i: (0, 0))
+
+    def part(height, width):
+        return pl.BlockSpec((height, count * width), lambda i: (0, block))
+
     return pl.pallas_call(
         functools.partial(state_kernel, first, count),
-        in_specs=[VMEM] * 4 + [HBM] * 2,
-        out_specs=[VMEM] * QUAD,
+        grid=(1,),
+        in_specs=[
+            whole(low),
+            part(matrix.shape[0], HK),
+            part(1, HK),
+            whole(shift),
+            part(length, HK),
+            part(length, HV),
+        ],
+        out_specs=[pl.BlockSpec((rows, HV), lambda i: (0, 0))] * QUAD,
         out_shape=[jax.ShapeDtypeStruct((rows, HV), BF16)] * QUAD,
-        scratch_shapes=[
-            pltpu.VMEM((count, length, HK), BF16),
-            pltpu.VMEM((count, length, HV), BF16),
-            pltpu.VMEM((HK, HV), F32),
-            pltpu.VMEM((8, HV), F32),
-            pltpu.SemaphoreType.DMA((2, count)),
-        ],
+        scratch_shapes=[pltpu.VMEM((HK, HV), F32), pltpu.VMEM((8, HV), F32)],
         compiler_params=params(60),
         cost_estimate=cost(count * 4e8, count * 5e5),
     )(low, matrix, bias, shift, key_rows, values)
@@ -275,79 +270,110 @@
         yield slice(k * rows, (k + 1) * rows), own, other
 
 
-def project_kernel(count, groups, gain, matrix, *refs):
-    mixed, keep, send, carried = refs[-4:]
-    chunks = len(refs[:-4]) // (2 + QUAD)
-    local, queries, pieces = refs[:chunks], refs[chunks : 2 * chunks], refs[2 * chunks : -4]
+def read_heads(count, groups, gain, local, queries, pieces, mixed, carried):
     me, my_core, my_line = place()
     me = me % QUAD
     piece = HK // QUAD
-    split = keep.shape[0]
-    rows = split // groups
-    for part in range(chunks):
-        for h in range(count):
-            span = slice(h * piece, (h + 1) * piece)
-            for k in range(QUAD):
-                start = pl.multiple_of((me ^ k) * piece, piece)
-                carried[pl.ds(start, piece), :] = pieces[part * QUAD + k][span, :]
-            narrow, wide = slice(h * HK, (h + 1) * HK), slice(h * HV, (h + 1) * HV)
-            out = local[part][:, wide] + jnp.dot(
-                queries[part][:, narrow], carried[...], preferred_element_type=F32
-            )
-            spread = lax.rsqrt(jnp.mean(out * out, axis=-1, keepdims=True) + EPSILON)
-            value = (out * spread * gain[...]).astype(BF16)
-            at = (part * count + h) * HV
-            for b in range(2 * groups):
-                line, core = b // 2, b % 2
-                there = (line ^ my_line) + (core ^ my_core) * groups
-                there = pl.multiple_of(there * rows, rows)
-                mixed[pl.ds(there, rows), at : at + HV] = value[b * rows : (b + 1) * rows, :]
-    keep[...] = jnp.dot(mixed[:split, :], matrix[...], preferred_element_type=F32)
-    send[...] = jnp.dot(mixed[split:, :], matrix[...], preferred_element_type=F32).astype(BF16)
-
-
-def project_rest_kernel(mixed, matrix, keep, send):
+    rows = mixed.shape[0] // (2 * groups)
+    for h in range(count):
+        span = slice(h * piece, (h + 1) * piece)
+        for k in range(QUAD):
+            start = pl.multiple_of((me ^ k) * piece, piece)
+            carried[pl.ds(start, piece), :] = pieces[k][span, :]
+        narrow, wide = slice(h * HK, (h + 1) * HK), slice(h * HV, (h + 1) * HV)
+        out = local[:, wide] + jnp.dot(
+            queries[:, narrow], carried[...], preferred_element_type=F32
+        )
+        spread = lax.rsqrt(jnp.mean(out * out, axis=-1, keepdims=True) + EPSILON)
+        value = (out * spread * gain[...]).astype(BF16)
+        for b in range(2 * groups):
+            line, core = b // 2, b % 2
+            there = (line ^ my_line) + (core ^ my_core) * groups
+            there = pl.multiple_of(there * rows, rows)
+            mixed[pl.ds(there, rows), wide] = value[b * rows : (b + 1) * rows, :]
+
+
+def project_early_kernel(count, groups, gain, matrix, local, queries, *refs):
+    pieces, (total, mixed, carried) = refs[:QUAD], refs[QUAD:]
+    read_heads(count, groups, gain, local, queries, pieces, mixed, carried)
+    total[...] = jnp.dot(mixed[...], matrix[...], preferred_element_type=F32)
+
+
+def project_kernel(count, groups, gain, matrix, local, queries, *refs):
+    pieces, early, (mixed, keep, send, carried) = refs[:QUAD], refs[QUAD:-4], refs[-4:]
+    read_heads(count, groups, gain, local, queries, pieces, mixed, carried)
+    project_rest_kernel(mixed, matrix, *early, keep, send)
+
+
+def project_rest_kernel(mixed, matrix, *refs):
+    early, (keep, send) = refs[:-2], refs[-2:]
     split = keep.shape[0]
     total = jnp.dot(mixed[...], matrix[...], preferred_element_type=F32)
+    for part in early:
+        total = total + part[...]
     keep[...] = total[:split, :]
     send[...] = total[split:, :].astype(BF16)
 
 
 def project(count, groups, gain, matrix, local, pieces):
-    outs = [array for array, _ in local] + [array for _, array in local]
-    length = outs[0].shape[0]
-    depth, width = matrix.shape
+    length = local[0][0].shape[0]
+    width = matrix.shape[1]
+    depth = count * HV
     cut = width // 2
     small = [
         jax.ShapeDtypeStruct((length // 2, cut), F32),
         jax.ShapeDtypeStruct((length // 2, cut), BF16),
     ]
     whole = [pl.BlockSpec((length // 2, cut), lambda i: (0, 0))] * 2
+    chunks = len(local)
+    early = []
+    for part in range(chunks - 1):
+        early.append(
+            pl.pallas_call(
+                functools.partial(project_early_kernel, count, groups),
+                grid=(1,),
+                in_specs=[VMEM, pl.BlockSpec((depth, width), lambda i, p=part: (p, 0))]
+                + [VMEM] * (2 + QUAD),
+                out_specs=pl.BlockSpec((length, width), lambda i: (0, 0)),
+                out_shape=jax.ShapeDtypeStruct((length, width), F32),
+                scratch_shapes=[
+                    pltpu.VMEM((length, depth), BF16),
+                    pltpu.VMEM((HK, HV), BF16),
+                ],
+                compiler_params=params(28),
+                cost_estimate=cost(2e9, 8e6),
+                name="project_early",
+            )(gain, matrix, *local[part], *pieces[part * QUAD : (part + 1) * QUAD])
+        )
+    last = chunks - 1
+
+    def side_spec(side):
+        return pl.BlockSpec((depth, cut), lambda i: (last, side))
+
+    def early_spec(side):
+        return [pl.BlockSpec((length, cut), lambda i: (0, side))] * len(early)
+
     mixed, keep, send = pl.pallas_call(
         functools.partial(project_kernel, count, groups),
         grid=(1,),
-        in_specs=[VMEM, pl.BlockSpec((depth, cut), lambda i: (0, 0))]
-        + [VMEM] * (len(outs) + len(pieces)),
+        in_specs=[VMEM, side_spec(0)] + [VMEM] * (2 + QUAD) + early_spec(0),
         out_specs=[pl.BlockSpec((length, depth), lambda i: (0, 0))] + whole,
         out_shape=[jax.ShapeDtypeStruct((length, depth), BF16)] + small,
         scratch_shapes=[pltpu.VMEM((HK, HV), BF16)],
         compiler_params=params(28),
-        cost_estimate=cost(2e9, 8e6),
+        cost_estimate=cost(1e9, 6e6),
         name="project",
-    )(gain, matrix, *outs, *pieces)
+    )(gain, matrix, *local[last], *pieces[last * QUAD :], *early)
     rest = pl.pallas_call(
         project_rest_kernel,
         grid=(1,),
-        in_specs=[
-            pl.BlockSpec((length, depth), lambda i: (0, 0)),
-            pl.BlockSpec((depth, cut), lambda i: (0, 1)),
-        ],
+        in_specs=[pl.BlockSpec((length, depth), lambda i: (0, 0)), side_spec(1)] + early_spec(1),
         out_specs=whole,
         out_shape=small,
         compiler_params=params(28),
         cost_estimate=cost(1e9, 6e6),
         name="project_rest",
-    )(mixed, matrix)
+    )(mixed, matrix, *early)
     return (keep, send), rest
 
 

time: 158 us -> 160 us (1.013)
  waiting for transfers between devices: 67.2 us -> 71.4 us
  starting transfers between devices: 58.2 us -> 55.5 us
    ppermute x47, waiting for transfers between devices: 67.2 us -> 71.4 us  [swap(): return lax.ppermute(value, axis, xor_perm(axis, k))]
    ppermute x47, starting transfers between devices: 48 us -> 45.4 us  [swap(): return lax.ppermute(value, axis, xor_perm(axis, k))]
    pallas_call x2 -> x3, Pallas kernels: 7.61 us -> 9.34 us  [the longest x2 7.64 us: device_states(): pl.pallas_call(functools.partial(state_kernel, first, count), grid=(1,),...]
  transfers between devices with their start and end apart: 49 -> 49, of which waited for: 22 -> 25; matrix products, arithmetic and copies ran while one was open for 0% -> 0% of each run, Pallas kernels for 11% -> 12%
where the time goes in v4:
time: 160 us
  waiting for transfers between devices  71.4 us (45%)
  starting transfers between devices  55.5 us (35%)
  Pallas kernels  30.3 us (19%)
  local copies, waits for them, and re-layouts  1.91 us (1%)
    ppermute x47, waiting for transfers between devices, swap(): return lax.ppermute(value, axis, xor_perm(axis, k))  71.4 us
    ppermute x47, starting transfers between devices, swap(): return lax.ppermute(value, axis, xor_perm(axis, k))  45.4 us
    ppermute x2, starting transfers between devices, quad_entry(): start = lax.ppermute(total, 'sp', perm)  10.2 us
    pallas_call x2, Pallas kernels, device_states(): pl.pallas_call(functools.partial(state_kernel, first, count), grid=(1,),...  7.64 us
    pallas_call x3, Pallas kernels, expert(): pl.pallas_call(functools.partial(expert_kernel, count), in_specs=[VMEM] *...  7.36 us
    pallas_call x2, Pallas kernels, local_attention(): pl.pallas_call(functools.partial(local_kernel, first, count), grid=(1,),...  5.12 us
  transfers between devices with their start and end apart: 49, of which 25 were waited for; matrix products, arithmetic and copies ran while one was open for 0% of the time, Pallas kernels for 12%

profile of v4, /device:TPU:0, one launch (start us, length us, event | category | flops | bytes accessed | tf_op | source)
XLA Modules:
  0.0 159.8 jit_solution(13046074824289397211)
XLA Ops:
  0.0 3.8 %shard_map.155 = (bf16[136,512]{1,0:T(8,128)(2,1)}, bf16[136,512]{1,0:T(8,128)(2,1)}, bf16[136,512]{1,0:T(8,128)(2,1)}, bf16[136,512]{1,0:T(8,128)(2,1)}) custom-call(bf16[16,256]{1,0:T(8,128)(2,1)} %bitcast.20, bf16[16,1024]{1,0:T(8,128)(2,1)} %matrix.10, f32[1,1024]{1,0:T(1,128)} %bitcast.24, f32[4,256]{1,0:T(4,128)} %bitcast.28, ...), custom_call_target="tpu_custom_call" | custom-call | flops 800000000 | bytes 1000000 | tf_op jit(solution)/shard_map/pallas_call | solution.py:108
  3.9 3.0 %collective-permute-start.7 = (bf16[136,512]{1,0:T(8,128)(2,1)}, bf16[136,512]{1,0:T(8,128)(2,1)S(1)}, u32[]{:S(2)}, u32[]{:S(2)}) collective-permute-start(bf16[136,512]{1,0:T(8,128)(2,1)} %get-tuple-element.86), channel_id=1, source_target_pairs={{0,4},{4,0},{8,12},{12,8},{16,20},{20,16},{24,28},{28,24},{1,5},{5... | collective-permute-start | bytes 417800 | tf_op jit(solution)/shard_map/ppermute | solution.py:629
  8.5 3.8 %shard_map.156 = (bf16[136,512]{1,0:T(8,128)(2,1)}, bf16[136,512]{1,0:T(8,128)(2,1)}, bf16[136,512]{1,0:T(8,128)(2,1)}, bf16[136,512]{1,0:T(8,128)(2,1)}) custom-call(bf16[16,256]{1,0:T(8,128)(2,1)} %bitcast.21, bf16[16,1024]{1,0:T(8,128)(2,1)} %matrix.10, f32[1,1024]{1,0:T(1,128)} %bitcast.25, f32[4,256]{1,0:T(4,128)} %bitcast.29, ...), custom_call_target="tpu_custom_call" | custom-call | flops 800000000 | bytes 1000000 | tf_op jit(solution)/shard_map/pallas_call | solution.py:108
  16.2 5.2 %collective-permute-start.10 = (bf16[128,512]{1,0:T(8,128)(2,1)S(1)}, bf16[128,512]{1,0:T(8,128)(2,1)S(1)}, u32[]{:S(2)}, u32[]{:S(2)}) collective-permute-start(bf16[128,512]{1,0:T(8,128)(2,1)S(1)} %quad_total.3), channel_id=1, source_target_pairs={{0,16},{4,20},{8,24},{12,28},{1,17},{5,21},{9,25},{13,29},{2,18},{... | collective-permute-start | bytes 393224 | tf_op jit(solution)/shard_map/ppermute | solution.py:259
  23.4 5.0 %collective-permute-start.3 = (bf16[128,512]{1,0:T(8,128)(2,1)S(1)}, bf16[128,512]{1,0:T(8,128)(2,1)S(1)}, u32[]{:S(2)}, u32[]{:S(2)}) collective-permute-start(bf16[128,512]{1,0:T(8,128)(2,1)S(1)} %quad_total.2), channel_id=1, source_target_pairs={{0,16},{4,20},{8,24},{12,28},{1,17},{5,21},{9,25},{13,29},{2,18},{... | collective-permute-start | bytes 393224 | tf_op jit(solution)/shard_map/ppermute | solution.py:259
  29.8 2.8 %collective-permute-start.12 = (bf16[128,512]{1,0:T(8,128)(2,1)S(1)}, bf16[128,512]{1,0:T(8,128)(2,1)S(1)}, u32[]{:S(2)}, u32[]{:S(2)}) collective-permute-start(bf16[128,512]{1,0:T(8,128)(2,1)S(1)} %get-tuple-element.102), channel_id=1, source_target_pairs={{0,8},{4,12},{8,0},{12,4},{16,24},{20,28},{24,16},{28,20},{1,9},{5... | collective-permute-start | bytes 393224 | tf_op jit(solution)/shard_map/ppermute | solution.py:629
  32.7 2.6 %shard_map.157 = (f32[256,1024]{1,0:T(8,128)S(1)}, bf16[256,512]{1,0:T(8,128)(2,1)S(1)}) custom-call(bf16[16,256]{1,0:T(8,128)(2,1)S(1)} %bitcast.22, bf16[16,1024]{1,0:T(8,128)(2,1)S(1)} %copy-done.13, f32[1,1024]{1,0:T(1,128)S(1)} %bitcast.26, f32[4,256]{1,0:T(4,128)S(1)} %bitcast.30, bf16[256,1024]{1,0:T(8,128)(2,1)S(1)} %copy-done.11, ...), custom_call_target="tpu_custom_call" | custom-call | flops 800000000 | bytes 2400000 | tf_op jit(solution)/shard_map/pallas_call | solution.py:171
  35.3 2.6 %shard_map.154 = (f32[256,1024]{1,0:T(8,128)S(1)}, bf16[256,512]{1,0:T(8,128)(2,1)S(1)}) custom-call(bf16[16,256]{1,0:T(8,128)(2,1)S(1)} %bitcast.23, bf16[16,1024]{1,0:T(8,128)(2,1)S(1)} %copy-done.13, f32[1,1024]{1,0:T(1,128)S(1)} %bitcast.27, f32[4,256]{1,0:T(4,128)S(1)} %bitcast.31, bf16[256,1024]{1,0:T(8,128)(2,1)S(1)} %copy-done.11, ...), custom_call_target="tpu_custom_call" | custom-call | flops 800000000 | bytes 2400000 | tf_op jit(solution)/shard_map/pallas_call | solution.py:171
  45.9 2.9 %collective-permute-done.6.refs_3_ = bf16[128,512]{1,0:T(8,128)(2,1)S(1)} collective-permute-done((bf16[128,512]{1,0:T(8,128)(2,1)S(1)}, bf16[128,512]{1,0:T(8,128)(2,1)S(1)}, u32[]{:S(2)}, u32[]{:S(2)}) %collective-permute-start.6) | collective-permute-done | bytes 131104 | tf_op jit(solution)/shard_map/ppermute | solution.py:629
  58.0 3.7 %collective-permute-done.18.refs_7_ = bf16[128,1024]{1,0:T(8,128)(2,1)S(1)} collective-permute-done((bf16[128,1024]{1,0:T(8,128)(2,1)S(1)}, bf16[128,1024]{1,0:T(8,128)(2,1)S(1)}, u32[]{:S(2)}, u32[]{:S(2)}) %collective-permute-start.18) | collective-permute-done | bytes 262176 | tf_op jit(solution)/shard_map/ppermute | solution.py:629
  61.7 5.6 %collective-permute-done.17.refs_6_ = bf16[128,1024]{1,0:T(8,128)(2,1)S(1)} collective-permute-done((bf16[128,1024]{1,0:T(8,128)(2,1)S(1)}, bf16[128,1024]{1,0:T(8,128)(2,1)S(1)}, u32[]{:S(2)}, u32[]{:S(2)}) %collective-permute-start.17) | collective-permute-done | bytes 262176 | tf_op jit(solution)/shard_map/ppermute | solution.py:629
  67.3 4.8 %collective-permute-done.16.refs_5_ = bf16[64,2048]{1,0:T(8,128)(2,1)S(1)} collective-permute-done((bf16[64,2048]{1,0:T(8,128)(2,1)S(1)}, bf16[64,2048]{1,0:T(8,128)(2,1)S(1)}, u32[]{:S(2)}, u32[]{:S(2)}) %collective-permute-start.16) | collective-permute-done | bytes 262176 | tf_op jit(solution)/shard_map/ppermute | solution.py:629
  77.7 9.1 %collective-permute-done.23.refs_0_ = bf16[32,2048]{1,0:T(8,128)(2,1)S(1)} collective-permute-done((bf16[32,2048]{1,0:T(8,128)(2,1)S(1)}, bf16[32,2048]{1,0:T(8,128)(2,1)S(1)}, u32[]{:S(2)}, u32[]{:S(2)}) %collective-permute-start.23) | collective-permute-done | bytes 131104 | tf_op jit(solution)/shard_map/ppermute | solution.py:629
  86.9 2.8 %collective-permute-done.24.refs_1_ = bf16[32,2048]{1,0:T(8,128)(2,1)S(1)} collective-permute-done((bf16[32,2048]{1,0:T(8,128)(2,1)S(1)}, bf16[32,2048]{1,0:T(8,128)(2,1)S(1)}, u32[]{:S(2)}, u32[]{:S(2)}) %collective-permute-start.24) | collective-permute-done | bytes 131104 | tf_op jit(solution)/shard_map/ppermute | solution.py:629
  91.0 2.4 %shard_map.158 = (f32[64,2048]{1,0:T(8,128)S(1)}, bf16[64,2048]{1,0:T(8,128)(2,1)S(1)}) custom-call(bf16[704,2048]{1,0:T(8,128)(2,1)S(1)} %get-tuple-element.124.gate, bf16[704,2048]{1,0:T(8,128)(2,1)S(1)} %get-tuple-element.125.widen, bf16[704,2048]{1,0:T(8,128)(2,1)S(1)} %get-tuple-element.126.down, bf16[32,2048]{1,0:T(8,128)(2,1)S(1)} %collective-permute-done.23.refs_0_, ...), custom_call_target="tpu_custom_call" | custom-call | flops 1200000000 | bytes 4000000 | tf_op jit(solution)/shard_map/pallas_call | solution.py:542
  106.4 2.6 %collective-permute-start.39 = (bf16[32,2048]{1,0:T(8,128)(2,1)S(1)}, bf16[32,2048]{1,0:T(8,128)(2,1)S(1)}, u32[]{:S(2)}, u32[]{:S(2)}) collective-permute-start(bf16[32,2048]{1,0:T(8,128)(2,1)S(1)} %get-tuple-element.150), channel_id=1, source_target_pairs={{0,28},{4,24},{8,20},{12,16},{16,12},{20,8},{24,4},{28,0},{1,29},{... | collective-permute-start | bytes 393224 | tf_op jit(solution)/shard_map/ppermute | solution.py:629
  109.0 2.6 %shard_map.160 = (f32[128,2048]{1,0:T(8,128)S(1)}, bf16[128,2048]{1,0:T(8,128)(2,1)S(1)}) custom-call(bf16[704,2048]{1,0:T(8,128)(2,1)S(1)} %get-tuple-element.124.gate, bf16[704,2048]{1,0:T(8,128)(2,1)S(1)} %get-tuple-element.125.widen, bf16[704,2048]{1,0:T(8,128)(2,1)S(1)} %get-tuple-element.126.down, bf16[32,2048]{1,0:T(8,128)(2,1)S(1)} %get-tuple-element.139.refs_0_, ...), custom_call_target="tpu_custom_call" | custom-call | flops 2400000000 | bytes 4000000 | tf_op jit(solution)/shard_map/pallas_call | solution.py:542
  112.6 2.7 %collective-permute-done.39.refs_1_ = bf16[32,2048]{1,0:T(8,128)(2,1)S(1)} collective-permute-done((bf16[32,2048]{1,0:T(8,128)(2,1)S(1)}, bf16[32,2048]{1,0:T(8,128)(2,1)S(1)}, u32[]{:S(2)}, u32[]{:S(2)}) %collective-permute-start.39) | collective-permute-done | bytes 131104 | tf_op jit(solution)/shard_map/ppermute | solution.py:629
  116.8 2.4 %shard_map.162 = (f32[64,2048]{1,0:T(8,128)S(1)}, bf16[64,2048]{1,0:T(8,128)(2,1)S(1)}) custom-call(bf16[704,2048]{1,0:T(8,128)(2,1)S(1)} %get-tuple-element.124.gate, bf16[704,2048]{1,0:T(8,128)(2,1)S(1)} %get-tuple-element.125.widen, bf16[704,2048]{1,0:T(8,128)(2,1)S(1)} %get-tuple-element.126.down, bf16[32,2048]{1,0:T(8,128)(2,1)S(1)} %collective-permute-done.38.refs_0_, ...), custom_call_target="tpu_custom_call" | custom-call | flops 1200000000 | bytes 4000000 | tf_op jit(solution)/shard_map/pallas_call | solution.py:542
  119.6 3.7 %collective-permute-start.36 = (bf16[32,2048]{1,0:T(8,128)(2,1)S(1)}, bf16[32,2048]{1,0:T(8,128)(2,1)S(1)}, u32[]{:S(2)}, u32[]{:S(2)}) collective-permute-start(bf16[32,2048]{1,0:T(8,128)(2,1)S(1)} %get-tuple-element.137), channel_id=1, source_target_pairs={{0,16},{4,20},{8,24},{12,28},{16,0},{20,4},{24,8},{28,12},{1,17},{... | collective-permute-start | bytes 393224 | tf_op jit(solution)/shard_map/ppermute | solution.py:629
  129.8 8.9 %collective-permute-done.36.refs_4_ = bf16[32,2048]{1,0:T(8,128)(2,1)S(1)} collective-permute-done((bf16[32,2048]{1,0:T(8,128)(2,1)S(1)}, bf16[32,2048]{1,0:T(8,128)(2,1)S(1)}, u32[]{:S(2)}, u32[]{:S(2)}) %collective-permute-start.36) | collective-permute-done | bytes 131104 | tf_op jit(solution)/shard_map/ppermute | solution.py:629
  138.8 3.9 %collective-permute-done.37.refs_5_ = bf16[32,2048]{1,0:T(8,128)(2,1)S(1)} collective-permute-done((bf16[32,2048]{1,0:T(8,128)(2,1)S(1)}, bf16[32,2048]{1,0:T(8,128)(2,1)S(1)}, u32[]{:S(2)}, u32[]{:S(2)}) %collective-permute-start.37) | collective-permute-done | bytes 131104 | tf_op jit(solution)/shard_map/ppermute | solution.py:629
  144.0 4.5 %collective-permute-done.35.refs_3_ = bf16[32,2048]{1,0:T(8,128)(2,1)S(1)} collective-permute-done((bf16[32,2048]{1,0:T(8,128)(2,1)S(1)}, bf16[32,2048]{1,0:T(8,128)(2,1)S(1)}, u32[]{:S(2)}, u32[]{:S(2)}) %collective-permute-start.35) | collective-permute-done | bytes 131104 | tf_op jit(solution)/shard_map/ppermute | solution.py:629
  152.8 4.2 %collective-permute-done.48.refs_5_ = bf16[64,1024]{1,0:T(8,128)(2,1)S(1)} collective-permute-done((bf16[64,1024]{1,0:T(8,128)(2,1)S(1)}, bf16[64,1024]{1,0:T(8,128)(2,1)S(1)}, u32[]{:S(2)}, u32[]{:S(2)}) %collective-permute-start.48) | collective-permute-done | bytes 131104 | tf_op jit(solution)/shard_map/ppermute | solution.py:629
  (140 shorter events, 63.7 us)
Async XLA Ops:
  3.9 11.9 %collective-permute-start.7 = (bf16[136,512]{1,0:T(8,128)(2,1)}, bf16[136,512]{1,0:T(8,128)(2,1)S(1)}, u32[]{:S(2)}, u32[]{:S(2)}) collective-permute-start(bf16[136,512]{1,0:T(8,128)(2,1)} %get-tuple-element.86), channel_id=1, source_target_pairs={{0,4},{4,0},{8,12},{12,8},{16,20},{20,16},{24,28},{28,24},{1,5},{5... | collective-permute-start | bytes 417800 | tf_op jit(solution)/shard_map/ppermute | solution.py:629
  6.9 8.9 %collective-permute-start.8 = (bf16[136,512]{1,0:T(8,128)(2,1)}, bf16[136,512]{1,0:T(8,128)(2,1)S(1)}, u32[]{:S(2)}, u32[]{:S(2)}) collective-permute-start(bf16[136,512]{1,0:T(8,128)(2,1)} %get-tuple-element.87), channel_id=1, source_target_pairs={{0,8},{4,12},{8,0},{12,4},{16,24},{20,28},{24,16},{28,20},{1,9},{5... | collective-permute-start | bytes 417800 | tf_op jit(solution)/shard_map/ppermute | solution.py:629
  8.5 7.3 %collective-permute-start.9 = (bf16[136,512]{1,0:T(8,128)(2,1)}, bf16[136,512]{1,0:T(8,128)(2,1)S(1)}, u32[]{:S(2)}, u32[]{:S(2)}) collective-permute-start(bf16[136,512]{1,0:T(8,128)(2,1)} %get-tuple-element.88), channel_id=1, source_target_pairs={{0,12},{4,8},{8,4},{12,0},{16,28},{20,24},{24,20},{28,16},{1,13},{... | collective-permute-start | bytes 417800 | tf_op jit(solution)/shard_map/ppermute | solution.py:629
  12.3 9.1 %collective-permute-start = (bf16[136,512]{1,0:T(8,128)(2,1)}, bf16[136,512]{1,0:T(8,128)(2,1)S(1)}, u32[]{:S(2)}, u32[]{:S(2)}) collective-permute-start(bf16[136,512]{1,0:T(8,128)(2,1)} %get-tuple-element.91), channel_id=1, source_target_pairs={{0,4},{4,0},{8,12},{12,8},{16,20},{20,16},{24,28},{28,24},{1,5},{5... | collective-permute-start | bytes 417800 | tf_op jit(solution)/shard_map/ppermute | solution.py:629
  14.2 7.2 %collective-permute-start.1 = (bf16[136,512]{1,0:T(8,128)(2,1)}, bf16[136,512]{1,0:T(8,128)(2,1)S(1)}, u32[]{:S(2)}, u32[]{:S(2)}) collective-permute-start(bf16[136,512]{1,0:T(8,128)(2,1)} %get-tuple-element.92), channel_id=1, source_target_pairs={{0,8},{4,12},{8,0},{12,4},{16,24},{20,28},{24,16},{28,20},{1,9},{5... | collective-permute-start | bytes 417800 | tf_op jit(solution)/shard_map/ppermute | solution.py:629
  16.2 12.2 %collective-permute-start.10 = (bf16[128,512]{1,0:T(8,128)(2,1)S(1)}, bf16[128,512]{1,0:T(8,128)(2,1)S(1)}, u32[]{:S(2)}, u32[]{:S(2)}) collective-permute-start(bf16[128,512]{1,0:T(8,128)(2,1)S(1)} %quad_total.3), channel_id=1, source_target_pairs={{0,16},{4,20},{8,24},{12,28},{1,17},{5,21},{9,25},{13,29},{2,18},{... | collective-permute-start | bytes 393224 | tf_op jit(solution)/shard_map/ppermute | solution.py:259
  23.4 14.5 %collective-permute-start.3 = (bf16[128,512]{1,0:T(8,128)(2,1)S(1)}, bf16[128,512]{1,0:T(8,128)(2,1)S(1)}, u32[]{:S(2)}, u32[]{:S(2)}) collective-permute-start(bf16[128,512]{1,0:T(8,128)(2,1)S(1)} %quad_total.2), channel_id=1, source_target_pairs={{0,16},{4,20},{8,24},{12,28},{1,17},{5,21},{9,25},{13,29},{2,18},{... | collective-permute-start | bytes 393224 | tf_op jit(solution)/shard_map/ppermute | solution.py:259
  29.0 13.9 %collective-permute-start.11 = (bf16[128,512]{1,0:T(8,128)(2,1)S(1)}, bf16[128,512]{1,0:T(8,128)(2,1)S(1)}, u32[]{:S(2)}, u32[]{:S(2)}) collective-permute-start(bf16[128,512]{1,0:T(8,128)(2,1)S(1)} %get-tuple-element.101), channel_id=1, source_target_pairs={{0,4},{4,0},{8,12},{12,8},{16,20},{20,16},{24,28},{28,24},{1,5},{5... | collective-permute-start | bytes 393224 | tf_op jit(solution)/shard_map/ppermute | solution.py:629
  29.8 13.1 %collective-permute-start.12 = (bf16[128,512]{1,0:T(8,128)(2,1)S(1)}, bf16[128,512]{1,0:T(8,128)(2,1)S(1)}, u32[]{:S(2)}, u32[]{:S(2)}) collective-permute-start(bf16[128,512]{1,0:T(8,128)(2,1)S(1)} %get-tuple-element.102), channel_id=1, source_target_pairs={{0,8},{4,12},{8,0},{12,4},{16,24},{20,28},{24,16},{28,20},{1,9},{5... | collective-permute-start | bytes 393224 | tf_op jit(solution)/shard_map/ppermute | solution.py:629
  32.7 10.3 %collective-permute-start.13 = (bf16[128,512]{1,0:T(8,128)(2,1)S(1)}, bf16[128,512]{1,0:T(8,128)(2,1)S(1)}, u32[]{:S(2)}, u32[]{:S(2)}) collective-permute-start(bf16[128,512]{1,0:T(8,128)(2,1)S(1)} %get-tuple-element.103), channel_id=1, source_target_pairs={{0,12},{4,8},{8,4},{12,0},{16,28},{20,24},{24,20},{28,16},{1,13},{... | collective-permute-start | bytes 393224 | tf_op jit(solution)/shard_map/ppermute | solution.py:629
  52.5 9.2 %collective-permute-start.18 = (bf16[128,1024]{1,0:T(8,128)(2,1)S(1)}, bf16[128,1024]{1,0:T(8,128)(2,1)S(1)}, u32[]{:S(2)}, u32[]{:S(2)}) collective-permute-start(bf16[128,1024]{1,0:T(8,128)(2,1)S(1)} %add_convert_fusion), channel_id=1, source_target_pairs={{0,2},{1,3},{2,0},{3,1},{4,6},{5,7},{6,4},{7,5},{8,10},{9,11},{10,... | collective-permute-start | bytes 786440 | tf_op jit(solution)/shard_map/ppermute | solution.py:629
  54.1 13.2 %collective-permute-start.17 = (bf16[128,1024]{1,0:T(8,128)(2,1)S(1)}, bf16[128,1024]{1,0:T(8,128)(2,1)S(1)}, u32[]{:S(2)}, u32[]{:S(2)}) collective-permute-start(bf16[128,1024]{1,0:T(8,128)(2,1)S(1)} %add_convert_fusion.1), channel_id=1, source_target_pairs={{0,2},{1,3},{2,0},{3,1},{4,6},{5,7},{6,4},{7,5},{8,10},{9,11},{10,... | collective-permute-start | bytes 786440 | tf_op jit(solution)/shard_map/ppermute | solution.py:629
  54.7 17.4 %collective-permute-start.16 = (bf16[64,2048]{1,0:T(8,128)(2,1)S(1)}, bf16[64,2048]{1,0:T(8,128)(2,1)S(1)}, u32[]{:S(2)}, u32[]{:S(2)}) collective-permute-start(bf16[64,2048]{1,0:T(8,128)(2,1)S(1)} %copy-done.7), channel_id=1, source_target_pairs={{0,2},{1,3},{2,0},{3,1},{4,6},{5,7},{6,4},{7,5},{8,10},{9,11},{10,... | collective-permute-start | bytes 786440 | tf_op jit(solution)/shard_map/ppermute | solution.py:629
  75.2 11.6 %collective-permute-start.23 = (bf16[32,2048]{1,0:T(8,128)(2,1)S(1)}, bf16[32,2048]{1,0:T(8,128)(2,1)S(1)}, u32[]{:S(2)}, u32[]{:S(2)}) collective-permute-start(bf16[32,2048]{1,0:T(8,128)(2,1)S(1)} %get-tuple-element.133), channel_id=1, source_target_pairs={{0,16},{4,20},{8,24},{12,28},{16,0},{20,4},{24,8},{28,12},{1,17},{... | collective-permute-start | bytes 393224 | tf_op jit(solution)/shard_map/ppermute | solution.py:629
  76.4 13.2 %collective-permute-start.24 = (bf16[32,2048]{1,0:T(8,128)(2,1)S(1)}, bf16[32,2048]{1,0:T(8,128)(2,1)S(1)}, u32[]{:S(2)}, u32[]{:S(2)}) collective-permute-start(bf16[32,2048]{1,0:T(8,128)(2,1)S(1)} %get-tuple-element.134), channel_id=1, source_target_pairs={{0,20},{4,16},{8,28},{12,24},{16,4},{20,0},{24,12},{28,8},{1,21},{... | collective-permute-start | bytes 393224 | tf_op jit(solution)/shard_map/ppermute | solution.py:629
  95.0 8.3 %collective-permute-start.22 = (bf16[32,2048]{1,0:T(8,128)(2,1)S(1)}, bf16[32,2048]{1,0:T(8,128)(2,1)S(1)}, u32[]{:S(2)}, u32[]{:S(2)}) collective-permute-start(bf16[32,2048]{1,0:T(8,128)(2,1)S(1)} %get-tuple-element.132), channel_id=1, source_target_pairs={{0,12},{4,8},{8,4},{12,0},{16,28},{20,24},{24,20},{28,16},{1,13},{... | collective-permute-start | bytes 393224 | tf_op jit(solution)/shard_map/ppermute | solution.py:629
  104.3 8.3 %collective-permute-start.38 = (bf16[32,2048]{1,0:T(8,128)(2,1)S(1)}, bf16[32,2048]{1,0:T(8,128)(2,1)S(1)}, u32[]{:S(2)}, u32[]{:S(2)}) collective-permute-start(bf16[32,2048]{1,0:T(8,128)(2,1)S(1)} %get-tuple-element.149), channel_id=1, source_target_pairs={{0,24},{4,28},{8,16},{12,20},{16,8},{20,12},{24,0},{28,4},{1,25},{... | collective-permute-start | bytes 393224 | tf_op jit(solution)/shard_map/ppermute | solution.py:629
  106.4 8.9 %collective-permute-start.39 = (bf16[32,2048]{1,0:T(8,128)(2,1)S(1)}, bf16[32,2048]{1,0:T(8,128)(2,1)S(1)}, u32[]{:S(2)}, u32[]{:S(2)}) collective-permute-start(bf16[32,2048]{1,0:T(8,128)(2,1)S(1)} %get-tuple-element.150), channel_id=1, source_target_pairs={{0,28},{4,24},{8,20},{12,16},{16,12},{20,8},{24,4},{28,0},{1,29},{... | collective-permute-start | bytes 393224 | tf_op jit(solution)/shard_map/ppermute | solution.py:629
  111.7 16.5 %collective-permute-start.32 = (bf16[128,2048]{1,0:T(8,128)(2,1)S(1)}, bf16[128,2048]{1,0:T(8,128)(2,1)S(1)}, u32[]{:S(2)}, u32[]{:S(2)}) collective-permute-start(bf16[128,2048]{1,0:T(8,128)(2,1)S(1)} %get-tuple-element.144), channel_id=1, source_target_pairs={{0,1},{1,0},{2,3},{3,2},{4,5},{5,4},{6,7},{7,6},{8,9},{9,8},{10,11... | collective-permute-start | bytes 1572872 | tf_op jit(solution)/shard_map/ppermute | solution.py:629
  119.6 19.2 %collective-permute-start.36 = (bf16[32,2048]{1,0:T(8,128)(2,1)S(1)}, bf16[32,2048]{1,0:T(8,128)(2,1)S(1)}, u32[]{:S(2)}, u32[]{:S(2)}) collective-permute-start(bf16[32,2048]{1,0:T(8,128)(2,1)S(1)} %get-tuple-element.137), channel_id=1, source_target_pairs={{0,16},{4,20},{8,24},{12,28},{16,0},{20,4},{24,8},{28,12},{1,17},{... | collective-permute-start | bytes 393224 | tf_op jit(solution)/shard_map/ppermute | solution.py:629
  123.3 19.3 %collective-permute-start.37 = (bf16[32,2048]{1,0:T(8,128)(2,1)S(1)}, bf16[32,2048]{1,0:T(8,128)(2,1)S(1)}, u32[]{:S(2)}, u32[]{:S(2)}) collective-permute-start(bf16[32,2048]{1,0:T(8,128)(2,1)S(1)} %get-tuple-element.138), channel_id=1, source_target_pairs={{0,20},{4,16},{8,28},{12,24},{16,4},{20,0},{24,12},{28,8},{1,21},{... | collective-permute-start | bytes 393224 | tf_op jit(solution)/shard_map/ppermute | solution.py:629
  124.3 18.3 %collective-permute-start.43 = (bf16[32,2048]{1,0:T(8,128)(2,1)S(1)}, bf16[32,2048]{1,0:T(8,128)(2,1)S(1)}, u32[]{:S(2)}, u32[]{:S(2)}) collective-permute-start(bf16[32,2048]{1,0:T(8,128)(2,1)S(1)} %get-tuple-element.155), channel_id=1, source_target_pairs={{0,24},{4,28},{8,16},{12,20},{16,8},{20,12},{24,0},{28,4},{1,25},{... | collective-permute-start | bytes 393224 | tf_op jit(solution)/shard_map/ppermute | solution.py:629
  126.1 16.5 %collective-permute-start.44 = (bf16[32,2048]{1,0:T(8,128)(2,1)S(1)}, bf16[32,2048]{1,0:T(8,128)(2,1)S(1)}, u32[]{:S(2)}, u32[]{:S(2)}) collective-permute-start(bf16[32,2048]{1,0:T(8,128)(2,1)S(1)} %get-tuple-element.156), channel_id=1, source_target_pairs={{0,28},{4,24},{8,20},{12,16},{16,12},{20,8},{24,4},{28,0},{1,29},{... | collective-permute-start | bytes 393224 | tf_op jit(solution)/shard_map/ppermute | solution.py:629
  128.3 14.4 %collective-permute-start.33 = (bf16[32,2048]{1,0:T(8,128)(2,1)S(1)}, bf16[32,2048]{1,0:T(8,128)(2,1)S(1)}, u32[]{:S(2)}, u32[]{:S(2)}) collective-permute-start(bf16[32,2048]{1,0:T(8,128)(2,1)S(1)} %get-tuple-element.146), channel_id=1, source_target_pairs={{0,4},{4,0},{8,12},{12,8},{16,20},{20,16},{24,28},{28,24},{1,5},{5... | collective-permute-start | bytes 393224 | tf_op jit(solution)/shard_map/ppermute | solution.py:629
  (44 other events, 435.6 us)

commit v5 on v4

--- a/solution.py
+++ b/solution.py
@@ -119,7 +119,7 @@
         out_specs=[pl.BlockSpec((rows, HV), lambda i: (0, 0))] * QUAD,
         out_shape=[jax.ShapeDtypeStruct((rows, HV), BF16)] * QUAD,
         scratch_shapes=[pltpu.VMEM((HK, HV), F32), pltpu.VMEM((8, HV), F32)],
-        compiler_params=params(60),
+        compiler_params=params(60 if first == 0 else 53),
         cost_estimate=cost(count * 4e8, count * 5e5),
     )(low, matrix, bias, shift, key_rows, values)
 
@@ -245,7 +245,7 @@
         out_shape=[jax.ShapeDtypeStruct((rows, HV), BF16)] * outs,
         compiler_params=params(24),
         cost_estimate=cost(1e8, 1e6),
-        name="quad_prefix" if emit else "quad_total",
+        name="prefix" if emit else "total",
     )(*primed, *pieces)
 
 
@@ -342,7 +342,7 @@
                 ],
                 compiler_params=params(28),
                 cost_estimate=cost(2e9, 8e6),
-                name="project_early",
+                name="early",
             )(gain, matrix, *local[part], *pieces[part * QUAD : (part + 1) * QUAD])
         )
     last = chunks - 1
@@ -372,7 +372,7 @@
         out_shape=small,
         compiler_params=params(28),
         cost_estimate=cost(1e9, 6e6),
-        name="project_rest",
+        name="rest",
     )(mixed, matrix, *early)
     return (keep, send), rest
 
@@ -417,7 +417,7 @@
         ],
         compiler_params=params(24),
         cost_estimate=cost(1e7, 3e6),
-        name="midstream_norm",
+        name="norm",
     )(gain, *arrays)
 
 
@@ -473,7 +473,7 @@
         scratch_shapes=[pltpu.VMEM((3, length, n * half), F32)],
         compiler_params=params(16),
         cost_estimate=cost(1e8, 5e5),
-        name="slot_tables",
+        name="slots",
     )(routes, weights)
 
 

time: 160 us -> 159 us (level)
  local copies, waits for them, and re-layouts: 1.91 us -> 0.08 us
  starting transfers between devices: 55.5 us -> 57.1 us
    unnamed x38 -> x34, local copies, waits for them, and re-layouts: 1.91 us -> 0.08 us
    ppermute x47, starting transfers between devices: 45.4 us -> 47.1 us  [swap(): return lax.ppermute(value, axis, xor_perm(axis, k))]
where the time goes in v5:
time: 159 us
  waiting for transfers between devices  71.9 us (45%)
  starting transfers between devices  57.1 us (36%)
  Pallas kernels  29.5 us (19%)
    ppermute x47, waiting for transfers between devices, swap(): return lax.ppermute(value, axis, xor_perm(axis, k))  71.9 us
    ppermute x47, starting transfers between devices, swap(): return lax.ppermute(value, axis, xor_perm(axis, k))  47.1 us
    ppermute x2, starting transfers between devices, quad_entry(): start = lax.ppermute(total, 'sp', perm)  9.97 us
    pallas_call x3, Pallas kernels, expert(): pl.pallas_call(functools.partial(expert_kernel, count), in_specs=[VMEM] *...  7.36 us
    pallas_call x2, Pallas kernels, device_states(): pl.pallas_call(functools.partial(state_kernel, first, count), grid=(1,),...  6.85 us
    pallas_call x2, Pallas kernels, local_attention(): pl.pallas_call(functools.partial(local_kernel, first, count), grid=(1,),...  5.11 us
  transfers between devices with their start and end apart: 49, of which 25 were waited for; matrix products, arithmetic and copies ran while one was open for 0% of the time, Pallas kernels for 12%

profile of v5, /device:TPU:0, one launch (start us, length us, event | category | flops | bytes accessed | tf_op | source)
XLA Modules:
  0.0 159.2 jit_solution(3917127378695835088)
XLA Ops:
  0.0 3.9 %shard_map.155 = (bf16[136,512]{1,0:T(8,128)(2,1)}, bf16[136,512]{1,0:T(8,128)(2,1)}, bf16[136,512]{1,0:T(8,128)(2,1)}, bf16[136,512]{1,0:T(8,128)(2,1)}) custom-call(bf16[16,256]{1,0:T(8,128)(2,1)} %bitcast.20, bf16[16,1024]{1,0:T(8,128)(2,1)} %matrix.10, f32[1,1024]{1,0:T(1,128)} %bitcast.24, f32[4,256]{1,0:T(4,128)} %bitcast.28, ...), custom_call_target="tpu_custom_call" | custom-call | flops 800000000 | bytes 1000000 | tf_op jit(solution)/shard_map/pallas_call | solution.py:108
  3.9 3.0 %collective-permute-start.7 = (bf16[136,512]{1,0:T(8,128)(2,1)}, bf16[136,512]{1,0:T(8,128)(2,1)S(1)}, u32[]{:S(2)}, u32[]{:S(2)}) collective-permute-start(bf16[136,512]{1,0:T(8,128)(2,1)} %get-tuple-element.86), channel_id=1, source_target_pairs={{0,4},{4,0},{8,12},{12,8},{16,20},{20,16},{24,28},{28,24},{1,5},{5... | collective-permute-start | bytes 417800 | tf_op jit(solution)/shard_map/ppermute | solution.py:629
  8.5 3.0 %shard_map.156 = (bf16[136,512]{1,0:T(8,128)(2,1)S(1)}, bf16[136,512]{1,0:T(8,128)(2,1)S(1)}, bf16[136,512]{1,0:T(8,128)(2,1)S(1)}, bf16[136,512]{1,0:T(8,128)(2,1)S(1)}) custom-call(bf16[16,256]{1,0:T(8,128)(2,1)S(1)} %bitcast.21, bf16[16,1024]{1,0:T(8,128)(2,1)S(1)} %copy-done.11, f32[1,1024]{1,0:T(1,128)S(1)} %bitcast.25, f32[4,256]{1,0:T(4,128)S(1)} %bitcast.29, ...), custom_call_target="tpu_custom_call" | custom-call | flops 800000000 | bytes 1000000 | tf_op jit(solution)/shard_map/pallas_call | solution.py:108
  15.8 5.0 %collective-permute-start.10 = (bf16[128,512]{1,0:T(8,128)(2,1)S(1)}, bf16[128,512]{1,0:T(8,128)(2,1)S(1)}, u32[]{:S(2)}, u32[]{:S(2)}) collective-permute-start(bf16[128,512]{1,0:T(8,128)(2,1)S(1)} %total.3), channel_id=1, source_target_pairs={{0,16},{4,20},{8,24},{12,28},{1,17},{5,21},{9,25},{13,29},{2,18},{... | collective-permute-start | bytes 393224 | tf_op jit(solution)/shard_map/ppermute | solution.py:259
  21.5 5.0 %collective-permute-start.3 = (bf16[128,512]{1,0:T(8,128)(2,1)S(1)}, bf16[128,512]{1,0:T(8,128)(2,1)S(1)}, u32[]{:S(2)}, u32[]{:S(2)}) collective-permute-start(bf16[128,512]{1,0:T(8,128)(2,1)S(1)} %total.2), channel_id=1, source_target_pairs={{0,16},{4,20},{8,24},{12,28},{1,17},{5,21},{9,25},{13,29},{2,18},{... | collective-permute-start | bytes 393224 | tf_op jit(solution)/shard_map/ppermute | solution.py:259
  28.3 2.8 %collective-permute-start.12 = (bf16[128,512]{1,0:T(8,128)(2,1)S(1)}, bf16[128,512]{1,0:T(8,128)(2,1)S(1)}, u32[]{:S(2)}, u32[]{:S(2)}) collective-permute-start(bf16[128,512]{1,0:T(8,128)(2,1)S(1)} %get-tuple-element.102), channel_id=1, source_target_pairs={{0,8},{4,12},{8,0},{12,4},{16,24},{20,28},{24,16},{28,20},{1,9},{5... | collective-permute-start | bytes 393224 | tf_op jit(solution)/shard_map/ppermute | solution.py:629
  31.1 2.6 %shard_map.157 = (f32[256,1024]{1,0:T(8,128)S(1)}, bf16[256,512]{1,0:T(8,128)(2,1)S(1)}) custom-call(bf16[16,256]{1,0:T(8,128)(2,1)S(1)} %bitcast.22, bf16[16,1024]{1,0:T(8,128)(2,1)S(1)} %copy-done.11, f32[1,1024]{1,0:T(1,128)S(1)} %bitcast.26, f32[4,256]{1,0:T(4,128)S(1)} %bitcast.30, bf16[256,1024]{1,0:T(8,128)(2,1)S(1)} %copy-done.9, ...), custom_call_target="tpu_custom_call" | custom-call | flops 800000000 | bytes 2400000 | tf_op jit(solution)/shard_map/pallas_call | solution.py:171
  33.7 2.6 %shard_map.154 = (f32[256,1024]{1,0:T(8,128)S(1)}, bf16[256,512]{1,0:T(8,128)(2,1)S(1)}) custom-call(bf16[16,256]{1,0:T(8,128)(2,1)S(1)} %bitcast.23, bf16[16,1024]{1,0:T(8,128)(2,1)S(1)} %copy-done.11, f32[1,1024]{1,0:T(1,128)S(1)} %bitcast.27, f32[4,256]{1,0:T(4,128)S(1)} %bitcast.31, bf16[256,1024]{1,0:T(8,128)(2,1)S(1)} %copy-done.9, ...), custom_call_target="tpu_custom_call" | custom-call | flops 800000000 | bytes 2400000 | tf_op jit(solution)/shard_map/pallas_call | solution.py:171
  43.4 2.9 %collective-permute-done.6.refs_3_ = bf16[128,512]{1,0:T(8,128)(2,1)S(1)} collective-permute-done((bf16[128,512]{1,0:T(8,128)(2,1)S(1)}, bf16[128,512]{1,0:T(8,128)(2,1)S(1)}, u32[]{:S(2)}, u32[]{:S(2)}) %collective-permute-start.6) | collective-permute-done | bytes 131104 | tf_op jit(solution)/shard_map/ppermute | solution.py:629
  55.4 3.8 %collective-permute-done.18.refs_7_ = bf16[128,1024]{1,0:T(8,128)(2,1)S(1)} collective-permute-done((bf16[128,1024]{1,0:T(8,128)(2,1)S(1)}, bf16[128,1024]{1,0:T(8,128)(2,1)S(1)}, u32[]{:S(2)}, u32[]{:S(2)}) %collective-permute-start.18) | collective-permute-done | bytes 262176 | tf_op jit(solution)/shard_map/ppermute | solution.py:629
  59.2 5.6 %collective-permute-done.17.refs_6_ = bf16[128,1024]{1,0:T(8,128)(2,1)S(1)} collective-permute-done((bf16[128,1024]{1,0:T(8,128)(2,1)S(1)}, bf16[128,1024]{1,0:T(8,128)(2,1)S(1)}, u32[]{:S(2)}, u32[]{:S(2)}) %collective-permute-start.17) | collective-permute-done | bytes 262176 | tf_op jit(solution)/shard_map/ppermute | solution.py:629
  64.8 4.8 %collective-permute-done.16.refs_5_ = bf16[64,2048]{1,0:T(8,128)(2,1)S(1)} collective-permute-done((bf16[64,2048]{1,0:T(8,128)(2,1)S(1)}, bf16[64,2048]{1,0:T(8,128)(2,1)S(1)}, u32[]{:S(2)}, u32[]{:S(2)}) %collective-permute-start.16) | collective-permute-done | bytes 262176 | tf_op jit(solution)/shard_map/ppermute | solution.py:629
  72.7 2.7 %collective-permute-start.23 = (bf16[32,2048]{1,0:T(8,128)(2,1)S(1)}, bf16[32,2048]{1,0:T(8,128)(2,1)S(1)}, u32[]{:S(2)}, u32[]{:S(2)}) collective-permute-start(bf16[32,2048]{1,0:T(8,128)(2,1)S(1)} %get-tuple-element.133), channel_id=1, source_target_pairs={{0,16},{4,20},{8,24},{12,28},{16,0},{20,4},{24,8},{28,12},{1,17},{... | collective-permute-start | bytes 393224 | tf_op jit(solution)/shard_map/ppermute | solution.py:629
  75.5 9.3 %collective-permute-done.23.refs_0_ = bf16[32,2048]{1,0:T(8,128)(2,1)S(1)} collective-permute-done((bf16[32,2048]{1,0:T(8,128)(2,1)S(1)}, bf16[32,2048]{1,0:T(8,128)(2,1)S(1)}, u32[]{:S(2)}, u32[]{:S(2)}) %collective-permute-start.23) | collective-permute-done | bytes 131104 | tf_op jit(solution)/shard_map/ppermute | solution.py:629
  84.9 2.8 %collective-permute-done.24.refs_1_ = bf16[32,2048]{1,0:T(8,128)(2,1)S(1)} collective-permute-done((bf16[32,2048]{1,0:T(8,128)(2,1)S(1)}, bf16[32,2048]{1,0:T(8,128)(2,1)S(1)}, u32[]{:S(2)}, u32[]{:S(2)}) %collective-permute-start.24) | collective-permute-done | bytes 131104 | tf_op jit(solution)/shard_map/ppermute | solution.py:629
  102.4 3.4 %collective-permute-start.38 = (bf16[32,2048]{1,0:T(8,128)(2,1)S(1)}, bf16[32,2048]{1,0:T(8,128)(2,1)S(1)}, u32[]{:S(2)}, u32[]{:S(2)}) collective-permute-start(bf16[32,2048]{1,0:T(8,128)(2,1)S(1)} %get-tuple-element.149), channel_id=1, source_target_pairs={{0,24},{4,28},{8,16},{12,20},{16,8},{20,12},{24,0},{28,4},{1,25},{... | collective-permute-start | bytes 393224 | tf_op jit(solution)/shard_map/ppermute | solution.py:629
  107.0 2.6 %shard_map.160 = (f32[128,2048]{1,0:T(8,128)S(1)}, bf16[128,2048]{1,0:T(8,128)(2,1)S(1)}) custom-call(bf16[704,2048]{1,0:T(8,128)(2,1)S(1)} %get-tuple-element.124.gate, bf16[704,2048]{1,0:T(8,128)(2,1)S(1)} %get-tuple-element.125.widen, bf16[704,2048]{1,0:T(8,128)(2,1)S(1)} %get-tuple-element.126.down, bf16[32,2048]{1,0:T(8,128)(2,1)S(1)} %get-tuple-element.139.refs_0_, ...), custom_call_target="tpu_custom_call" | custom-call | flops 2400000000 | bytes 4000000 | tf_op jit(solution)/shard_map/pallas_call | solution.py:542
  109.8 3.8 %collective-permute-done.39.refs_1_ = bf16[32,2048]{1,0:T(8,128)(2,1)S(1)} collective-permute-done((bf16[32,2048]{1,0:T(8,128)(2,1)S(1)}, bf16[32,2048]{1,0:T(8,128)(2,1)S(1)}, u32[]{:S(2)}, u32[]{:S(2)}) %collective-permute-start.39) | collective-permute-done | bytes 131104 | tf_op jit(solution)/shard_map/ppermute | solution.py:629
  117.9 4.9 %collective-permute-start.36 = (bf16[32,2048]{1,0:T(8,128)(2,1)S(1)}, bf16[32,2048]{1,0:T(8,128)(2,1)S(1)}, u32[]{:S(2)}, u32[]{:S(2)}) collective-permute-start(bf16[32,2048]{1,0:T(8,128)(2,1)S(1)} %get-tuple-element.137), channel_id=1, source_target_pairs={{0,16},{4,20},{8,24},{12,28},{16,0},{20,4},{24,8},{28,12},{1,17},{... | collective-permute-start | bytes 393224 | tf_op jit(solution)/shard_map/ppermute | solution.py:629
  124.9 2.7 %collective-permute-start.44 = (bf16[32,2048]{1,0:T(8,128)(2,1)S(1)}, bf16[32,2048]{1,0:T(8,128)(2,1)S(1)}, u32[]{:S(2)}, u32[]{:S(2)}) collective-permute-start(bf16[32,2048]{1,0:T(8,128)(2,1)S(1)} %get-tuple-element.156), channel_id=1, source_target_pairs={{0,28},{4,24},{8,20},{12,16},{16,12},{20,8},{24,4},{28,0},{1,29},{... | collective-permute-start | bytes 393224 | tf_op jit(solution)/shard_map/ppermute | solution.py:629
  129.2 9.2 %collective-permute-done.36.refs_4_ = bf16[32,2048]{1,0:T(8,128)(2,1)S(1)} collective-permute-done((bf16[32,2048]{1,0:T(8,128)(2,1)S(1)}, bf16[32,2048]{1,0:T(8,128)(2,1)S(1)}, u32[]{:S(2)}, u32[]{:S(2)}) %collective-permute-start.36) | collective-permute-done | bytes 131104 | tf_op jit(solution)/shard_map/ppermute | solution.py:629
  138.4 3.7 %collective-permute-done.37.refs_5_ = bf16[32,2048]{1,0:T(8,128)(2,1)S(1)} collective-permute-done((bf16[32,2048]{1,0:T(8,128)(2,1)S(1)}, bf16[32,2048]{1,0:T(8,128)(2,1)S(1)}, u32[]{:S(2)}, u32[]{:S(2)}) %collective-permute-start.37) | collective-permute-done | bytes 131104 | tf_op jit(solution)/shard_map/ppermute | solution.py:629
  143.5 4.4 %collective-permute-done.35.refs_3_ = bf16[32,2048]{1,0:T(8,128)(2,1)S(1)} collective-permute-done((bf16[32,2048]{1,0:T(8,128)(2,1)S(1)}, bf16[32,2048]{1,0:T(8,128)(2,1)S(1)}, u32[]{:S(2)}, u32[]{:S(2)}) %collective-permute-start.35) | collective-permute-done | bytes 131104 | tf_op jit(solution)/shard_map/ppermute | solution.py:629
  152.2 4.2 %collective-permute-done.48.refs_5_ = bf16[64,1024]{1,0:T(8,128)(2,1)S(1)} collective-permute-done((bf16[64,1024]{1,0:T(8,128)(2,1)S(1)}, bf16[64,1024]{1,0:T(8,128)(2,1)S(1)}, u32[]{:S(2)}, u32[]{:S(2)}) %collective-permute-start.48) | collective-permute-done | bytes 131104 | tf_op jit(solution)/shard_map/ppermute | solution.py:629
  (136 shorter events, 60.2 us)
Async XLA Ops:
  3.9 11.2 %collective-permute-start.7 = (bf16[136,512]{1,0:T(8,128)(2,1)}, bf16[136,512]{1,0:T(8,128)(2,1)S(1)}, u32[]{:S(2)}, u32[]{:S(2)}) collective-permute-start(bf16[136,512]{1,0:T(8,128)(2,1)} %get-tuple-element.86), channel_id=1, source_target_pairs={{0,4},{4,0},{8,12},{12,8},{16,20},{20,16},{24,28},{28,24},{1,5},{5... | collective-permute-start | bytes 417800 | tf_op jit(solution)/shard_map/ppermute | solution.py:629
  6.9 8.2 %collective-permute-start.8 = (bf16[136,512]{1,0:T(8,128)(2,1)}, bf16[136,512]{1,0:T(8,128)(2,1)S(1)}, u32[]{:S(2)}, u32[]{:S(2)}) collective-permute-start(bf16[136,512]{1,0:T(8,128)(2,1)} %get-tuple-element.87), channel_id=1, source_target_pairs={{0,8},{4,12},{8,0},{12,4},{16,24},{20,28},{24,16},{28,20},{1,9},{5... | collective-permute-start | bytes 417800 | tf_op jit(solution)/shard_map/ppermute | solution.py:629
  8.5 7.0 %collective-permute-start.9 = (bf16[136,512]{1,0:T(8,128)(2,1)}, bf16[136,512]{1,0:T(8,128)(2,1)S(1)}, u32[]{:S(2)}, u32[]{:S(2)}) collective-permute-start(bf16[136,512]{1,0:T(8,128)(2,1)} %get-tuple-element.88), channel_id=1, source_target_pairs={{0,12},{4,8},{8,4},{12,0},{16,28},{20,24},{24,20},{28,16},{1,13},{... | collective-permute-start | bytes 417800 | tf_op jit(solution)/shard_map/ppermute | solution.py:629
  11.5 9.3 %collective-permute-start = (bf16[136,512]{1,0:T(8,128)(2,1)S(1)}, bf16[136,512]{1,0:T(8,128)(2,1)S(1)}, u32[]{:S(2)}, u32[]{:S(2)}) collective-permute-start(bf16[136,512]{1,0:T(8,128)(2,1)S(1)} %get-tuple-element.91), channel_id=1, source_target_pairs={{0,4},{4,0},{8,12},{12,8},{16,20},{20,16},{24,28},{28,24},{1,5},{5... | collective-permute-start | bytes 417800 | tf_op jit(solution)/shard_map/ppermute | solution.py:629
  13.5 7.3 %collective-permute-start.1 = (bf16[136,512]{1,0:T(8,128)(2,1)S(1)}, bf16[136,512]{1,0:T(8,128)(2,1)S(1)}, u32[]{:S(2)}, u32[]{:S(2)}) collective-permute-start(bf16[136,512]{1,0:T(8,128)(2,1)S(1)} %get-tuple-element.92), channel_id=1, source_target_pairs={{0,8},{4,12},{8,0},{12,4},{16,24},{20,28},{24,16},{28,20},{1,9},{5... | collective-permute-start | bytes 417800 | tf_op jit(solution)/shard_map/ppermute | solution.py:629
  15.8 10.6 %collective-permute-start.10 = (bf16[128,512]{1,0:T(8,128)(2,1)S(1)}, bf16[128,512]{1,0:T(8,128)(2,1)S(1)}, u32[]{:S(2)}, u32[]{:S(2)}) collective-permute-start(bf16[128,512]{1,0:T(8,128)(2,1)S(1)} %total.3), channel_id=1, source_target_pairs={{0,16},{4,20},{8,24},{12,28},{1,17},{5,21},{9,25},{13,29},{2,18},{... | collective-permute-start | bytes 393224 | tf_op jit(solution)/shard_map/ppermute | solution.py:259
  21.5 14.8 %collective-permute-start.3 = (bf16[128,512]{1,0:T(8,128)(2,1)S(1)}, bf16[128,512]{1,0:T(8,128)(2,1)S(1)}, u32[]{:S(2)}, u32[]{:S(2)}) collective-permute-start(bf16[128,512]{1,0:T(8,128)(2,1)S(1)} %total.2), channel_id=1, source_target_pairs={{0,16},{4,20},{8,24},{12,28},{1,17},{5,21},{9,25},{13,29},{2,18},{... | collective-permute-start | bytes 393224 | tf_op jit(solution)/shard_map/ppermute | solution.py:259
  27.1 13.3 %collective-permute-start.11 = (bf16[128,512]{1,0:T(8,128)(2,1)S(1)}, bf16[128,512]{1,0:T(8,128)(2,1)S(1)}, u32[]{:S(2)}, u32[]{:S(2)}) collective-permute-start(bf16[128,512]{1,0:T(8,128)(2,1)S(1)} %get-tuple-element.101), channel_id=1, source_target_pairs={{0,4},{4,0},{8,12},{12,8},{16,20},{20,16},{24,28},{28,24},{1,5},{5... | collective-permute-start | bytes 393224 | tf_op jit(solution)/shard_map/ppermute | solution.py:629
  28.3 12.2 %collective-permute-start.12 = (bf16[128,512]{1,0:T(8,128)(2,1)S(1)}, bf16[128,512]{1,0:T(8,128)(2,1)S(1)}, u32[]{:S(2)}, u32[]{:S(2)}) collective-permute-start(bf16[128,512]{1,0:T(8,128)(2,1)S(1)} %get-tuple-element.102), channel_id=1, source_target_pairs={{0,8},{4,12},{8,0},{12,4},{16,24},{20,28},{24,16},{28,20},{1,9},{5... | collective-permute-start | bytes 393224 | tf_op jit(solution)/shard_map/ppermute | solution.py:629
  31.1 9.4 %collective-permute-start.13 = (bf16[128,512]{1,0:T(8,128)(2,1)S(1)}, bf16[128,512]{1,0:T(8,128)(2,1)S(1)}, u32[]{:S(2)}, u32[]{:S(2)}) collective-permute-start(bf16[128,512]{1,0:T(8,128)(2,1)S(1)} %get-tuple-element.103), channel_id=1, source_target_pairs={{0,12},{4,8},{8,4},{12,0},{16,28},{20,24},{24,20},{28,16},{1,13},{... | collective-permute-start | bytes 393224 | tf_op jit(solution)/shard_map/ppermute | solution.py:629
  50.0 9.2 %collective-permute-start.18 = (bf16[128,1024]{1,0:T(8,128)(2,1)S(1)}, bf16[128,1024]{1,0:T(8,128)(2,1)S(1)}, u32[]{:S(2)}, u32[]{:S(2)}) collective-permute-start(bf16[128,1024]{1,0:T(8,128)(2,1)S(1)} %add_convert_fusion), channel_id=1, source_target_pairs={{0,2},{1,3},{2,0},{3,1},{4,6},{5,7},{6,4},{7,5},{8,10},{9,11},{10,... | collective-permute-start | bytes 786440 | tf_op jit(solution)/shard_map/ppermute | solution.py:629
  51.6 13.2 %collective-permute-start.17 = (bf16[128,1024]{1,0:T(8,128)(2,1)S(1)}, bf16[128,1024]{1,0:T(8,128)(2,1)S(1)}, u32[]{:S(2)}, u32[]{:S(2)}) collective-permute-start(bf16[128,1024]{1,0:T(8,128)(2,1)S(1)} %add_convert_fusion.1), channel_id=1, source_target_pairs={{0,2},{1,3},{2,0},{3,1},{4,6},{5,7},{6,4},{7,5},{8,10},{9,11},{10,... | collective-permute-start | bytes 786440 | tf_op jit(solution)/shard_map/ppermute | solution.py:629
  52.2 17.4 %collective-permute-start.16 = (bf16[64,2048]{1,0:T(8,128)(2,1)S(1)}, bf16[64,2048]{1,0:T(8,128)(2,1)S(1)}, u32[]{:S(2)}, u32[]{:S(2)}) collective-permute-start(bf16[64,2048]{1,0:T(8,128)(2,1)S(1)} %copy-done.5), channel_id=1, source_target_pairs={{0,2},{1,3},{2,0},{3,1},{4,6},{5,7},{6,4},{7,5},{8,10},{9,11},{10,... | collective-permute-start | bytes 786440 | tf_op jit(solution)/shard_map/ppermute | solution.py:629
  72.7 12.2 %collective-permute-start.23 = (bf16[32,2048]{1,0:T(8,128)(2,1)S(1)}, bf16[32,2048]{1,0:T(8,128)(2,1)S(1)}, u32[]{:S(2)}, u32[]{:S(2)}) collective-permute-start(bf16[32,2048]{1,0:T(8,128)(2,1)S(1)} %get-tuple-element.133), channel_id=1, source_target_pairs={{0,16},{4,20},{8,24},{12,28},{16,0},{20,4},{24,8},{28,12},{1,17},{... | collective-permute-start | bytes 393224 | tf_op jit(solution)/shard_map/ppermute | solution.py:629
  75.4 12.3 %collective-permute-start.24 = (bf16[32,2048]{1,0:T(8,128)(2,1)S(1)}, bf16[32,2048]{1,0:T(8,128)(2,1)S(1)}, u32[]{:S(2)}, u32[]{:S(2)}) collective-permute-start(bf16[32,2048]{1,0:T(8,128)(2,1)S(1)} %get-tuple-element.134), channel_id=1, source_target_pairs={{0,20},{4,16},{8,28},{12,24},{16,4},{20,0},{24,12},{28,8},{1,21},{... | collective-permute-start | bytes 393224 | tf_op jit(solution)/shard_map/ppermute | solution.py:629
  93.0 8.4 %collective-permute-start.22 = (bf16[32,2048]{1,0:T(8,128)(2,1)S(1)}, bf16[32,2048]{1,0:T(8,128)(2,1)S(1)}, u32[]{:S(2)}, u32[]{:S(2)}) collective-permute-start(bf16[32,2048]{1,0:T(8,128)(2,1)S(1)} %get-tuple-element.132), channel_id=1, source_target_pairs={{0,12},{4,8},{8,4},{12,0},{16,28},{20,24},{24,20},{28,16},{1,13},{... | collective-permute-start | bytes 393224 | tf_op jit(solution)/shard_map/ppermute | solution.py:629
  102.4 7.4 %collective-permute-start.38 = (bf16[32,2048]{1,0:T(8,128)(2,1)S(1)}, bf16[32,2048]{1,0:T(8,128)(2,1)S(1)}, u32[]{:S(2)}, u32[]{:S(2)}) collective-permute-start(bf16[32,2048]{1,0:T(8,128)(2,1)S(1)} %get-tuple-element.149), channel_id=1, source_target_pairs={{0,24},{4,28},{8,16},{12,20},{16,8},{20,12},{24,0},{28,4},{1,25},{... | collective-permute-start | bytes 393224 | tf_op jit(solution)/shard_map/ppermute | solution.py:629
  105.8 7.8 %collective-permute-start.39 = (bf16[32,2048]{1,0:T(8,128)(2,1)S(1)}, bf16[32,2048]{1,0:T(8,128)(2,1)S(1)}, u32[]{:S(2)}, u32[]{:S(2)}) collective-permute-start(bf16[32,2048]{1,0:T(8,128)(2,1)S(1)} %get-tuple-element.150), channel_id=1, source_target_pairs={{0,28},{4,24},{8,20},{12,16},{16,12},{20,8},{24,4},{28,0},{1,29},{... | collective-permute-start | bytes 393224 | tf_op jit(solution)/shard_map/ppermute | solution.py:629
  109.7 17.9 %collective-permute-start.32 = (bf16[128,2048]{1,0:T(8,128)(2,1)S(1)}, bf16[128,2048]{1,0:T(8,128)(2,1)S(1)}, u32[]{:S(2)}, u32[]{:S(2)}) collective-permute-start(bf16[128,2048]{1,0:T(8,128)(2,1)S(1)} %get-tuple-element.144), channel_id=1, source_target_pairs={{0,1},{1,0},{2,3},{3,2},{4,5},{5,4},{6,7},{7,6},{8,9},{9,8},{10,11... | collective-permute-start | bytes 1572872 | tf_op jit(solution)/shard_map/ppermute | solution.py:629
  117.9 20.4 %collective-permute-start.36 = (bf16[32,2048]{1,0:T(8,128)(2,1)S(1)}, bf16[32,2048]{1,0:T(8,128)(2,1)S(1)}, u32[]{:S(2)}, u32[]{:S(2)}) collective-permute-start(bf16[32,2048]{1,0:T(8,128)(2,1)S(1)} %get-tuple-element.137), channel_id=1, source_target_pairs={{0,16},{4,20},{8,24},{12,28},{16,0},{20,4},{24,8},{28,12},{1,17},{... | collective-permute-start | bytes 393224 | tf_op jit(solution)/shard_map/ppermute | solution.py:629
  122.8 19.3 %collective-permute-start.37 = (bf16[32,2048]{1,0:T(8,128)(2,1)S(1)}, bf16[32,2048]{1,0:T(8,128)(2,1)S(1)}, u32[]{:S(2)}, u32[]{:S(2)}) collective-permute-start(bf16[32,2048]{1,0:T(8,128)(2,1)S(1)} %get-tuple-element.138), channel_id=1, source_target_pairs={{0,20},{4,16},{8,28},{12,24},{16,4},{20,0},{24,12},{28,8},{1,21},{... | collective-permute-start | bytes 393224 | tf_op jit(solution)/shard_map/ppermute | solution.py:629
  123.7 18.3 %collective-permute-start.43 = (bf16[32,2048]{1,0:T(8,128)(2,1)S(1)}, bf16[32,2048]{1,0:T(8,128)(2,1)S(1)}, u32[]{:S(2)}, u32[]{:S(2)}) collective-permute-start(bf16[32,2048]{1,0:T(8,128)(2,1)S(1)} %get-tuple-element.155), channel_id=1, source_target_pairs={{0,24},{4,28},{8,16},{12,20},{16,8},{20,12},{24,0},{28,4},{1,25},{... | collective-permute-start | bytes 393224 | tf_op jit(solution)/shard_map/ppermute | solution.py:629
  124.9 17.1 %collective-permute-start.44 = (bf16[32,2048]{1,0:T(8,128)(2,1)S(1)}, bf16[32,2048]{1,0:T(8,128)(2,1)S(1)}, u32[]{:S(2)}, u32[]{:S(2)}) collective-permute-start(bf16[32,2048]{1,0:T(8,128)(2,1)S(1)} %get-tuple-element.156), channel_id=1, source_target_pairs={{0,28},{4,24},{8,20},{12,16},{16,12},{20,8},{24,4},{28,0},{1,29},{... | collective-permute-start | bytes 393224 | tf_op jit(solution)/shard_map/ppermute | solution.py:629
  127.7 14.3 %collective-permute-start.33 = (bf16[32,2048]{1,0:T(8,128)(2,1)S(1)}, bf16[32,2048]{1,0:T(8,128)(2,1)S(1)}, u32[]{:S(2)}, u32[]{:S(2)}) collective-permute-start(bf16[32,2048]{1,0:T(8,128)(2,1)S(1)} %get-tuple-element.146), channel_id=1, source_target_pairs={{0,4},{4,0},{8,12},{12,8},{16,20},{20,16},{24,28},{28,24},{1,5},{5... | collective-permute-start | bytes 393224 | tf_op jit(solution)/shard_map/ppermute | solution.py:629
  (42 other events, 322.1 us)
